TPU v7x, 32 devices: a whole 2x2x4 slice. The times are simulated.
32 devices in a mesh: ep: 16 (over z, y, core), tp: 2 (over x).
Axes of the slice: x: 2, y: 2, z: 4, core: 2. Of those that a mesh axis runs over, the one named last changes fastest.
Arguments:
- tokens: bfloat16 [128, 1024], P(('ep', 'tp')), may hold values from -6 to 6
- lengths: int32 [128], P(('ep', 'tp')), may hold values from 256 to 1024, as said below
- cache_latent: bfloat16 [128, 1024, 256], P(('ep', 'tp')), may hold values from -160 to 160
- cache_rope: bfloat16 [128, 32, 1024], P(('ep', 'tp')), may hold values from -6 to 6
- attn_gain: float32 [1024], replicated, may hold values from 0.1 to 1.9
- latent_gain: float32 [256], replicated, may hold values from 0.1 to 1.9
- post_gain: float32 [1024], replicated, may hold values from 0.1 to 1.9
- ffn_gain: float32 [1024], replicated, may hold values from 0.1 to 1.9
- out_gain: float32 [1024], replicated, may hold values from 0.1 to 1.9
- w_latent: bfloat16 [1024, 256], P(None, 'tp'), may hold values from -0.1875 to 0.1875
- w_rope_key: bfloat16 [1024, 32], replicated, may hold values from -0.1875 to 0.1875
- w_query: bfloat16 [1024, 768], P(None, 'tp'), may hold values from -0.1875 to 0.1875
- w_absorb_key: bfloat16 [8, 64, 256], P('tp'), may hold values from -0.75 to 0.75
- w_absorb_value: bfloat16 [8, 256, 64], P('tp'), may hold values from -0.375 to 0.375
- w_out: bfloat16 [512, 1024], P('tp'), may hold values from -0.25 to 0.25
- routes: int32 [128, 6], P(('ep', 'tp')), may hold values from 0 to 15, all different within a row; in each aligned block of 8 rows (0 to 7, 8 to 15, ...) at most 5 rows name the same one
- route_weights: float32 [128, 6], P(('ep', 'tp')), may hold values from 0.2 to 1
- w_exp_gate: bfloat16 [16, 1024, 256], P('ep'), may hold values from -0.1875 to 0.1875
- w_exp_up: bfloat16 [16, 1024, 256], P('ep'), may hold values from -0.1875 to 0.1875
- w_exp_down: bfloat16 [16, 256, 1024], P('ep'), may hold values from -0.375 to 0.375
- w_dense_gate: bfloat16 [4096, 1024], P('ep'), may hold values from -0.1875 to 0.1875
- w_dense_up: bfloat16 [4096, 1024], P('ep'), may hold values from -0.1875 to 0.1875
- w_dense_down: bfloat16 [4096, 1024], P('ep'), may hold values from -0.09375 to 0.09375
- dense_gate_vector: float32 [1024], replicated, may hold values from -0.1875 to 0.1875
Outputs:
- output: bfloat16 [128, 1024], P(('ep', 'tp'))
- new_latent: bfloat16 [128, 256], P(('ep', 'tp'))
- new_rope_key: bfloat16 [128, 32], P(('ep', 'tp'))
Inputs may be any that keep to these rules, and one draw needn't show every extreme that they name: `routes`: in each aligned block of 8 rows no expert is named by more than 5 rows; each row names 6 different experts. `lengths`: some sequence holds exactly 1024 cached positions.
All inputs are finite; a program needn't handle non-finite values.
Results may differ from a plain program's by a relative error of at most 0.015.
Values may be sent and summed in bfloat16 or wider, within the bound.
No kernel may reach another device: no remote copies, remote signals or barrier semaphores. Data moves between devices by JAX's collectives and lax.ppermute only.
A program may use at most 64 MiB of HBM per device.

v0:
```python
import jax
import jax.numpy as jnp
from jax import lax
from jax.sharding import PartitionSpec as P

epsilon = 1e-06
rope_base = 10000.0
negative = -1e30


def normalize(values, gain_vec):
    values = values.astype(jnp.float32)
    return (
        values * lax.rsqrt(jnp.mean(values * values, axis=-1, keepdims=True) + epsilon) * gain_vec
    )


def rotate(values, positions):
    half_width = values.shape[-1] // 2
    inverse = rope_base ** (-jnp.arange(half_width, dtype=jnp.float32) / half_width)
    angles = positions.astype(jnp.float32)[..., None] * inverse
    cosine = jnp.cos(angles)
    sine_part = jnp.sin(angles)
    first_half = values[..., :half_width]
    second = values[..., half_width:]
    return jnp.concatenate(
        [first_half * cosine - second * sine_part, first_half * sine_part + second * cosine],
        axis=-1,
    )


def attend(q_latent, q_rope, cache_lat, cache_rot, new_lat, new_rot, seq_lengths, scaling):
    scores = jnp.einsum("shc,slc->shl", q_latent, cache_lat, preferred_element_type=jnp.float32)
    scores = scores + jnp.einsum(
        "shr,srl->shl", q_rope, cache_rot, preferred_element_type=jnp.float32
    )
    scores = scores * scaling
    own_score = jnp.sum(
        q_latent.astype(jnp.float32) * new_lat.astype(jnp.float32)[:, None, :], axis=-1
    )
    own_score = (
        own_score
        + jnp.sum(q_rope.astype(jnp.float32) * new_rot.astype(jnp.float32)[:, None, :], axis=-1)
    ) * scaling
    visible = (
        jnp.arange(cache_lat.shape[1], dtype=jnp.int32)[None, None, :] < seq_lengths[:, None, None]
    )
    scores = jnp.where(visible, scores, negative)
    row_max = jnp.maximum(jnp.max(scores, axis=-1), own_score)
    weights = jnp.exp(scores - row_max[..., None])
    own_weight = jnp.exp(own_score - row_max)
    totals = jnp.sum(weights, axis=-1) + own_weight
    probabilities = (weights / totals[..., None]).astype(jnp.bfloat16)
    own_prob = (own_weight / totals).astype(jnp.bfloat16)
    mixed = jnp.einsum("shl,slc->shc", probabilities, cache_lat, preferred_element_type=jnp.float32)
    mixed = (
        mixed + own_prob.astype(jnp.float32)[..., None] * new_lat.astype(jnp.float32)[:, None, :]
    )
    return mixed.astype(jnp.bfloat16)


def expert_rows(rows_in, gate_w, up_w, down_w):
    model_width = rows_in.shape[-1]
    flattened = rows_in.reshape(-1, model_width)
    gate_pre = jnp.dot(flattened, gate_w, preferred_element_type=jnp.float32)
    up_proj = jnp.dot(flattened, up_w, preferred_element_type=jnp.float32)
    activity = (jax.nn.silu(gate_pre) * up_proj).astype(jnp.bfloat16)
    result = jnp.dot(activity, down_w, preferred_element_type=jnp.float32).astype(jnp.bfloat16)
    return result.reshape(rows_in.shape)


def rank_in_expert(flattened, experts):
    route_count = flattened.shape[0]
    onehot = (flattened[:, None] == jnp.arange(experts, dtype=jnp.int32)[None, :]).astype(
        jnp.float32
    )
    strictly = (jnp.arange(route_count)[:, None] > jnp.arange(route_count)[None, :]).astype(
        jnp.float32
    )
    earlier = jnp.dot(strictly, onehot, precision=lax.Precision.HIGHEST)
    return jnp.sum(earlier * onehot, axis=1).astype(jnp.int32)


def shards(
    tokens,
    lengths,
    cache_latent,
    cache_rope,
    attn_gain,
    latent_gain,
    post_gain,
    ffn_gain,
    out_gain,
    w_latent,
    w_rope_key,
    w_query,
    w_absorb_key,
    w_absorb_value,
    w_out,
    routes,
    route_weights,
    w_exp_gate,
    w_exp_up,
    w_exp_down,
    w_dense_gate,
    w_dense_up,
    w_dense_down,
    dense_gate_vector,
):
    own_rows = tokens.shape[0]
    model_width = tokens.shape[1]
    tp_count = lax.axis_size("tp")
    ep_count = lax.axis_size("ep")
    rope_width = w_rope_key.shape[1]
    nope_width = w_absorb_key.shape[1]
    head_span = nope_width + rope_width
    scaling = head_span ** (-0.5)
    top_count = routes.shape[1]
    group_size = own_rows * tp_count
    capacity = min(
        group_size, max(2, (3 * group_size * top_count + 2 * ep_count - 1) // (2 * ep_count))
    )
    hidden = normalize(tokens, attn_gain).astype(jnp.bfloat16)
    new_rope_key = rotate(
        jnp.dot(hidden, w_rope_key, preferred_element_type=jnp.float32), lengths
    ).astype(jnp.bfloat16)
    local_heads = w_absorb_key.shape[0]
    group_hidden = lax.all_gather(hidden, "tp", axis=0, tiled=True)
    latent_part = jnp.dot(group_hidden, w_latent, preferred_element_type=jnp.float32)
    latent_full = lax.all_to_all(latent_part, "tp", split_axis=0, concat_axis=1, tiled=True)
    new_latent = normalize(latent_full, latent_gain).astype(jnp.bfloat16)
    queries = jnp.dot(group_hidden, w_query, preferred_element_type=jnp.float32).astype(
        jnp.bfloat16
    )
    queries = queries.reshape(group_size, local_heads, head_span)
    query_latent = jnp.einsum(
        "shn,hnc->shc", queries[..., :nope_width], w_absorb_key, preferred_element_type=jnp.float32
    ).astype(jnp.bfloat16)
    query_latent, query_rope = (
        lax.all_to_all(query_latent, "tp", split_axis=0, concat_axis=1, tiled=True),
        lax.all_to_all(queries[..., nope_width:], "tp", split_axis=0, concat_axis=1, tiled=True),
    )
    query_rope = rotate(query_rope.astype(jnp.float32), lengths[:, None]).astype(jnp.bfloat16)
    attended = attend(
        query_latent,
        query_rope,
        cache_latent,
        cache_rope,
        new_latent,
        new_rope_key,
        lengths,
        scaling,
    )
    attended = lax.all_to_all(attended, "tp", split_axis=1, concat_axis=0, tiled=True)
    head_out = (
        jnp.einsum("shc,hcv->shv", attended, w_absorb_value, preferred_element_type=jnp.float32)
        .astype(jnp.bfloat16)
        .reshape(group_size, -1)
    )
    mixed = lax.psum_scatter(
        jnp.dot(head_out, w_out, preferred_element_type=jnp.float32).astype(jnp.bfloat16),
        "tp",
        scatter_dimension=0,
        tiled=True,
    ).astype(jnp.float32)
    residual = (tokens.astype(jnp.float32) + normalize(mixed, post_gain)).astype(jnp.bfloat16)
    ffn_in = normalize(residual, ffn_gain).astype(jnp.bfloat16)
    gate_w = w_exp_gate[0]
    up_w = w_exp_up[0]
    down_w = w_exp_down[0]
    flattened = routes.reshape(-1)
    order_rank = rank_in_expert(flattened, ep_count)
    slot_index = (flattened * capacity + order_rank).reshape(own_rows, top_count)
    dispatch = jnp.any(
        slot_index[None, :, :] == jnp.arange(ep_count * capacity, dtype=jnp.int32)[:, None, None],
        axis=-1,
    ).astype(jnp.bfloat16)
    outgoing = jnp.dot(dispatch, ffn_in, preferred_element_type=jnp.float32).astype(jnp.bfloat16)
    outgoing = outgoing.reshape(ep_count, capacity, model_width)
    result = expert_rows(
        lax.all_to_all(outgoing, "ep", split_axis=0, concat_axis=0, tiled=True),
        gate_w,
        up_w,
        down_w,
    )
    returned = lax.all_to_all(result, "ep", split_axis=0, concat_axis=0, tiled=True)
    picked = returned.reshape(ep_count * capacity, model_width)[slot_index].astype(jnp.float32)
    routed = jnp.sum(route_weights[..., None] * picked, axis=1)
    piece_rows = lax.all_gather(ffn_in, "ep", axis=0, tiled=True)
    dims = (((1,), (1,)), ((), ()))
    gate_pre = lax.dot_general(piece_rows, w_dense_gate, dims, preferred_element_type=jnp.float32)
    up_proj = lax.dot_general(piece_rows, w_dense_up, dims, preferred_element_type=jnp.float32)
    dense_act = (jax.nn.silu(gate_pre) * up_proj).astype(jnp.bfloat16)
    dense_out = lax.psum_scatter(
        jnp.dot(dense_act, w_dense_down, preferred_element_type=jnp.float32),
        "ep",
        scatter_dimension=0,
        tiled=True,
    )
    dense_gate = jax.nn.sigmoid(jnp.sum(ffn_in.astype(jnp.float32) * dense_gate_vector, axis=-1))
    combined = routed + dense_gate[:, None] * dense_out
    output = (residual.astype(jnp.float32) + normalize(combined, out_gain)).astype(jnp.bfloat16)
    return (output, new_latent, new_rope_key)


def solution(mesh):
    placed = (
        P(("ep", "tp"), None),
        P(("ep", "tp")),
        P(("ep", "tp"), None, None),
        P(("ep", "tp"), None, None),
        P(),
        P(),
        P(),
        P(),
        P(),
        P(None, "tp"),
        P(),
        P(None, "tp"),
        P("tp", None, None),
        P("tp", None, None),
        P("tp", None),
        P(("ep", "tp"), None),
        P(("ep", "tp"), None),
        P("ep", None, None),
        P("ep", None, None),
        P("ep", None, None),
        P("ep", None),
        P("ep", None),
        P("ep", None),
        P(),
    )
    return jax.shard_map(
        shards,
        mesh=mesh,
        in_specs=placed,
        out_specs=(P(("ep", "tp"), None), P(("ep", "tp"), None), P(("ep", "tp"), None)),
        check_vma=False,
    )
```

profile of v0, /device:TPU:0, one launch (start us, length us, event | category | flops | bytes accessed | tf_op | source)
XLA Modules:
  0.0 204.9 jit_solution(364668685929764041)
XLA Ops:
  7.2 1.0 fusion.31
  8.2 0.8 fusion.54
  9.0 5.3 %all-gather = bf16[2,4,1024]{2,1,0:T(4,128)(2,1)S(1)} all-gather(bf16[1,4,1024]{2,1,0:T(4,128)(2,1)S(1)} %fusion.54), channel_id=1, replica_groups=mesh['ep'=16,'tp'=2] {'tp'}, dimensions={0}, use_global_device_ids=true | all-gather | bytes 24576 | tf_op jit(solution)/shard_map/all_gather | solution.py:128
  14.2 1.3 convolution_convert_fusion.5
  16.4 3.3 %all-to-all-start.1 = ((bf16[2,2,256]{2,1,0:T(2,128)(2,1)}), bf16[2,2,256]{2,1,0:T(2,128)(2,1)S(1)}, u32[]{:S(2)}, u32[]{:S(2)}) async-start(bf16[2,2,256]{2,1,0:T(2,128)(2,1)} %reshape.295), calls=%async_computation.1 | async-start | bytes 4096 | tf_op jit(solution)/shard_map/all_to_all | solution.py:141
  20.4 0.7 iota_compare_fusion
  21.1 1.1 fusion.52
  22.2 1.7 fusion.62
  23.9 0.8 eq.28
  25.6 1.0 fusion.6
  28.1 3.3 %all-to-all-start.2 = ((f32[2,4,128]{2,1,0:T(4,128)}), f32[2,4,128]{2,1,0:T(4,128)S(1)}, u32[]{:S(2)}, u32[]{:S(2)}) async-start(f32[2,4,128]{2,1,0:T(4,128)} %bitcast.9), calls=%async_computation.2 | async-start | bytes 8192 | tf_op jit(solution)/shard_map/all_to_all | solution.py:130
  31.7 3.5 %all-to-all-done.2 = f32[2,4,128]{2,1,0:T(4,128)S(1)} async-done(((f32[2,4,128]{2,1,0:T(4,128)}), f32[2,4,128]{2,1,0:T(4,128)S(1)}, u32[]{:S(2)}, u32[]{:S(2)}) %all-to-all-start.2) | async-done | bytes 4128 | tf_op jit(solution)/shard_map/all_to_all | solution.py:130
  35.2 3.2 %all-to-all-start = ((bf16[8,4,256]{2,1,0:T(4,128)(2,1)}), bf16[8,4,256]{2,1,0:T(4,128)(2,1)S(1)}, u32[]{:S(2)}, u32[]{:S(2)}) async-start(bf16[8,4,256]{2,1,0:T(4,128)(2,1)} %copy.49), calls=%async_computation | async-start | bytes 32768 | tf_op jit(solution)/shard_map/all_to_all | solution.py:140
  38.5 1.3 fusion.58
  39.9 2.4 %all-to-all-done = bf16[8,4,256]{2,1,0:T(4,128)(2,1)S(1)} async-done(((bf16[8,4,256]{2,1,0:T(4,128)(2,1)}), bf16[8,4,256]{2,1,0:T(4,128)(2,1)S(1)}, u32[]{:S(2)}, u32[]{:S(2)}) %all-to-all-start) | async-done | bytes 16416 | tf_op jit(solution)/shard_map/all_to_all | solution.py:140
  44.8 3.2 %all-to-all-start.3 = ((bf16[4,8,256]{2,0,1:T(4,128)(2,1)}), bf16[4,8,256]{2,0,1:T(4,128)(2,1)S(1)}, u32[]{:S(2)}, u32[]{:S(2)}) async-start(bf16[4,8,256]{2,0,1:T(4,128)(2,1)} %copy.55), calls=%async_computation.3 | async-start | bytes 32768 | tf_op jit(solution)/shard_map/all_to_all | solution.py:154
  49.5 2.4 %all-to-all-done.3 = bf16[4,8,256]{2,0,1:T(4,128)(2,1)S(1)} async-done(((bf16[4,8,256]{2,0,1:T(4,128)(2,1)}), bf16[4,8,256]{2,0,1:T(4,128)(2,1)S(1)}, u32[]{:S(2)}, u32[]{:S(2)}) %all-to-all-start.3) | async-done | bytes 16416 | tf_op jit(solution)/shard_map/all_to_all | solution.py:154
  52.4 6.7 %all-reduce = bf16[8,1024]{1,0:T(8,128)(2,1)S(1)} all-reduce(bf16[8,1024]{1,0:T(8,128)(2,1)S(1)} %convolution_convert_fusion.3), channel_id=2, replica_groups=mesh['ep'=16,'tp'=2] {'tp'}, use_global_device_ids=true, to_apply=%region_6.7.clone | all-reduce | flops 8192 | bytes 32768
  60.5 0.8 reshape.272
  61.2 6.4 %all-to-all-start.4 = ((bf16[16,5,1024]{2,1,0:T(8,128)(2,1)}), bf16[16,5,1024]{2,1,0:T(8,128)(2,1)S(1)}, u32[]{:S(2)}, u32[]{:S(2)}) async-start(bf16[16,5,1024]{2,1,0:T(8,128)(2,1)} %reshape.272), calls=%async_computation.4 | async-start | bytes 524288 | tf_op jit(solution)/shard_map/all_to_all | solution.py:181
  67.6 1.3 dynamic-slice.2
  69.6 22.1 %all-gather.1 = bf16[16,4,1024]{2,1,0:T(4,128)(2,1)S(1)} all-gather(bf16[1,4,1024]{2,1,0:T(4,128)(2,1)S(1)} %bitcast.76), channel_id=1, replica_groups=mesh['ep'=16,'tp'=2] {'ep'}, dimensions={0}, use_global_device_ids=true | all-gather | bytes 139264 | tf_op jit(solution)/shard_map/all_gather | solution.py:189
  91.7 0.9 fusion.63
  92.7 1.3 fusion.12
  93.9 1.7 convolution_convert_fusion
  95.7 0.8 reshape.274
  96.4 3.5 %all-to-all-start.5 = ((bf16[16,5,1024]{2,1,0:T(8,128)(2,1)}), bf16[16,5,1024]{2,1,0:T(8,128)(2,1)S(1)}, u32[]{:S(2)}, u32[]{:S(2)}) async-start(bf16[16,5,1024]{2,1,0:T(8,128)(2,1)} %reshape.274), calls=%async_computation.5 | async-start | bytes 524288 | tf_op jit(solution)/shard_map/all_to_all | solution.py:186
  100.0 2.3 %fusion.4 = f32[64,1024]{1,0:T(8,128)} fusion(bf16[256,1024]{1,0:T(8,128)(2,1)S(1)} %copy-done.1, bf16[64,1024]{1,0:T(8,128)(2,1)S(1)} %reshape.292, bf16[256,1024]{1,0:T(8,128)(2,1)} %param.45, f32[64,256]{1,0:T(8,128)S(1)} %copy-done.5), kind=kOutput, calls=%fused_computation.10 | convolution fusion | flops 67207168 | bytes 1507328 | tf_op jit(solution)/shard_map/dot_general | solution.py:195
  102.4 7.5 %all-to-all-done.5 = bf16[16,5,1024]{2,1,0:T(8,128)(2,1)S(1)} async-done(((bf16[16,5,1024]{2,1,0:T(8,128)(2,1)}), bf16[16,5,1024]{2,1,0:T(8,128)(2,1)S(1)}, u32[]{:S(2)}, u32[]{:S(2)}) %all-to-all-start.5) | async-done | bytes 163872 | tf_op jit(solution)/shard_map/all_to_all | solution.py:186
  110.8 84.8 %all-reduce.4.cloned.1.call-done = f32[64,1024]{1,0:T(8,128)} async-done(((f32[64,1024]{1,0:T(8,128)}), f32[64,1024]{1,0:T(8,128)}) %all-reduce.4.cloned.1.call-update) | async-done | bytes 262160
  195.6 0.9 multiply_reduce_fusion.2
  196.6 1.4 fusion.38
  (91 shorter events, 10.5 us)
Async XLA Ops:
  7.2 35.4 %copy-start = (bf16[4,1024,256]{2,1,0:T(8,128)(2,1)S(1)}, bf16[4,1024,256]{2,1,0:T(8,128)(2,1)}, u32[]{:S(2)}) copy-start(bf16[4,1024,256]{2,1,0:T(8,128)(2,1)} %param.26) | copy-start | bytes 6291460
  7.2 36.0 %copy-start.4 = (bf16[4,32,1024]{2,1,0:T(8,128)(2,1)S(1)}, bf16[4,32,1024]{2,1,0:T(8,128)(2,1)}, u32[]{:S(2)}) copy-start(bf16[4,32,1024]{2,1,0:T(8,128)(2,1)} %param.27) | copy-start | bytes 786436
  16.4 11.7 %all-to-all-start.1 = ((bf16[2,2,256]{2,1,0:T(2,128)(2,1)}), bf16[2,2,256]{2,1,0:T(2,128)(2,1)S(1)}, u32[]{:S(2)}, u32[]{:S(2)}) async-start(bf16[2,2,256]{2,1,0:T(2,128)(2,1)} %reshape.295), calls=%async_computation.1 | async-start | bytes 4096 | tf_op jit(solution)/shard_map/all_to_all | solution.py:141
  28.1 7.1 %all-to-all-start.2 = ((f32[2,4,128]{2,1,0:T(4,128)}), f32[2,4,128]{2,1,0:T(4,128)S(1)}, u32[]{:S(2)}, u32[]{:S(2)}) async-start(f32[2,4,128]{2,1,0:T(4,128)} %bitcast.9), calls=%async_computation.2 | async-start | bytes 8192 | tf_op jit(solution)/shard_map/all_to_all | solution.py:130
  35.2 7.1 %all-to-all-start = ((bf16[8,4,256]{2,1,0:T(4,128)(2,1)}), bf16[8,4,256]{2,1,0:T(4,128)(2,1)S(1)}, u32[]{:S(2)}, u32[]{:S(2)}) async-start(bf16[8,4,256]{2,1,0:T(4,128)(2,1)} %copy.49), calls=%async_computation | async-start | bytes 32768 | tf_op jit(solution)/shard_map/all_to_all | solution.py:140
  42.6 5.7 %copy-start.14 = (u32[32]{0:T(128)S(1)}, u32[32]{0:T(128)}, u32[]{:S(2)}) copy-start(u32[32]{0:T(128)} %constant.51) | copy-start | bytes 388
  43.2 8.7 %copy-start.6 = (bf16[4,256,64]{1,2,0:T(8,128)(2,1)S(1)}, bf16[4,256,64]{1,2,0:T(8,128)(2,1)}, u32[]{:S(2)}) copy-start(bf16[4,256,64]{1,2,0:T(8,128)(2,1)} %param.37) | copy-start | bytes 393220
  43.2 9.0 %copy-start.2 = (bf16[256,1024]{1,0:T(8,128)(2,1)S(1)}, bf16[256,1024]{1,0:T(8,128)(2,1)}, u32[]{:S(2)}) copy-start(bf16[256,1024]{1,0:T(8,128)(2,1)} %param.38) | copy-start | bytes 1572868
  43.2 16.0 %copy-start.7 = (bf16[4,1024]{1,0:T(4,128)(2,1)S(1)}, bf16[4,1024]{1,0:T(4,128)(2,1)}, u32[]{:S(2)}) copy-start(bf16[4,1024]{1,0:T(4,128)(2,1)} %param.24) | copy-start | bytes 24580
  43.2 16.0 %copy-start.10 = (f32[1024]{0:T(1024)S(1)}, f32[1024]{0:T(1024)}, u32[]{:S(2)}) copy-start(f32[1024]{0:T(1024)} %param.30) | copy-start | bytes 12292
  43.3 16.2 %copy-start.8 = (f32[1024]{0:T(1024)S(1)}, f32[1024]{0:T(1024)}, u32[]{:S(2)}) copy-start(f32[1024]{0:T(1024)} %param.47) | copy-start | bytes 12292
  43.3 16.2 %copy-start.9 = (f32[1024]{0:T(1024)S(1)}, f32[1024]{0:T(1024)}, u32[]{:S(2)}) copy-start(f32[1024]{0:T(1024)} %param.31) | copy-start | bytes 12292
  43.8 47.9 %copy-start.3 = (bf16[256,1024]{1,0:T(8,128)(2,1)S(1)}, bf16[256,1024]{1,0:T(8,128)(2,1)}, u32[]{:S(2)}) copy-start(bf16[256,1024]{1,0:T(8,128)(2,1)} %param.44) | copy-start | bytes 1572868
  44.8 7.1 %all-to-all-start.3 = ((bf16[4,8,256]{2,0,1:T(4,128)(2,1)}), bf16[4,8,256]{2,0,1:T(4,128)(2,1)S(1)}, u32[]{:S(2)}, u32[]{:S(2)}) async-start(bf16[4,8,256]{2,0,1:T(4,128)(2,1)} %copy.55), calls=%async_computation.3 | async-start | bytes 32768 | tf_op jit(solution)/shard_map/all_to_all | solution.py:154
  61.2 31.4 %all-to-all-start.4 = ((bf16[16,5,1024]{2,1,0:T(8,128)(2,1)}), bf16[16,5,1024]{2,1,0:T(8,128)(2,1)S(1)}, u32[]{:S(2)}, u32[]{:S(2)}) async-start(bf16[16,5,1024]{2,1,0:T(8,128)(2,1)} %reshape.272), calls=%async_computation.4 | async-start | bytes 524288 | tf_op jit(solution)/shard_map/all_to_all | solution.py:181
  91.7 8.4 %copy-start.1 = (bf16[256,1024]{1,0:T(8,128)(2,1)S(1)}, bf16[256,1024]{1,0:T(8,128)(2,1)}, u32[]{:S(2)}) copy-start(bf16[256,1024]{1,0:T(8,128)(2,1)} %param.46) | copy-start | bytes 1572868
  92.6 7.5 %copy-start.5 = (f32[64,256]{1,0:T(8,128)S(1)}, f32[64,256]{1,0:T(8,128)}, u32[]{:S(2)}) copy-start(f32[64,256]{1,0:T(8,128)} %fusion.63) | copy-start | bytes 196612
  93.9 8.5 %copy-start.13 = (f32[4]{0:T(128)S(1)}, f32[4]{0:T(128)}, u32[]{:S(2)}) copy-start(f32[4]{0:T(128)} %get-tuple-element.3) | copy-start | bytes 52
  95.7 15.0 %copy-start.12 = (f32[4,6]{1,0:T(4,128)S(1)}, f32[4,6]{1,0:T(4,128)}, u32[]{:S(2)}) copy-start(f32[4,6]{1,0:T(4,128)} %param.40) | copy-start | bytes 292
  95.7 100.9 %copy-start.11 = (f32[1024]{0:T(1024)S(1)}, f32[1024]{0:T(1024)}, u32[]{:S(2)}) copy-start(f32[1024]{0:T(1024)} %param.32) | copy-start | bytes 12292
  96.4 13.5 %all-to-all-start.5 = ((bf16[16,5,1024]{2,1,0:T(8,128)(2,1)}), bf16[16,5,1024]{2,1,0:T(8,128)(2,1)S(1)}, u32[]{:S(2)}, u32[]{:S(2)}) async-start(bf16[16,5,1024]{2,1,0:T(8,128)(2,1)} %reshape.274), calls=%async_computation.5 | async-start | bytes 524288 | tf_op jit(solution)/shard_map/all_to_all | solution.py:186
  100.0 95.7 %all-reduce.4.cloned.1.call-start = ((), (), s32[]{:S(2)}) async-start(), calls=%async_computation.6 | async-start | bytes 524288
Sparse Core Ops, SparseCore 0:
  104.2 91.4 all-reduce.3
where the time goes:
time: 206 us; the launch traced here: 205 us
  waiting for transfers between devices  101 us (49%)
  blocking collectives  34.1 us (17%)
  starting transfers between devices  23 us (11%)
  between operations  15.6 us (8%)
  matrix products  13.3 us (6%)
  other arithmetic  10.3 us (5%)
  local copies, waits for them, and re-layouts  7.86 us (4%)
    unnamed x2, waiting for transfers between devices  84.8 us
    all_gather x1, blocking collectives, shards(): piece_rows = lax.all_gather(ffn_in, 'ep', axis=0, tiled=True)  22.1 us
    all_to_all x1, waiting for transfers between devices, shards(): lax.all_to_all(result, 'ep', split_axis=0, concat_axis=0, tiled=True)  7.54 us
    unnamed x1, blocking collectives  6.72 us
    all_to_all x1, starting transfers between devices, shards(): lax.all_to_all(outgoing, 'ep', split_axis=0, concat_axis=0, tiled=True)  6.39 us
    all_gather x1, blocking collectives, shards(): group_hidden = lax.all_gather(hidden, 'tp', axis=0, tiled=True)  5.27 us
  transfers between devices with their start and end apart: 7, of which 5 were waited for; matrix products, arithmetic and copies ran while one was open for 8% of the time, Pallas kernels for 0%

commit v1 on v0

v1 whole, which is shorter than its diff:
```python
import jax
import jax.numpy as jnp
from jax import lax
from jax.sharding import PartitionSpec as P

epsilon = 1e-06
rope_base = 10000.0
negative = -1e30
f32 = jnp.float32
bf16 = jnp.bfloat16


def normalize(values, gain_vec):
    values = values.astype(f32)
    return (
        values * lax.rsqrt(jnp.mean(values * values, axis=-1, keepdims=True) + epsilon) * gain_vec
    )


def rotate(values, positions):
    half_width = values.shape[-1] // 2
    inverse = rope_base ** (-jnp.arange(half_width, dtype=f32) / half_width)
    angles = positions.astype(f32)[..., None] * inverse
    cosine = jnp.cos(angles)
    sine_part = jnp.sin(angles)
    first_half = values[..., :half_width]
    second = values[..., half_width:]
    return jnp.concatenate(
        [first_half * cosine - second * sine_part, first_half * sine_part + second * cosine],
        axis=-1,
    )


def split_float(values):
    high = lax.reduce_precision(values, 8, 7)
    return high.astype(bf16), (values - high).astype(bf16)


def join_float(high, low):
    return high.astype(f32) + low.astype(f32)


def shift(values, step, axis):
    count = lax.axis_size(axis)
    return lax.ppermute(values, axis, [(i, (i + step) % count) for i in range(count)])


def attend(q_latent, q_rope, cache_lat, cache_rot, new_lat, new_rot, seq_lengths, scaling):
    scores = jnp.einsum("shc,slc->shl", q_latent, cache_lat, preferred_element_type=f32)
    scores = scores + jnp.einsum("shr,srl->shl", q_rope, cache_rot, preferred_element_type=f32)
    scores = scores * scaling
    own_score = jnp.sum(q_latent.astype(f32) * new_lat.astype(f32)[:, None, :], axis=-1)
    own_score = (
        own_score + jnp.sum(q_rope.astype(f32) * new_rot.astype(f32)[:, None, :], axis=-1)
    ) * scaling
    visible = (
        jnp.arange(cache_lat.shape[1], dtype=jnp.int32)[None, None, :] < seq_lengths[:, None, None]
    )
    scores = jnp.where(visible, scores, negative)
    row_max = jnp.maximum(jnp.max(scores, axis=-1), own_score)
    weights = jnp.exp(scores - row_max[..., None])
    own_weight = jnp.exp(own_score - row_max)
    totals = jnp.sum(weights, axis=-1) + own_weight
    probabilities = (weights / totals[..., None]).astype(bf16)
    own_prob = (own_weight / totals).astype(bf16)
    mixed = jnp.einsum("shl,slc->shc", probabilities, cache_lat, preferred_element_type=f32)
    mixed = mixed + own_prob.astype(f32)[..., None] * new_lat.astype(f32)[:, None, :]
    return mixed.astype(bf16)


def shards(
    tokens,
    lengths,
    cache_latent,
    cache_rope,
    attn_gain,
    latent_gain,
    post_gain,
    ffn_gain,
    out_gain,
    w_latent,
    w_rope_key,
    w_query,
    w_absorb_key,
    w_absorb_value,
    w_out,
    routes,
    route_weights,
    w_exp_gate,
    w_exp_up,
    w_exp_down,
    w_dense_gate,
    w_dense_up,
    w_dense_down,
    dense_gate_vector,
):
    own_rows, model_width = tokens.shape
    tp_count = lax.axis_size("tp")
    ep_count = lax.axis_size("ep")
    me = lax.axis_index("tp")
    rope_width = w_rope_key.shape[1]
    local_heads, nope_width, rank = w_absorb_key.shape
    part = w_latent.shape[1]
    head_span = nope_width + rope_width
    scaling = head_span ** (-0.5)
    group_size = own_rows * tp_count

    rows = jnp.concatenate([tokens] + [shift(tokens, s, "tp") for s in range(1, tp_count)])
    hidden = normalize(rows, attn_gain).astype(bf16)
    new_rope_key = rotate(
        jnp.dot(hidden[:own_rows], w_rope_key, preferred_element_type=f32), lengths
    ).astype(bf16)
    latent_part = jnp.dot(hidden, w_latent, preferred_element_type=f32)
    queries = jnp.dot(hidden, w_query, preferred_element_type=f32).astype(bf16)
    queries = queries.reshape(group_size, local_heads, head_span)
    query_latent = jnp.einsum(
        "shn,hnc->shc", queries[..., :nope_width], w_absorb_key, preferred_element_type=f32
    ).astype(bf16)
    packed = jnp.concatenate(
        [
            query_latent.reshape(group_size, -1),
            queries[..., nope_width:].reshape(group_size, -1),
            *split_float(latent_part),
        ],
        axis=1,
    )
    blocks = [packed[:own_rows]] + [
        shift(packed[s * own_rows : (s + 1) * own_rows], -s, "tp") for s in range(1, tp_count)
    ]
    cut = local_heads * rank
    rope_cut = cut + local_heads * rope_width
    query_latent = jnp.concatenate(
        [b[:, :cut].reshape(own_rows, local_heads, rank) for b in blocks], axis=1
    )
    query_rope = jnp.concatenate(
        [b[:, cut:rope_cut].reshape(own_rows, local_heads, rope_width) for b in blocks], axis=1
    )
    pieces = [join_float(b[:, rope_cut : rope_cut + part], b[:, rope_cut + part :]) for b in blocks]
    columns = []
    for j in range(tp_count):
        column = pieces[0]
        for s in range(1, tp_count):
            column = jnp.where((me + s) % tp_count == j, pieces[s], column)
        columns.append(column)
    new_latent = normalize(jnp.concatenate(columns, axis=1), latent_gain).astype(bf16)
    query_rope = rotate(query_rope.astype(f32), lengths[:, None]).astype(bf16)
    attended = attend(
        query_latent, query_rope, cache_latent, cache_rope, new_latent, new_rope_key, lengths, scaling
    )
    attended = jnp.concatenate(
        [attended[:, :local_heads]]
        + [
            shift(attended[:, s * local_heads : (s + 1) * local_heads], s, "tp")
            for s in range(1, tp_count)
        ]
    )
    head_out = (
        jnp.einsum("shc,hcv->shv", attended, w_absorb_value, preferred_element_type=f32)
        .astype(bf16)
        .reshape(group_size, -1)
    )
    product = jnp.dot(head_out, w_out, preferred_element_type=f32).astype(bf16)
    mixed = product[:own_rows].astype(f32)
    for s in range(1, tp_count):
        mixed = mixed + shift(product[s * own_rows : (s + 1) * own_rows], -s, "tp").astype(f32)
    residual = (tokens.astype(f32) + normalize(mixed, post_gain)).astype(bf16)
    ffn_in = normalize(residual, ffn_gain).astype(bf16)
    dense_gate = jax.nn.sigmoid(jnp.sum(ffn_in.astype(f32) * dense_gate_vector, axis=-1))

    chosen = routes[:, :, None] == jnp.arange(ep_count, dtype=jnp.int32)[None, None, :]
    expert_weight = jnp.sum(jnp.where(chosen, route_weights[:, :, None], 0.0), axis=1)
    w_high, w_low = split_float(expert_weight.T)
    g_high, g_low = split_float(jnp.broadcast_to(dense_gate[None, :], (ep_count, own_rows)))
    extra = jnp.stack([w_high, w_low, g_high, g_low], axis=-1)
    extra = jnp.pad(extra, ((0, 0), (0, 0), (0, 124)))
    outgoing = jnp.concatenate(
        [jnp.broadcast_to(ffn_in[None], (ep_count, own_rows, model_width)), extra], axis=-1
    )
    arrived = lax.all_to_all(outgoing, "ep", split_axis=0, concat_axis=0, tiled=True)
    arrived = arrived.reshape(ep_count * own_rows, -1)
    all_rows = arrived[:, :model_width]
    extra = arrived[:, model_width:].astype(f32)
    row_weight = extra[:, 0:1] + extra[:, 1:2]
    row_gate = extra[:, 2:3] + extra[:, 3:4]
    gate_pre = jnp.dot(all_rows, w_exp_gate[0], preferred_element_type=f32)
    up_proj = jnp.dot(all_rows, w_exp_up[0], preferred_element_type=f32)
    activity = (jax.nn.silu(gate_pre) * up_proj).astype(bf16)
    result = jnp.dot(activity, w_exp_down[0], preferred_element_type=f32).astype(bf16)
    dims = (((1,), (1,)), ((), ()))
    gate_pre = lax.dot_general(all_rows, w_dense_gate, dims, preferred_element_type=f32)
    up_proj = lax.dot_general(all_rows, w_dense_up, dims, preferred_element_type=f32)
    dense_act = (jax.nn.silu(gate_pre) * up_proj).astype(bf16)
    dense_part = jnp.dot(dense_act, w_dense_down, preferred_element_type=f32)
    partial = (row_weight * result.astype(f32) + row_gate * dense_part).astype(bf16)
    returned = lax.all_to_all(
        partial.reshape(ep_count, own_rows, model_width),
        "ep",
        split_axis=0,
        concat_axis=0,
        tiled=True,
    )
    combined = jnp.sum(returned.astype(f32), axis=0)
    output = (residual.astype(f32) + normalize(combined, out_gain)).astype(bf16)
    return (output, new_latent, new_rope_key)


def solution(mesh):
    placed = (
        P(("ep", "tp"), None),
        P(("ep", "tp")),
        P(("ep", "tp"), None, None),
        P(("ep", "tp"), None, None),
        P(),
        P(),
        P(),
        P(),
        P(),
        P(None, "tp"),
        P(),
        P(None, "tp"),
        P("tp", None, None),
        P("tp", None, None),
        P("tp", None),
        P(("ep", "tp"), None),
        P(("ep", "tp"), None),
        P("ep", None, None),
        P("ep", None, None),
        P("ep", None, None),
        P("ep", None),
        P("ep", None),
        P("ep", None),
        P(),
    )
    return jax.shard_map(
        shards,
        mesh=mesh,
        in_specs=placed,
        out_specs=(P(("ep", "tp"), None), P(("ep", "tp"), None), P(("ep", "tp"), None)),
        check_vma=False,
    )
```

time: 206 us -> 59.7 us (0.29)
  waiting for transfers between devices: 101 us -> 7.24 us
  starting transfers between devices: 23 us -> 6.04 us
  between operations: 15.6 us -> 0.91 us
  blocking collectives: 34.1 us -> 24.4 us
  local copies, waits for them, and re-layouts: 7.86 us -> 2.74 us
  matrix products: 13.3 us -> 10.1 us
  other arithmetic: 10.3 us -> 7.7 us
    unnamed x2 -> x0, waiting for transfers between devices: 84.8 us -> none
    all_gather x2 -> x0, blocking collectives: 27.3 us -> none  [the longest x1 22.1 us: shards(): piece_rows = lax.all_gather(ffn_in, 'ep', axis=0, tiled=True)]
    all_to_all x0 -> x2, blocking collectives: none -> 24.4 us  [the longest x1 13.9 us: shards(): lax.all_to_all(outgoing, 'ep', split_axis=0, concat_axis=0, tiled=True)]
    all_to_all x6 -> x0, starting transfers between devices: 23 us -> none  [the longest x1 6.39 us: shards(): lax.all_to_all(outgoing, 'ep', split_axis=0, concat_axis=0, tiled=True)]
    all_to_all x6 -> x0, waiting for transfers between devices: 15.8 us -> none  [the longest x1 7.54 us: shards(): lax.all_to_all(result, 'ep', split_axis=0, concat_axis=0, tiled=True)]
    ppermute x0 -> x4, waiting for transfers between devices: none -> 7.24 us  [shift(): lax.ppermute(values, axis, [(i, (i + step) % count) for i in range(count)])]
    unnamed x1 -> x0, blocking collectives: 6.72 us -> none
    ppermute x0 -> x4, starting transfers between devices: none -> 6.04 us  [shift(): lax.ppermute(values, axis, [(i, (i + step) % count) for i in range(count)])]
  transfers between devices with their start and end apart: 7 -> 4, of which waited for: 5 -> 3; matrix products, arithmetic and copies ran while one was open for 8% -> 7% of each run, Pallas kernels for 0% -> 0%
where the time goes in v1:
time: 59.7 us; the launch traced here: 59.1 us
  blocking collectives  24.4 us (41%)
  matrix products  10.1 us (17%)
  other arithmetic  7.7 us (13%)
  waiting for transfers between devices  7.24 us (12%)
  starting transfers between devices  6.04 us (10%)
  local copies, waits for them, and re-layouts  2.74 us (5%)
  between operations  0.91 us (2%)
    all_to_all x1, blocking collectives, shards(): lax.all_to_all(outgoing, 'ep', split_axis=0, concat_axis=0, tiled=True)  13.9 us
    all_to_all x1, blocking collectives, shards(): lax.all_to_all(partial.reshape(ep_count, own_rows, model_width), 'ep', sp...  10.5 us
    ppermute x4, waiting for transfers between devices, shift(): lax.ppermute(values, axis, [(i, (i + step) % count) for i in range(count)])  7.24 us
    ppermute x4, starting transfers between devices, shift(): lax.ppermute(values, axis, [(i, (i + step) % count) for i in range(count)])  6.04 us
    dot_general x1, matrix products, shards(): dense_part = jnp.dot(dense_act, w_dense_down, preferred_element_type=f32)  1.77 us
    unnamed x25, local copies, waits for them, and re-layouts  1.73 us
    dot_general x1, matrix products, shards(): jnp.dot(activity, w_exp_down[0], preferred_element_type=f32).astype(bf16)  1.7 us
    reduce_sum x5, other arithmetic, normalize(): jnp.mean(values * values, axis=-1, keepdims=True) + epsilon  1.39 us
  transfers between devices with their start and end apart: 4, of which 3 were waited for; matrix products, arithmetic and copies ran while one was open for 7% of the time, Pallas kernels for 0%

profile of v1, /device:TPU:0, one launch (start us, length us, event | category | flops | bytes accessed | tf_op | source)
XLA Modules:
  0.0 59.1 jit_solution(14344937172174620412)
XLA Ops:
  0.7 3.0 %collective-permute-start = (bf16[4,1024]{1,0:T(4,128)(2,1)}, bf16[4,1024]{1,0:T(4,128)(2,1)S(1)}, u32[]{:S(2)}, u32[]{:S(2)}) collective-permute-start(bf16[4,1024]{1,0:T(4,128)(2,1)} %param.24), channel_id=1, source_target_pairs={{0,1},{1,0},{2,3},{3,2},{4,5},{5,4},{6,7},{7,6},{8,9},{9,8},{10,11... | collective-permute-start | bytes 24584 | tf_op jit(solution)/shard_map/ppermute | solution.py:45
  3.7 0.7 %iota_compare_fusion.1 = pred[4,1024]{1,0:T(4,128)(4,1)S(1)} fusion(s32[4]{0:T(128)} %param.25), kind=kLoop, calls=%fused_computation.84 | loop fusion | flops 4096 | bytes 4112 | tf_op jit(solution)/shard_map/lt | solution.py:57
  4.4 0.7 %convert_element_type.176 = f32[4]{0:T(128)S(1)} convert(s32[4]{0:T(128)} %param.25) | non-fusion elementwise | flops 4 | bytes 32 | tf_op jit(solution)/shard_map/convert_element_type | solution.py:23
  5.1 0.8 %copy.67 = s32[4,6]{0,1:T(8,128)S(1)} copy(s32[4,6]{1,0:T(4,128)} %param.39) | data formatting | bytes 192 | tf_op args[15]
  5.9 0.8 %copy.68 = f32[4,6]{0,1:T(8,128)S(1)} copy(f32[4,6]{1,0:T(4,128)} %param.40) | data formatting | bytes 192 | tf_op args[16]
  6.6 0.8 %fusion.37 = f32[8]{0:T(128)S(1)} fusion(bf16[4,1024]{1,0:T(4,128)(2,1)S(1)} %collective-permute-done, bf16[4,1024]{1,0:T(4,128)(2,1)} %param.24), kind=kLoop, calls=%fused_computation.49 | loop fusion | flops 49144 | bytes 16416 | tf_op jit(solution)/shard_map/reduce_sum | solution.py:16
  7.5 0.8 %fusion.39 = bf16[8,1024]{1,0:T(8,128)(2,1)S(1)} fusion(f32[1024]{0:T(1024)} %param.28, f32[8]{0:T(128)S(1)} %add_rsqrt_fusion.4, bf16[4,1024]{1,0:T(4,128)(2,1)S(1)} %collective-permute-done, bf16[4,1024]{1,0:T(4,128)(2,1)} %param.24), kind=kLoop, calls=%fused_computation.51 | loop fusion | flops 57344 | bytes 36896 | tf_op jit(solution)/shard_map/convert_element_type | solution.py:109
  8.3 1.0 %fusion.54 = f32[4,32]{1,0:T(4,128)S(1)} fusion(bf16[1024,32]{0,1:T(8,128)(2,1)} %param.34, bf16[8,1024]{1,0:T(8,128)(2,1)S(1)} %fusion.39), kind=kOutput, calls=%fused_computation.90 | convolution fusion | flops 262144 | bytes 74240 | tf_op jit(solution)/shard_map/dot_general | solution.py:111
  9.2 1.1 %reduce-precision_convert_fusion = (bf16[8,128]{1,0:T(8,128)(2,1)S(1)}, bf16[8,128]{1,0:T(8,128)(2,1)S(1)}) fusion(bf16[8,1024]{1,0:T(8,128)(2,1)S(1)} %fusion.39, bf16[1024,128]{1,0:T(8,128)(2,1)} %param.33), kind=kOutput, calls=%fused_computation.96 | convolution fusion | flops 2101248 | bytes 282624 | tf_op jit(solution)/shard_map/dot_general | solution.py:113
  10.3 1.3 %convolution_convert_fusion.4 = bf16[8,384]{1,0:T(8,128)(2,1)S(1)} fusion(bf16[8,1024]{1,0:T(8,128)(2,1)S(1)} %fusion.39, bf16[1024,384]{1,0:T(8,128)(2,1)} %param.35), kind=kOutput, calls=%fused_computation.16 | convolution fusion | flops 6294528 | bytes 808960 | tf_op jit(solution)/shard_map/dot_general | solution.py:114
  11.9 1.0 %convolution_convert_fusion.1 = bf16[4,8,256]{2,1,0:T(8,128)(2,1)S(1)} fusion(bf16[4,64,256]{2,1,0:T(8,128)(2,1)} %param.36, bf16[8,4,64]{2,1,0:T(4,128)(2,1)S(1)} %bitcast.45), kind=kOutput, calls=%fused_computation.13 | convolution fusion | flops 1056768 | bytes 151552 | tf_op jit(solution)/shard_map/shn,hnc->shc/dot_general | solution.py:116
  13.0 1.0 %collective-permute-start.1 = (bf16[4,1408]{1,0:T(4,128)(2,1)S(1)}, bf16[4,1408]{1,0:T(4,128)(2,1)S(1)}, u32[]{:S(2)}, u32[]{:S(2)}) collective-permute-start(bf16[4,1408]{1,0:T(4,128)(2,1)S(1)} %pad_maximum_fusion.2), channel_id=1, source_target_pairs={{0,1},{1,0},{2,3},{3,2},{4,5},{5,4},{6,7},{7,6},{8,9},{9,8},{10,11... | collective-permute-start | bytes 33800 | tf_op jit(solution)/shard_map/ppermute | solution.py:45
  14.1 0.6 %fusion.72 = (f32[4,32]{1,0:T(4,128)S(1)}, bf16[4,32]{1,0:T(4,128)(2,1)}) fusion(bf16[4,16]{1,0:T(4,128)(2,1)S(1)} %get-tuple-element.26, bf16[4,16]{1,0:T(4,128)(2,1)S(1)} %get-tuple-element.25), kind=kLoop, calls=%fused_computation.136 | loop fusion | flops 640 | bytes 1024 | tf_op jit(solution)/shard_map/convert_element_type | solution.py:54
  14.8 1.9 %collective-permute-done.1 = bf16[4,1408]{1,0:T(4,128)(2,1)S(1)} collective-permute-done((bf16[4,1408]{1,0:T(4,128)(2,1)S(1)}, bf16[4,1408]{1,0:T(4,128)(2,1)S(1)}, u32[]{:S(2)}, u32[]{:S(2)}) %collective-permute-start.1) | collective-permute-done | bytes 11296 | tf_op jit(solution)/shard_map/ppermute | solution.py:45
  17.0 1.3 %fusion.73 = (f32[4,256]{1,0:T(4,128)S(1)}, bf16[4,256]{1,0:T(4,128)(2,1)}) fusion(f32[256]{0:T(256)} %param.29, f32[4]{0:T(128)S(1)} %add_rsqrt_fusion.3, f32[4,128]{1,0:T(4,128)S(1)} %get-tuple-element.20, f32[4,128]{1,0:T(4,128)S(1)} %get-tuple-element.19), kind=kLoop, calls=%fused_computation.137 | loop fusion | flops 5120 | bytes 11280 | tf_op jit(solution)/shard_map/convert_element_type | solution.py:52
  18.5 0.6 %fusion.52 = f32[4,8,1024]{2,1,0:T(8,128)S(1)} fusion(bf16[4,1024,256]{2,1,0:T(8,128)(2,1)S(1)} %copy-done, bf16[4,8,256]{2,0,1:T(4,128)(2,1)S(1)} %pad_maximum_fusion.1), kind=kOutput, calls=%fused_computation.74 | convolution fusion | flops 16777216 | bytes 2244608 | tf_op jit(solution)/shard_map/shc,slc->shl/dot_general | solution.py:49
  19.5 0.3 fusion.75
  20.0 0.4 fusion.24
  20.6 1.0 %collective-permute-start.2 = (bf16[4,4,256]{2,0,1:T(4,128)(2,1)S(1)}, bf16[4,4,256]{2,0,1:T(4,128)(2,1)S(1)}, u32[]{:S(2)}, u32[]{:S(2)}) collective-permute-start(bf16[4,4,256]{2,0,1:T(4,128)(2,1)S(1)} %get-tuple-element.18), channel_id=1, source_target_pairs={{0,1},{1,0},{2,3},{3,2},{4,5},{5,4},{6,7},{7,6},{8,9},{9,8},{10,11... | collective-permute-start | bytes 24584 | tf_op jit(solution)/shard_map/ppermute | solution.py:45
  21.7 2.7 %collective-permute-done.2 = bf16[4,4,256]{2,0,1:T(4,128)(2,1)S(1)} collective-permute-done((bf16[4,4,256]{2,0,1:T(4,128)(2,1)S(1)}, bf16[4,4,256]{2,0,1:T(4,128)(2,1)S(1)}, u32[]{:S(2)}, u32[]{:S(2)}) %collective-permute-start.2) | collective-permute-done | bytes 8224 | tf_op jit(solution)/shard_map/ppermute | solution.py:45
  24.6 0.2 convolution_convert_fusion.2
  24.8 1.1 %collective-permute-start.3 = (bf16[4,1024]{1,0:T(4,128)(2,1)S(1)}, bf16[4,1024]{1,0:T(4,128)(2,1)S(1)}, u32[]{:S(2)}, u32[]{:S(2)}) collective-permute-start(bf16[4,1024]{1,0:T(4,128)(2,1)S(1)} %slice.130), channel_id=1, source_target_pairs={{0,1},{1,0},{2,3},{3,2},{4,5},{5,4},{6,7},{7,6},{8,9},{9,8},{10,11... | collective-permute-start | bytes 24584 | tf_op jit(solution)/shard_map/ppermute | solution.py:45
  25.9 2.7 %collective-permute-done.3 = bf16[4,1024]{1,0:T(4,128)(2,1)S(1)} collective-permute-done((bf16[4,1024]{1,0:T(4,128)(2,1)S(1)}, bf16[4,1024]{1,0:T(4,128)(2,1)S(1)}, u32[]{:S(2)}, u32[]{:S(2)}) %collective-permute-start.3) | collective-permute-done | bytes 8224 | tf_op jit(solution)/shard_map/ppermute | solution.py:45
  28.7 0.2 fusion.45
  28.9 0.2 multiply_reduce_fusion.2
  29.5 13.9 %all_to_all.10 = bf16[16,4,1152]{2,1,0:T(4,128)(2,1)S(1)} all-to-all(bf16[16,4,1152]{2,1,0:T(4,128)(2,1)S(1)} %fusion.15), channel_id=1, replica_groups=mesh['ep'=16,'tp'=2] {'ep'}, dimensions={0} | all-to-all | bytes 294912 | tf_op jit(solution)/shard_map/all_to_all | solution.py:179
  43.7 0.3 fusion.19
  44.0 0.2 fusion.12
  44.2 1.7 %fusion.3 = f32[64,1024]{1,0:T(8,128)S(1)} fusion(bf16[1,256,1024]{2,1,0:T(8,128)(2,1)} %param.43, bf16[1,1024,256]{2,1,0:T(8,128)(2,1)} %param.42, f32[64]{0:T(128)S(1)} %get-tuple-element.4, bf16[64,1152]{1,0:T(8,128)(2,1)S(1)} %reshape.277, f32[64,256]{1,0:T(8,128)S(1)} %fusion.12), kind=kOutput, calls=%fused_computation.5 | convolution fusion | flops 67403776 | bytes 1507840 | tf_op jit(solution)/shard_map/dot_general | solution.py:188
  45.9 1.8 %fusion.1 = bf16[64,1024]{1,0:T(8,128)(2,1)S(1)} fusion(f32[64,1024]{1,0:T(8,128)S(1)} %fusion.3, bf16[256,1024]{1,0:T(8,128)(2,1)} %param.46, bf16[256,1024]{1,0:T(8,128)(2,1)} %param.45, f32[64]{0:T(128)S(1)} %get-tuple-element.3, bf16[64,1152]{1,0:T(8,128)(2,1)S(1)} %reshape.277, f32[64,256]{1,0:T(8,128)S(1)} %fusion.19), kind=kOutput, calls=%fused_computation.2 | convolution fusion | flops 67403776 | bytes 1638912 | tf_op jit(solution)/shard_map/dot_general | solution.py:193
  47.7 10.5 %all_to_all.11 = bf16[16,4,1024]{2,1,0:T(4,128)(2,1)S(1)} all-to-all(bf16[16,4,1024]{2,1,0:T(4,128)(2,1)S(1)} %reshape.278), channel_id=1, replica_groups=mesh['ep'=16,'tp'=2] {'ep'}, dimensions={0} | all-to-all | bytes 262144 | tf_op jit(solution)/shard_map/all_to_all | solution.py:195
  58.4 0.7 %fusion.48 = bf16[4,1024]{1,0:T(4,128)(2,1)} fusion(bf16[4,1024]{1,0:T(4,128)(2,1)S(1)} %get-tuple-element.10, f32[4,1024]{1,0:T(4,128)S(1)} %convert_reduce_fusion, f32[1024]{0:T(1024)S(1)} %copy-done.10, f32[4]{0:T(128)S(1)} %add_rsqrt_fusion), kind=kLoop, calls=%fused_computation.67 | loop fusion | flops 20480 | bytes 36880 | tf_op jit(solution)/shard_map/convert_element_type | solution.py:203
  (74 shorter events, 3.0 us)
Async XLA Ops:
  0.6 17.9 %copy-start = (bf16[4,1024,256]{2,1,0:T(8,128)(2,1)S(1)}, bf16[4,1024,256]{2,1,0:T(8,128)(2,1)}, u32[]{:S(2)}) copy-start(bf16[4,1024,256]{2,1,0:T(8,128)(2,1)} %param.26) | copy-start | bytes 6291460
  0.6 18.8 %copy-start.4 = (bf16[4,32,1024]{2,1,0:T(8,128)(2,1)S(1)}, bf16[4,32,1024]{2,1,0:T(8,128)(2,1)}, u32[]{:S(2)}) copy-start(bf16[4,32,1024]{2,1,0:T(8,128)(2,1)} %param.27) | copy-start | bytes 786436
  0.7 6.0 %collective-permute-start = (bf16[4,1024]{1,0:T(4,128)(2,1)}, bf16[4,1024]{1,0:T(4,128)(2,1)S(1)}, u32[]{:S(2)}, u32[]{:S(2)}) collective-permute-start(bf16[4,1024]{1,0:T(4,128)(2,1)} %param.24), channel_id=1, source_target_pairs={{0,1},{1,0},{2,3},{3,2},{4,5},{5,4},{6,7},{7,6},{8,9},{9,8},{10,11... | collective-permute-start | bytes 24584 | tf_op jit(solution)/shard_map/ppermute | solution.py:45
  13.0 3.7 %collective-permute-start.1 = (bf16[4,1408]{1,0:T(4,128)(2,1)S(1)}, bf16[4,1408]{1,0:T(4,128)(2,1)S(1)}, u32[]{:S(2)}, u32[]{:S(2)}) collective-permute-start(bf16[4,1408]{1,0:T(4,128)(2,1)S(1)} %pad_maximum_fusion.2), channel_id=1, source_target_pairs={{0,1},{1,0},{2,3},{3,2},{4,5},{5,4},{6,7},{7,6},{8,9},{9,8},{10,11... | collective-permute-start | bytes 33800 | tf_op jit(solution)/shard_map/ppermute | solution.py:45
  19.2 5.2 %copy-start.5 = (bf16[4,256,64]{1,2,0:T(8,128)(2,1)S(1)}, bf16[4,256,64]{1,2,0:T(8,128)(2,1)}, u32[]{:S(2)}) copy-start(bf16[4,256,64]{1,2,0:T(8,128)(2,1)} %param.37) | copy-start | bytes 393220
  19.2 5.4 %copy-start.1 = (bf16[256,1024]{1,0:T(8,128)(2,1)S(1)}, bf16[256,1024]{1,0:T(8,128)(2,1)}, u32[]{:S(2)}) copy-start(bf16[256,1024]{1,0:T(8,128)(2,1)} %param.38) | copy-start | bytes 1572868
  19.2 9.5 %copy-start.6 = (bf16[4,1024]{1,0:T(4,128)(2,1)S(1)}, bf16[4,1024]{1,0:T(4,128)(2,1)}, u32[]{:S(2)}) copy-start(bf16[4,1024]{1,0:T(4,128)(2,1)} %param.24) | copy-start | bytes 24580
  19.2 9.5 %copy-start.7 = (f32[1024]{0:T(1024)S(1)}, f32[1024]{0:T(1024)}, u32[]{:S(2)}) copy-start(f32[1024]{0:T(1024)} %param.30) | copy-start | bytes 12292
  19.2 9.7 %copy-start.8 = (f32[1024]{0:T(1024)S(1)}, f32[1024]{0:T(1024)}, u32[]{:S(2)}) copy-start(f32[1024]{0:T(1024)} %param.47) | copy-start | bytes 12292
  19.2 9.7 %copy-start.9 = (f32[1024]{0:T(1024)S(1)}, f32[1024]{0:T(1024)}, u32[]{:S(2)}) copy-start(f32[1024]{0:T(1024)} %param.31) | copy-start | bytes 12292
  20.0 23.7 %copy-start.2 = (bf16[256,1024]{1,0:T(8,128)(2,1)S(1)}, bf16[256,1024]{1,0:T(8,128)(2,1)}, u32[]{:S(2)}) copy-start(bf16[256,1024]{1,0:T(8,128)(2,1)} %param.44) | copy-start | bytes 1572868
  20.6 3.7 %collective-permute-start.2 = (bf16[4,4,256]{2,0,1:T(4,128)(2,1)S(1)}, bf16[4,4,256]{2,0,1:T(4,128)(2,1)S(1)}, u32[]{:S(2)}, u32[]{:S(2)}) collective-permute-start(bf16[4,4,256]{2,0,1:T(4,128)(2,1)S(1)} %get-tuple-element.18), channel_id=1, source_target_pairs={{0,1},{1,0},{2,3},{3,2},{4,5},{5,4},{6,7},{7,6},{8,9},{9,8},{10,11... | collective-permute-start | bytes 24584 | tf_op jit(solution)/shard_map/ppermute | solution.py:45
  24.8 19.2 %copy-start.3 = (bf16[1,1024,256]{2,1,0:T(8,128)(2,1)S(1)}, bf16[1,1024,256]{2,1,0:T(8,128)(2,1)}, u32[]{:S(2)}) copy-start(bf16[1,1024,256]{2,1,0:T(8,128)(2,1)} %param.41) | copy-start | bytes 1572868
  24.8 3.7 %collective-permute-start.3 = (bf16[4,1024]{1,0:T(4,128)(2,1)S(1)}, bf16[4,1024]{1,0:T(4,128)(2,1)S(1)}, u32[]{:S(2)}, u32[]{:S(2)}) collective-permute-start(bf16[4,1024]{1,0:T(4,128)(2,1)S(1)} %slice.130), channel_id=1, source_target_pairs={{0,1},{1,0},{2,3},{3,2},{4,5},{5,4},{6,7},{7,6},{8,9},{9,8},{10,11... | collective-permute-start | bytes 24584 | tf_op jit(solution)/shard_map/ppermute | solution.py:45
  44.2 14.3 %copy-start.10 = (f32[1024]{0:T(1024)S(1)}, f32[1024]{0:T(1024)}, u32[]{:S(2)}) copy-start(f32[1024]{0:T(1024)} %param.32) | copy-start | bytes 12292

commit v2 on v1

v2 whole, which is shorter than its diff:
```python
import functools

import jax
import jax.numpy as jnp
from jax import lax
from jax.experimental import pallas as pl
from jax.experimental.pallas import tpu as pltpu
from jax.sharding import PartitionSpec as P

epsilon = 1e-06
rope_base = 10000.0
negative = -1e30
f32 = jnp.float32
bf16 = jnp.bfloat16
LANES = 128


def shift(values, step, axis):
    count = lax.axis_size(axis)
    return lax.ppermute(values, axis, [(i, (i + step) % count) for i in range(count)])


def split_float(values):
    high = lax.reduce_precision(values, 8, 7)
    return high.astype(bf16), (values - high).astype(bf16)


def unit_rows(values):
    mean = jnp.mean(values * values, axis=-1, keepdims=True)
    return values * lax.rsqrt(mean + epsilon)


def mm(left, right):
    return jnp.dot(left, right, preferred_element_type=f32)


def mm_t(left, right):
    return lax.dot_general(left, right, (((1,), (1,)), ((), ())), preferred_element_type=f32)


def swap_halves(values):
    half = values.shape[-1] // 2
    return jnp.concatenate([values[:, half:], values[:, :half]], axis=-1)


def silu(values):
    return values / (1.0 + jnp.exp(-values))


def project_body(blocks, heads, *refs):
    tok = refs[:blocks]
    gain, cosine, sine, w_lat, w_rope, w_query, w_key = refs[blocks : blocks + 7]
    outs = refs[blocks + 7 : 2 * blocks + 7]
    rope_key_out, rope_key_own = refs[2 * blocks + 7 :]
    rows = tok[0].shape[0]
    nope, rank = w_key.shape[1:]
    rope = w_rope.shape[0]
    span = nope + rope
    part = w_lat.shape[1]
    values = jnp.concatenate([t[...].astype(f32) for t in tok], axis=0)
    hidden = (unit_rows(values) * gain[...]).astype(bf16)
    queries = mm(hidden, w_query[...])
    latent = mm(hidden, w_lat[...])
    rope_key = mm_t(hidden, w_rope[...])[:rows]
    rope_key = rope_key * cosine[...] + swap_halves(rope_key) * sine[...]
    rope_key_out[...] = rope_key.astype(bf16)
    rope_key_own[...] = rope_key.astype(bf16)
    high = latent.astype(bf16)
    low = (latent - high.astype(f32)).astype(bf16)
    cut = heads * rank
    for h in range(heads):
        nope_part = queries[:, h * span : h * span + nope].astype(bf16)
        absorbed = mm(nope_part, w_key[h]).astype(bf16)
        for s in range(blocks):
            outs[s][:, h * rank : (h + 1) * rank] = absorbed[s * rows : (s + 1) * rows]
    ropes = jnp.concatenate(
        [queries[:, h * span + nope : (h + 1) * span] for h in range(heads)], axis=-1
    ).astype(bf16)
    for s in range(blocks):
        mine = slice(s * rows, (s + 1) * rows)
        start = cut
        for value in (ropes, high, low):
            width = value.shape[1]
            outs[s][:, start : start + width] = value[mine]
            start += width


def prepare_body(lengths, inverse, routes, route_weights, cosine, sine, extra):
    angles = lengths[...].astype(f32) * inverse[...]
    sign = jnp.where(
        lax.broadcasted_iota(jnp.int32, angles.shape, 1) < angles.shape[1] // 2, -1.0, 1.0
    )
    cosine[...] = jnp.cos(angles)
    sine[...] = jnp.sin(angles) * sign
    experts, rows = extra.shape[:2]
    span = -(-experts // LANES) * LANES
    place = lax.broadcasted_iota(jnp.int32, (rows, span), 1)
    table = jnp.zeros((rows, span), f32)
    for k in range(routes.shape[1]):
        one = slice(k, k + 1)
        table = table + jnp.where(place == routes[:, one], route_weights[:, one], 0.0)
    high = table.astype(bf16).astype(f32)
    low = table - high
    lane = lax.broadcasted_iota(jnp.int32, (rows, LANES), 1)
    for e in range(experts):
        one = slice(e, e + 1)
        extra[e] = jnp.where(lane == 0, high[:, one], jnp.where(lane == 1, low[:, one], 0.0))


def attend_body(blocks, heads, scale, *refs):
    packed = refs[:blocks]
    rest = refs[blocks:]
    me_ref, len_ref, cosine, sine, rope_key, gain, cache_lat, cache_rot = rest[:8]
    new_latent_out = rest[8]
    attended = rest[9 : 9 + blocks]
    latents, ropes = rest[9 + blocks :]
    rows = packed[0].shape[0]
    length, rank = cache_lat.shape[1:]
    rope = cache_rot.shape[1]
    span_scale = scale
    part = rank // blocks
    cut = heads * rank
    rope_cut = cut + heads * rope
    me = me_ref[0]
    pieces = []
    for s in range(blocks):
        values = packed[s][...].astype(f32)
        for h in range(heads):
            g = s * heads + h
            latents[:, g, :] = values[:, h * rank : (h + 1) * rank]
            ropes[:, g, :] = values[:, cut + h * rope : cut + (h + 1) * rope]
        pieces.append(
            values[:, rope_cut : rope_cut + part] + values[:, rope_cut + part : rope_cut + 2 * part]
        )
    columns = []
    for j in range(blocks):
        column = pieces[0]
        for s in range(1, blocks):
            column = jnp.where((me + s) % blocks == j, pieces[s], column)
        columns.append(column)
    new_latent = (unit_rows(jnp.concatenate(columns, axis=-1)) * gain[...]).astype(bf16)
    new_latent_out[...] = new_latent
    new_latent = new_latent.astype(f32)
    new_rope = rope_key[...].astype(f32)
    position = lax.broadcasted_iota(jnp.int32, (blocks * heads, length), 1)
    for b in range(rows):
        one = slice(b, b + 1)
        q_lat = latents[b]
        q_rot = ropes[b]
        q_rot = q_rot * cosine[one, :] + swap_halves(q_rot) * sine[one, :]
        q_rot = q_rot.astype(bf16)
        scores = mm_t(q_lat.astype(bf16), cache_lat[b]) + mm(q_rot, cache_rot[b])
        own = jnp.sum(q_lat * new_latent[one], axis=-1, keepdims=True)
        own = own + jnp.sum(q_rot.astype(f32) * new_rope[one], axis=-1, keepdims=True)
        own = own * span_scale
        scores = jnp.where(position < len_ref[b], scores * span_scale, negative)
        top = jnp.maximum(jnp.max(scores, axis=-1, keepdims=True), own)
        weights = jnp.exp(scores - top)
        own = jnp.exp(own - top)
        total = jnp.sum(weights, axis=-1, keepdims=True) + own
        mixed = mm((weights / total).astype(bf16), cache_lat[b])
        own = (own / total).astype(bf16).astype(f32)
        mixed = (mixed + own * new_latent[one]).astype(bf16)
        for s in range(blocks):
            for h in range(heads):
                g = s * heads + h
                attended[s][one, h * rank : (h + 1) * rank] = mixed[g : g + 1]


def heads_body(blocks, heads, *refs):
    attended = refs[:blocks]
    value_t, w_out = refs[blocks : blocks + 2]
    products = refs[blocks + 2 :]
    rows = attended[0].shape[0]
    rank = value_t.shape[2]
    values = jnp.concatenate([a[...].astype(f32) for a in attended], axis=0).astype(bf16)
    pieces = [
        mm_t(values[:, h * rank : (h + 1) * rank], value_t[h]) for h in range(heads)
    ]
    product = mm(jnp.concatenate(pieces, axis=-1).astype(bf16), w_out[...]).astype(bf16)
    for s in range(blocks):
        products[s][...] = product[s * rows : (s + 1) * rows]


def residual_body(blocks, *refs):
    products = refs[:blocks]
    tokens, post_gain, ffn_gain, gate_vec, extra, residual_out, outgoing = refs[blocks:]
    rows = tokens.shape[0]
    mixed = products[0][...].astype(f32)
    for s in range(1, blocks):
        mixed = mixed + products[s][...].astype(f32)
    residual = (tokens[...].astype(f32) + unit_rows(mixed) * post_gain[...]).astype(bf16)
    residual_out[...] = residual
    ffn_in = (unit_rows(residual.astype(f32)) * ffn_gain[...]).astype(bf16)
    logit = jnp.sum(ffn_in.astype(f32) * gate_vec[...], axis=-1, keepdims=True)
    gate = 1.0 / (1.0 + jnp.exp(-logit))
    high = gate.astype(bf16).astype(f32)
    lane = lax.broadcasted_iota(jnp.int32, (rows, LANES), 1)
    gates = jnp.where(lane == 2, high, jnp.where(lane == 3, gate - high, 0.0))
    width = ffn_in.shape[1]
    for e in range(outgoing.shape[0]):
        outgoing[e, :, :width] = ffn_in
        outgoing[e, :, width:] = (extra[e] + gates).astype(bf16)


def hidden_units(rows, gate_w, up_w, product):
    return (silu(product(rows, gate_w[...])) * product(rows, up_w[...])).astype(bf16)


def units_body(arrived, exp_gate, exp_up, exp_down, gate_w, up_w, down_w, out):
    width = exp_gate.shape[0]
    rows = arrived[:, :width]
    extra = arrived[:, width:].astype(f32)
    row_weight = extra[:, 0:1] + extra[:, 1:2]
    row_gate = extra[:, 2:3] + extra[:, 3:4]
    routed = mm(hidden_units(rows, exp_gate, exp_up, mm), exp_down[...]).astype(bf16)
    dense = mm(hidden_units(rows, gate_w, up_w, mm_t), down_w[...])
    out[...] = (row_weight * routed.astype(f32) + row_gate * dense).astype(bf16)


def finish_body(returned, residual, gain, out):
    combined = returned[0].astype(f32)
    for e in range(1, returned.shape[0]):
        combined = combined + returned[e].astype(f32)
    out[...] = (residual[...].astype(f32) + unit_rows(combined) * gain[...]).astype(bf16)


VMEM = pl.BlockSpec(memory_space=pltpu.VMEM)
HBM = pl.BlockSpec(memory_space=pltpu.HBM)
SMEM = pl.BlockSpec(memory_space=pltpu.SMEM)


def call(body, shapes, specs, scratch, flops, limit, name, args):
    return pl.pallas_call(
        body,
        out_shape=[jax.ShapeDtypeStruct(s, t) for s, t in shapes],
        in_specs=specs,
        out_specs=[VMEM] * len(shapes),
        scratch_shapes=scratch,
        cost_estimate=pl.CostEstimate(flops=flops, bytes_accessed=1 << 20, transcendentals=0),
        compiler_params=pltpu.CompilerParams(vmem_limit_bytes=limit << 20),
        name=name,
    )(*args)


def shards(
    tokens,
    lengths,
    cache_latent,
    cache_rope,
    attn_gain,
    latent_gain,
    post_gain,
    ffn_gain,
    out_gain,
    w_latent,
    w_rope_key,
    w_query,
    w_absorb_key,
    w_absorb_value,
    w_out,
    routes,
    route_weights,
    w_exp_gate,
    w_exp_up,
    w_exp_down,
    w_dense_gate,
    w_dense_up,
    w_dense_down,
    dense_gate_vector,
):
    own_rows, model_width = tokens.shape
    tp_count = lax.axis_size("tp")
    ep_count = lax.axis_size("ep")
    rope_width = w_rope_key.shape[1]
    heads, nope_width, rank = w_absorb_key.shape
    part = w_latent.shape[1]
    scale = (nope_width + rope_width) ** (-0.5)
    others = range(1, tp_count)

    rows = [shift(tokens, s, "tp") for s in others]
    value_t = jnp.swapaxes(w_absorb_value, 1, 2)

    half = rope_width // 2
    inverse = rope_base ** (-(jnp.arange(rope_width, dtype=f32) % half) / half)
    cosine, sine, extra = call(
        prepare_body,
        [((own_rows, rope_width), f32)] * 2 + [((ep_count, own_rows, LANES), f32)],
        [VMEM] * 4,
        [],
        1 << 33,
        4,
        "prepare",
        [lengths.reshape(-1, 1), inverse.reshape(1, -1), routes, route_weights],
    )
    packed_width = heads * (rank + rope_width) + 2 * part
    *packed, new_rope_key, rope_key = call(
        functools.partial(project_body, tp_count, heads),
        [((own_rows, packed_width), bf16)] * tp_count + [((own_rows, rope_width), bf16)] * 2,
        [VMEM] * (tp_count + 7),
        [],
        1 << 33,
        6,
        "project",
        [tokens, *rows, attn_gain.reshape(1, -1), cosine, sine, w_latent, w_rope_key.T, w_query, w_absorb_key],
    )
    packed = [packed[0]] + [shift(packed[s], -s, "tp") for s in others]
    me = jnp.full((1,), lax.axis_index("tp"), jnp.int32)
    new_latent, *attended = call(
        functools.partial(attend_body, tp_count, heads, scale),
        [((own_rows, rank), bf16)] + [((own_rows, heads * rank), bf16)] * tp_count,
        [VMEM] * tp_count + [SMEM, SMEM] + [VMEM] * 6,
        [
            pltpu.VMEM((own_rows, tp_count * heads, rank), f32),
            pltpu.VMEM((own_rows, tp_count * heads, rope_width), f32),
        ],
        1 << 33,
        8,
        "attend",
        [*packed, me, lengths, cosine, sine, rope_key, latent_gain.reshape(1, -1), cache_latent, cache_rope],
    )
    attended = [attended[0]] + [shift(attended[s], s, "tp") for s in others]
    products = call(
        functools.partial(heads_body, tp_count, heads),
        [((own_rows, model_width), bf16)] * tp_count,
        [VMEM] * (tp_count + 2),
        [],
        1 << 31,
        4,
        "heads",
        [*attended, value_t, w_out],
    )
    products = [products[0]] + [shift(products[s], -s, "tp") for s in others]
    residual, outgoing = call(
        functools.partial(residual_body, tp_count),
        [
            ((own_rows, model_width), bf16),
            ((ep_count, own_rows, model_width + LANES), bf16),
        ],
        [VMEM] * (tp_count + 5),
        [],
        1 << 31,
        4,
        "residual",
        [*products, tokens, post_gain.reshape(1, -1), ffn_gain.reshape(1, -1), dense_gate_vector.reshape(1, -1), extra],
    )
    arrived = lax.all_to_all(outgoing, "ep", split_axis=0, concat_axis=0, tiled=True)
    (partial,) = call(
        units_body,
        [((ep_count * own_rows, model_width), bf16)],
        [VMEM] * 7,
        [],
        1 << 33,
        12,
        "units",
        [
            arrived.reshape(ep_count * own_rows, -1),
            w_exp_gate[0],
            w_exp_up[0],
            w_exp_down[0],
            w_dense_gate,
            w_dense_up,
            w_dense_down,
        ],
    )
    returned = lax.all_to_all(
        partial.reshape(ep_count, own_rows, model_width),
        "ep",
        split_axis=0,
        concat_axis=0,
        tiled=True,
    )
    (output,) = call(
        finish_body,
        [((own_rows, model_width), bf16)],
        [VMEM] * 3,
        [],
        1 << 30,
        2,
        "finish",
        [returned, residual, out_gain.reshape(1, -1)],
    )
    return (output, new_latent, new_rope_key)


def solution(mesh):
    placed = (
        P(("ep", "tp"), None),
        P(("ep", "tp")),
        P(("ep", "tp"), None, None),
        P(("ep", "tp"), None, None),
        P(),
        P(),
        P(),
        P(),
        P(),
        P(None, "tp"),
        P(),
        P(None, "tp"),
        P("tp", None, None),
        P("tp", None, None),
        P("tp", None),
        P(("ep", "tp"), None),
        P(("ep", "tp"), None),
        P("ep", None, None),
        P("ep", None, None),
        P("ep", None, None),
        P("ep", None),
        P("ep", None),
        P("ep", None),
        P(),
    )
    return jax.shard_map(
        shards,
        mesh=mesh,
        in_specs=placed,
        out_specs=(P(("ep", "tp"), None), P(("ep", "tp"), None), P(("ep", "tp"), None)),
        check_vma=False,
    )
```

time: 59.7 us -> 49.5 us (0.83)
  matrix products: 10.1 us -> 0 us
  other arithmetic: 7.7 us -> 0.02 us
  Pallas kernels: 0 us -> 6.52 us
  waiting for transfers between devices: 7.24 us -> 9.35 us
  starting transfers between devices: 6.04 us -> 4.7 us
    dot_general x13 -> x0, matrix products: 10.1 us -> none  [the longest x1 1.77 us: shards(): dense_part = jnp.dot(dense_act, w_dense_down, preferred_element_type=f32)]
    pallas_call x0 -> x7, Pallas kernels: none -> 6.52 us  [call(): pl.pallas_call(body, out_shape=[jax.ShapeDtypeStruct(s, t) for s, t in sh...]
    convert_element_type x11 -> x0, other arithmetic: 4.24 us -> none  [the longest x1 1.33 us: attend(): new_lat.astype(f32)[:, None, :]]
    reduce_sum x11 -> x0, other arithmetic: 2.17 us -> none  [the longest x5 1.39 us: normalize(): jnp.mean(values * values, axis=-1, keepdims=True) + epsilon]
    ppermute x4, waiting for transfers between devices: 7.24 us -> 9.35 us  [shift(): lax.ppermute(values, axis, [(i, (i + step) % count) for i in range(count)])]
    ppermute x4, starting transfers between devices: 6.04 us -> 4.7 us  [shift(): lax.ppermute(values, axis, [(i, (i + step) % count) for i in range(count)])]
    lt x1 -> x0, other arithmetic: 0.73 us -> none  [attend(): jnp.arange(cache_lat.shape[1], dtype=jnp.int32)[None, None, :]]
    unnamed x25 -> x48, local copies, waits for them, and re-layouts: 1.73 us -> 2.44 us
  transfers between devices with their start and end apart: 4 -> 4, of which waited for: 3 -> 3; matrix products, arithmetic and copies ran while one was open for 7% -> 2% of each run, Pallas kernels for 0% -> 0%
where the time goes in v2:
time: 49.5 us; the launch traced here: 49.3 us
  blocking collectives  24.5 us (49%)
  waiting for transfers between devices  9.35 us (19%)
  Pallas kernels  6.52 us (13%)
  starting transfers between devices  4.7 us (9%)
  local copies, waits for them, and re-layouts  3.28 us (7%)
  between operations  0.88 us (2%)
    all_to_all x1, blocking collectives, shards(): lax.all_to_all(outgoing, 'ep', split_axis=0, concat_axis=0, tiled=True)  14 us
    all_to_all x1, blocking collectives, shards(): lax.all_to_all(partial.reshape(ep_count, own_rows, model_width), 'ep', sp...  10.5 us
    ppermute x4, waiting for transfers between devices, shift(): lax.ppermute(values, axis, [(i, (i + step) % count) for i in range(count)])  9.35 us
    pallas_call x7, Pallas kernels, call(): pl.pallas_call(body, out_shape=[jax.ShapeDtypeStruct(s, t) for s, t in sh...  6.52 us
    ppermute x4, starting transfers between devices, shift(): lax.ppermute(values, axis, [(i, (i + step) % count) for i in range(count)])  4.7 us
    unnamed x48, local copies, waits for them, and re-layouts  2.44 us
  transfers between devices with their start and end apart: 4, of which 3 were waited for; matrix products, arithmetic and copies ran while one was open for 2% of the time, Pallas kernels for 0%

profile of v2, /device:TPU:0, one launch (start us, length us, event | category | flops | bytes accessed | tf_op | source)
XLA Modules:
  0.0 49.3 jit_solution(11054352049830339857)
XLA Ops:
  0.6 3.0 %collective-permute-start = (bf16[4,1024]{1,0:T(4,128)(2,1)}, bf16[4,1024]{1,0:T(4,128)(2,1)S(1)}, u32[]{:S(2)}, u32[]{:S(2)}) collective-permute-start(bf16[4,1024]{1,0:T(4,128)(2,1)} %refs_2_.1), channel_id=1, source_target_pairs={{0,1},{1,0},{2,3},{3,2},{4,5},{5,4},{6,7},{7,6},{8,9},{9,8},{10,11... | collective-permute-start | bytes 24584 | tf_op jit(solution)/shard_map/ppermute | solution.py:20
  3.7 0.7 %copy.27.lengths = s32[4,1]{1,0:T(4,128)S(1)} copy(s32[4,1]{0,1:T(1,128)} %bitcast.13) | data formatting | bytes 32 | tf_op jit(solution)/shard_map/reshape | solution.py:294
  4.4 0.7 %copy-done.21 = s32[4,6]{1,0:T(4,128)S(1)} copy-done((s32[4,6]{1,0:T(4,128)S(1)}, s32[4,6]{1,0:T(4,128)}, u32[]{:S(2)}) %copy-start.21) | copy-done | bytes 120
  5.1 0.7 %copy-done.22 = f32[4,6]{1,0:T(4,128)S(1)} copy-done((f32[4,6]{1,0:T(4,128)S(1)}, f32[4,6]{1,0:T(4,128)}, u32[]{:S(2)}) %copy-start.22) | copy-done | bytes 120
  5.8 0.0 copy-start.15
  5.8 0.0 copy-start.16
  5.8 0.2 prepare.1
  6.1 0.9 %copy-done.2 = bf16[1024,384]{1,0:T(8,128)(2,1)S(1)} copy-done((bf16[1024,384]{1,0:T(8,128)(2,1)S(1)}, bf16[1024,384]{1,0:T(8,128)(2,1)}, u32[]{:S(2)}) %copy-start.2) | copy-done | bytes 786456
  6.9 0.1 copy-done.10
  7.0 0.0 copy-done.12
  7.0 0.0 copy-start.1
  7.0 0.0 copy-start.11
  7.1 1.0 %project.1 = (bf16[4,1408]{1,0:T(4,128)(2,1)S(1)}, bf16[4,1408]{1,0:T(4,128)(2,1)S(1)}, bf16[4,32]{1,0:T(4,128)(2,1)}, bf16[4,32]{1,0:T(4,128)(2,1)S(1)}) custom-call(bf16[4,1024]{1,0:T(4,128)(2,1)S(1)} %copy-done.15, bf16[4,1024]{1,0:T(4,128)(2,1)S(1)} %collective-permute-done.refs_1_, f32[1,1024]{1,0:T(1,128)S(1)} %bitcast.19, ...), custom_call_target="tpu_custom_call" | custom-call | flops 8589934592 | bytes 1048576 | tf_op jit(solution)/shard_map/project/pallas_call | solution.py:234
  8.1 0.5 %collective-permute-start.1 = (bf16[4,1408]{1,0:T(4,128)(2,1)S(1)}, bf16[4,1408]{1,0:T(4,128)(2,1)S(1)}, u32[]{:S(2)}, u32[]{:S(2)}) collective-permute-start(bf16[4,1408]{1,0:T(4,128)(2,1)S(1)} %get-tuple-element.20), channel_id=1, source_target_pairs={{0,1},{1,0},{2,3},{3,2},{4,5},{5,4},{6,7},{7,6},{8,9},{9,8},{10,11... | collective-permute-start | bytes 33800 | tf_op jit(solution)/shard_map/ppermute | solution.py:20
  8.6 3.1 %collective-permute-done.1.refs_1_ = bf16[4,1408]{1,0:T(4,128)(2,1)S(1)} collective-permute-done((bf16[4,1408]{1,0:T(4,128)(2,1)S(1)}, bf16[4,1408]{1,0:T(4,128)(2,1)S(1)}, u32[]{:S(2)}, u32[]{:S(2)}) %collective-permute-start.1) | collective-permute-done | bytes 11296 | tf_op jit(solution)/shard_map/ppermute | solution.py:20
  11.8 3.0 %attend.1 = (bf16[4,256]{1,0:T(4,128)(2,1)}, bf16[4,1024]{1,0:T(4,128)(2,1)S(1)}, bf16[4,1024]{1,0:T(4,128)(2,1)S(1)}) custom-call(bf16[4,1408]{1,0:T(4,128)(2,1)S(1)} %get-tuple-element.19.refs_0_, bf16[4,1408]{1,0:T(4,128)(2,1)S(1)} %collective-permute-done.1.refs_1_, s32[1]{0:T(128)} %bitcast.3.refs_2_, s32[4]{0:T(128)S(1)} %copy-done, ...), custom_call_target="tpu_custom_call" | custom-call | flops 8589934592 | bytes 1048576 | tf_op jit(solution)/shard_map/attend/pallas_call | solution.py:234
  14.7 0.6 %collective-permute-start.2 = (bf16[4,1024]{1,0:T(4,128)(2,1)S(1)}, bf16[4,1024]{1,0:T(4,128)(2,1)S(1)}, u32[]{:S(2)}, u32[]{:S(2)}) collective-permute-start(bf16[4,1024]{1,0:T(4,128)(2,1)S(1)} %get-tuple-element.23), channel_id=1, source_target_pairs={{0,1},{1,0},{2,3},{3,2},{4,5},{5,4},{6,7},{7,6},{8,9},{9,8},{10,11... | collective-permute-start | bytes 24584 | tf_op jit(solution)/shard_map/ppermute | solution.py:20
  15.3 3.1 %collective-permute-done.2.refs_1_ = bf16[4,1024]{1,0:T(4,128)(2,1)S(1)} collective-permute-done((bf16[4,1024]{1,0:T(4,128)(2,1)S(1)}, bf16[4,1024]{1,0:T(4,128)(2,1)S(1)}, u32[]{:S(2)}, u32[]{:S(2)}) %collective-permute-start.2) | collective-permute-done | bytes 8224 | tf_op jit(solution)/shard_map/ppermute | solution.py:20
  18.4 0.0 copy-start.19
  18.4 0.4 heads.1
  18.8 0.6 %collective-permute-start.3 = (bf16[4,1024]{1,0:T(4,128)(2,1)S(1)}, bf16[4,1024]{1,0:T(4,128)(2,1)S(1)}, u32[]{:S(2)}, u32[]{:S(2)}) collective-permute-start(bf16[4,1024]{1,0:T(4,128)(2,1)S(1)} %get-tuple-element.25), channel_id=1, source_target_pairs={{0,1},{1,0},{2,3},{3,2},{4,5},{5,4},{6,7},{7,6},{8,9},{9,8},{10,11... | collective-permute-start | bytes 24584 | tf_op jit(solution)/shard_map/ppermute | solution.py:20
  19.3 3.1 %collective-permute-done.3.refs_1_ = bf16[4,1024]{1,0:T(4,128)(2,1)S(1)} collective-permute-done((bf16[4,1024]{1,0:T(4,128)(2,1)S(1)}, bf16[4,1024]{1,0:T(4,128)(2,1)S(1)}, u32[]{:S(2)}, u32[]{:S(2)}) %collective-permute-start.3) | collective-permute-done | bytes 8224 | tf_op jit(solution)/shard_map/ppermute | solution.py:20
  22.5 0.0 copy-start.4
  22.5 0.0 copy-start.7
  22.5 0.0 copy-start.8
  22.5 0.3 residual.1
  22.9 14.0 %all_to_all.10 = bf16[16,4,1152]{2,1,0:T(4,128)(2,1)S(1)} all-to-all(bf16[16,4,1152]{2,1,0:T(4,128)(2,1)S(1)} %get-tuple-element.27), channel_id=1, replica_groups=mesh['ep'=16,'tp'=2] {'ep'}, dimensions={0} | all-to-all | bytes 294912 | tf_op jit(solution)/shard_map/all_to_all | solution.py:347
  37.0 0.0 copy-start.20
  37.0 1.0 %units.1 = bf16[64,1024]{1,0:T(8,128)(2,1)S(1)} custom-call(bf16[64,1152]{1,0:T(8,128)(2,1)S(1)} %reshape.71.arrived, bf16[1024,256]{1,0:T(8,128)(2,1)S(1)} %bitcast.14, bf16[1024,256]{1,0:T(8,128)(2,1)S(1)} %bitcast.15, bf16[256,1024]{1,0:T(8,128)(2,1)S(1)} %bitcast.16, bf16[256,1024]{1,0:T(8,128)(2,1)S(1)} %copy-done.7, bf16[256,1024]{1,0:T(8,128)(2,1)S(1)} %copy-done.8, ...), custom_call_target="tpu_custom_call" | custom-call | flops 8589934592 | bytes 1048576 | tf_op jit(solution)/shard_map/units/pallas_call | solution.py:234
  38.0 0.1 reshape.72
  38.1 10.5 %all_to_all.11.returned = bf16[16,4,1024]{2,1,0:T(4,128)(2,1)S(1)} all-to-all(bf16[16,4,1024]{2,1,0:T(4,128)(2,1)S(1)} %reshape.72), channel_id=1, replica_groups=mesh['ep'=16,'tp'=2] {'ep'}, dimensions={0} | all-to-all | bytes 262144 | tf_op jit(solution)/shard_map/all_to_all | solution.py:366
  48.6 0.7 %finish.1 = bf16[4,1024]{1,0:T(4,128)(2,1)} custom-call(bf16[16,4,1024]{2,1,0:T(4,128)(2,1)S(1)} %all_to_all.11.returned, bf16[4,1024]{1,0:T(4,128)(2,1)S(1)} %get-tuple-element.28.residual, f32[1,1024]{1,0:T(1,128)S(1)} %bitcast.23), custom_call_target="tpu_custom_call" | custom-call | flops 1073741824 | bytes 1048576 | tf_op jit(solution)/shard_map/finish/pallas_call | solution.py:234
  (37 shorter events, 0.1 us)
Async XLA Ops:
  0.6 5.4 %collective-permute-start = (bf16[4,1024]{1,0:T(4,128)(2,1)}, bf16[4,1024]{1,0:T(4,128)(2,1)S(1)}, u32[]{:S(2)}, u32[]{:S(2)}) collective-permute-start(bf16[4,1024]{1,0:T(4,128)(2,1)} %refs_2_.1), channel_id=1, source_target_pairs={{0,1},{1,0},{2,3},{3,2},{4,5},{5,4},{6,7},{7,6},{8,9},{9,8},{10,11... | collective-permute-start | bytes 24584 | tf_op jit(solution)/shard_map/ppermute | solution.py:20
  4.4 0.7 %copy-start.21 = (s32[4,6]{1,0:T(4,128)S(1)}, s32[4,6]{1,0:T(4,128)}, u32[]{:S(2)}) copy-start(s32[4,6]{1,0:T(4,128)} %routes.1) | copy-start | bytes 292
  5.1 0.7 %copy-start.22 = (f32[4,6]{1,0:T(4,128)S(1)}, f32[4,6]{1,0:T(4,128)}, u32[]{:S(2)}) copy-start(f32[4,6]{1,0:T(4,128)} %route_weights.1) | copy-start | bytes 292
  5.8 1.1 %copy-start.2 = (bf16[1024,384]{1,0:T(8,128)(2,1)S(1)}, bf16[1024,384]{1,0:T(8,128)(2,1)}, u32[]{:S(2)}) copy-start(bf16[1024,384]{1,0:T(8,128)(2,1)} %refs_7_.1) | copy-start | bytes 2359300
  5.8 1.2 %copy-start.10 = (bf16[1024,128]{1,0:T(8,128)(2,1)S(1)}, bf16[1024,128]{1,0:T(8,128)(2,1)}, u32[]{:S(2)}) copy-start(bf16[1024,128]{1,0:T(8,128)(2,1)} %refs_5_.1) | copy-start | bytes 786436
  5.8 1.2 %copy-start.12 = (bf16[4,64,256]{2,1,0:T(8,128)(2,1)S(1)}, bf16[4,64,256]{2,1,0:T(8,128)(2,1)}, u32[]{:S(2)}) copy-start(bf16[4,64,256]{2,1,0:T(8,128)(2,1)} %refs_8_.2) | copy-start | bytes 393220
  5.8 1.2 %copy-start.14 = (bf16[1024,32]{0,1:T(8,128)(2,1)S(1)}, bf16[1024,32]{0,1:T(8,128)(2,1)}, u32[]{:S(2)}) copy-start(bf16[1024,32]{0,1:T(8,128)(2,1)} %param.34) | copy-start | bytes 196612
  5.8 1.2 %copy-start.15 = (bf16[4,1024]{1,0:T(4,128)(2,1)S(1)}, bf16[4,1024]{1,0:T(4,128)(2,1)}, u32[]{:S(2)}) copy-start(bf16[4,1024]{1,0:T(4,128)(2,1)} %refs_2_.1) | copy-start | bytes 24580
  5.8 1.2 %copy-start.16 = (f32[1024]{0:T(1024)S(1)}, f32[1024]{0:T(1024)}, u32[]{:S(2)}) copy-start(f32[1024]{0:T(1024)} %param.28) | copy-start | bytes 12292
  7.0 4.7 %copy-start = (s32[4]{0:T(128)S(1)}, s32[4]{0:T(128)}, u32[]{:S(2)}) copy-start(s32[4]{0:T(128)} %refs_3_.2) | copy-start | bytes 52
  7.0 4.7 %copy-start.1 = (bf16[4,1024,256]{2,1,0:T(8,128)(2,1)S(1)}, bf16[4,1024,256]{2,1,0:T(8,128)(2,1)}, u32[]{:S(2)}) copy-start(bf16[4,1024,256]{2,1,0:T(8,128)(2,1)} %refs_8_.3) | copy-start | bytes 6291460
  7.0 4.7 %copy-start.11 = (bf16[4,32,1024]{2,1,0:T(8,128)(2,1)S(1)}, bf16[4,32,1024]{2,1,0:T(8,128)(2,1)}, u32[]{:S(2)}) copy-start(bf16[4,32,1024]{2,1,0:T(8,128)(2,1)} %refs_9_.1) | copy-start | bytes 786436
  7.1 4.7 %copy-start.23 = (f32[256]{0:T(256)S(1)}, f32[256]{0:T(256)}, u32[]{:S(2)}) copy-start(f32[256]{0:T(256)} %param.29) | copy-start | bytes 3076
  8.1 3.7 %collective-permute-start.1 = (bf16[4,1408]{1,0:T(4,128)(2,1)S(1)}, bf16[4,1408]{1,0:T(4,128)(2,1)S(1)}, u32[]{:S(2)}, u32[]{:S(2)}) collective-permute-start(bf16[4,1408]{1,0:T(4,128)(2,1)S(1)} %get-tuple-element.20), channel_id=1, source_target_pairs={{0,1},{1,0},{2,3},{3,2},{4,5},{5,4},{6,7},{7,6},{8,9},{9,8},{10,11... | collective-permute-start | bytes 33800 | tf_op jit(solution)/shard_map/ppermute | solution.py:20
  11.8 6.6 %copy-start.3 = (bf16[256,1024]{1,0:T(8,128)(2,1)S(1)}, bf16[256,1024]{1,0:T(8,128)(2,1)}, u32[]{:S(2)}) copy-start(bf16[256,1024]{1,0:T(8,128)(2,1)} %refs_3_.3) | copy-start | bytes 1572868
  11.8 6.6 %copy-start.13 = (bf16[4,256,64]{1,2,0:T(8,128)(2,1)S(1)}, bf16[4,256,64]{1,2,0:T(8,128)(2,1)}, u32[]{:S(2)}) copy-start(bf16[4,256,64]{1,2,0:T(8,128)(2,1)} %param.37) | copy-start | bytes 393220
  14.7 3.7 %collective-permute-start.2 = (bf16[4,1024]{1,0:T(4,128)(2,1)S(1)}, bf16[4,1024]{1,0:T(4,128)(2,1)S(1)}, u32[]{:S(2)}, u32[]{:S(2)}) collective-permute-start(bf16[4,1024]{1,0:T(4,128)(2,1)S(1)} %get-tuple-element.23), channel_id=1, source_target_pairs={{0,1},{1,0},{2,3},{3,2},{4,5},{5,4},{6,7},{7,6},{8,9},{9,8},{10,11... | collective-permute-start | bytes 24584 | tf_op jit(solution)/shard_map/ppermute | solution.py:20
  18.4 4.0 %copy-start.17 = (f32[1024]{0:T(1024)S(1)}, f32[1024]{0:T(1024)}, u32[]{:S(2)}) copy-start(f32[1024]{0:T(1024)} %param.30) | copy-start | bytes 12292
  18.4 4.0 %copy-start.18 = (f32[1024]{0:T(1024)S(1)}, f32[1024]{0:T(1024)}, u32[]{:S(2)}) copy-start(f32[1024]{0:T(1024)} %param.31) | copy-start | bytes 12292
  18.4 4.0 %copy-start.19 = (f32[1024]{0:T(1024)S(1)}, f32[1024]{0:T(1024)}, u32[]{:S(2)}) copy-start(f32[1024]{0:T(1024)} %param.47) | copy-start | bytes 12292
  18.8 3.7 %collective-permute-start.3 = (bf16[4,1024]{1,0:T(4,128)(2,1)S(1)}, bf16[4,1024]{1,0:T(4,128)(2,1)S(1)}, u32[]{:S(2)}, u32[]{:S(2)}) collective-permute-start(bf16[4,1024]{1,0:T(4,128)(2,1)S(1)} %get-tuple-element.25), channel_id=1, source_target_pairs={{0,1},{1,0},{2,3},{3,2},{4,5},{5,4},{6,7},{7,6},{8,9},{9,8},{10,11... | collective-permute-start | bytes 24584 | tf_op jit(solution)/shard_map/ppermute | solution.py:20
  22.5 14.5 %copy-start.4 = (bf16[1,1024,256]{2,1,0:T(8,128)(2,1)S(1)}, bf16[1,1024,256]{2,1,0:T(8,128)(2,1)}, u32[]{:S(2)}) copy-start(bf16[1,1024,256]{2,1,0:T(8,128)(2,1)} %param.41) | copy-start | bytes 1572868
  22.5 14.5 %copy-start.5 = (bf16[1,1024,256]{2,1,0:T(8,128)(2,1)S(1)}, bf16[1,1024,256]{2,1,0:T(8,128)(2,1)}, u32[]{:S(2)}) copy-start(bf16[1,1024,256]{2,1,0:T(8,128)(2,1)} %param.42) | copy-start | bytes 1572868
  22.5 14.5 %copy-start.6 = (bf16[1,256,1024]{2,1,0:T(8,128)(2,1)S(1)}, bf16[1,256,1024]{2,1,0:T(8,128)(2,1)}, u32[]{:S(2)}) copy-start(bf16[1,256,1024]{2,1,0:T(8,128)(2,1)} %param.43) | copy-start | bytes 1572868
  22.5 14.5 %copy-start.7 = (bf16[256,1024]{1,0:T(8,128)(2,1)S(1)}, bf16[256,1024]{1,0:T(8,128)(2,1)}, u32[]{:S(2)}) copy-start(bf16[256,1024]{1,0:T(8,128)(2,1)} %gate_w.1) | copy-start | bytes 1572868
  22.5 14.5 %copy-start.8 = (bf16[256,1024]{1,0:T(8,128)(2,1)S(1)}, bf16[256,1024]{1,0:T(8,128)(2,1)}, u32[]{:S(2)}) copy-start(bf16[256,1024]{1,0:T(8,128)(2,1)} %up_w.1) | copy-start | bytes 1572868
  22.5 14.5 %copy-start.9 = (bf16[256,1024]{1,0:T(8,128)(2,1)S(1)}, bf16[256,1024]{1,0:T(8,128)(2,1)}, u32[]{:S(2)}) copy-start(bf16[256,1024]{1,0:T(8,128)(2,1)} %down_w.1) | copy-start | bytes 1572868
  37.0 11.6 %copy-start.20 = (f32[1024]{0:T(1024)S(1)}, f32[1024]{0:T(1024)}, u32[]{:S(2)}) copy-start(f32[1024]{0:T(1024)} %param.32) | copy-start | bytes 12292

commit v3 on v2

v3 whole, which is shorter than its diff:
```python
import functools
import math

import jax
import jax.numpy as jnp
from jax import lax
from jax.experimental import pallas as pl
from jax.experimental.pallas import tpu as pltpu
from jax.sharding import PartitionSpec as P


epsilon = 1e-06
rope_base = 10000.0
negative = -1e30
f32 = jnp.float32
bf16 = jnp.bfloat16
LANES = 128


def shift(values, step, axis):
    count = lax.axis_size(axis)
    return lax.ppermute(values, axis, [(i, (i + step) % count) for i in range(count)])


def unit_rows(values):
    mean = jnp.mean(values * values, axis=-1, keepdims=True)
    return values * lax.rsqrt(mean + epsilon)


def mm(left, right):
    return jnp.dot(left, right, preferred_element_type=f32)


def mm_t(left, right):
    return lax.dot_general(left, right, (((1,), (1,)), ((), ())), preferred_element_type=f32)


def swap_halves(values):
    half = values.shape[-1] // 2
    return jnp.concatenate([values[:, half:], values[:, :half]], axis=-1)


def silu(values):
    return values / (1.0 + jnp.exp(-values))


def project_body(blocks, heads, *refs):
    tok = refs[:blocks]
    gain, w_lat, w_rope, w_query, w_key = refs[blocks : blocks + 5]
    outs = refs[blocks + 5 : 2 * blocks + 5]
    raw_key = refs[2 * blocks + 5]
    rows = tok[0].shape[0]
    nope, rank = w_key.shape[1:]
    rope = w_rope.shape[0]
    span = nope + rope
    values = jnp.concatenate([t[...].astype(f32) for t in tok], axis=0)
    hidden = (unit_rows(values) * gain[...]).astype(bf16)
    queries = mm(hidden, w_query[...])
    latent = mm(hidden, w_lat[...])
    raw_key[...] = mm_t(hidden, w_rope[...])[:rows]
    high = latent.astype(bf16)
    low = (latent - high.astype(f32)).astype(bf16)
    cut = heads * rank
    for h in range(heads):
        nope_part = queries[:, h * span : h * span + nope].astype(bf16)
        absorbed = mm(nope_part, w_key[h]).astype(bf16)
        for s in range(blocks):
            outs[s][:, h * rank : (h + 1) * rank] = absorbed[s * rows : (s + 1) * rows]
    ropes = jnp.concatenate(
        [queries[:, h * span + nope : (h + 1) * span] for h in range(heads)], axis=-1
    ).astype(bf16)
    for s in range(blocks):
        mine = slice(s * rows, (s + 1) * rows)
        start = cut
        for value in (ropes, high, low):
            width = value.shape[1]
            outs[s][:, start : start + width] = value[mine]
            start += width


def frequency_body(out):
    half = out.shape[1] // 2
    place = lax.rem(lax.broadcasted_iota(jnp.int32, out.shape, 1), half).astype(f32)
    out[...] = jnp.exp(place * (-math.log(rope_base) / half))


def prepare_body(len_ref, inverse, raw_key, cosine, sine, key_out, key_own):
    rows = raw_key.shape[0]
    row = lax.broadcasted_iota(jnp.int32, (rows, 1), 0)
    position = jnp.zeros((rows, 1), f32)
    for b in range(rows):
        position = jnp.where(row == b, len_ref[b].astype(f32), position)
    angles = position * inverse[...]
    lane = lax.broadcasted_iota(jnp.int32, angles.shape, 1)
    cosines = jnp.cos(angles)
    sines = jnp.sin(angles) * jnp.where(lane < angles.shape[1] // 2, -1.0, 1.0)
    cosine[...] = cosines
    sine[...] = sines
    key = raw_key[...]
    key = (key * cosines + swap_halves(key) * sines).astype(bf16)
    key_out[...] = key
    key_own[...] = key


def attend_body(blocks, heads, scale, *refs):
    packed = refs[:blocks]
    rest = refs[blocks:]
    me_ref, len_ref, cosine, sine, rope_key, gain, cache_lat, cache_rot = rest[:8]
    new_latent_out = rest[8]
    attended = rest[9 : 9 + blocks]
    latents, ropes = rest[9 + blocks :]
    rows = packed[0].shape[0]
    length, rank = cache_lat.shape[1:]
    rope = cache_rot.shape[1]
    part = rank // blocks
    cut = heads * rank
    rope_cut = cut + heads * rope
    me = me_ref[0]
    pieces = []
    for s in range(blocks):
        values = packed[s][...].astype(f32)
        for h in range(heads):
            g = s * heads + h
            latents[:, g, :] = values[:, h * rank : (h + 1) * rank]
            ropes[:, g, :] = values[:, cut + h * rope : cut + (h + 1) * rope]
        pieces.append(
            values[:, rope_cut : rope_cut + part] + values[:, rope_cut + part : rope_cut + 2 * part]
        )
    columns = []
    for j in range(blocks):
        column = pieces[0]
        for s in range(1, blocks):
            column = jnp.where((me + s) % blocks == j, pieces[s], column)
        columns.append(column)
    new_latent = (unit_rows(jnp.concatenate(columns, axis=-1)) * gain[...]).astype(bf16)
    new_latent_out[...] = new_latent
    new_latent = new_latent.astype(f32)
    new_rope = rope_key[...].astype(f32)
    position = lax.broadcasted_iota(jnp.int32, (blocks * heads, length), 1)
    scores = []
    owns = []
    for b in range(rows):
        one = slice(b, b + 1)
        q_lat = latents[b]
        q_rot = ropes[b]
        q_rot = q_rot * cosine[one, :] + swap_halves(q_rot) * sine[one, :]
        q_rot = q_rot.astype(bf16)
        score = mm_t(q_lat.astype(bf16), cache_lat[b]) + mm(q_rot, cache_rot[b])
        scores.append(jnp.where(position < len_ref[b], score * scale, negative))
        own = jnp.sum(q_lat * new_latent[one], axis=-1, keepdims=True)
        own = own + jnp.sum(q_rot.astype(f32) * new_rope[one], axis=-1, keepdims=True)
        owns.append(own * scale)
    scores = jnp.concatenate(scores, axis=0)
    own = jnp.concatenate(owns, axis=0)
    top = jnp.maximum(jnp.max(scores, axis=-1, keepdims=True), own)
    weights = jnp.exp(scores - top)
    own = jnp.exp(own - top)
    total = jnp.sum(weights, axis=-1, keepdims=True) + own
    weights = (weights / total).astype(bf16).astype(f32)
    own = (own / total).astype(bf16).astype(f32)
    count = blocks * heads
    for b in range(rows):
        at = slice(b * count, (b + 1) * count)
        mixed = mm(weights[at].astype(bf16), cache_lat[b])
        mixed = (mixed + own[at] * new_latent[b : b + 1]).astype(bf16)
        for s in range(blocks):
            for h in range(heads):
                g = s * heads + h
                attended[s][b : b + 1, h * rank : (h + 1) * rank] = mixed[g : g + 1]


def mix_body(blocks, heads, cores, *refs):
    attended = refs[:blocks]
    core_ref, value_t, w_out = refs[blocks : blocks + 3]
    per_core = heads // cores
    count = (blocks - 1) * heads
    pieces = refs[blocks + 3 : blocks + 3 + count]
    rest = refs[blocks + 3 + count :]
    tokens, post_gain, ffn_gain, gate_vec, routes, route_weights, residual_out, outgoing = rest
    rows, width = tokens.shape
    rank = value_t.shape[1]
    span = value_t.shape[0] // heads
    core = core_ref[0]

    def columns(s, h):
        return attended[s][:, h * rank : (h + 1) * rank]

    outs = [mm_t(columns(0, h), value_t[h * span : (h + 1) * span]) for h in range(heads)]
    product = mm(jnp.concatenate(outs, axis=-1).astype(bf16), w_out[...])
    mixed = product.astype(bf16).astype(f32)
    for s in range(1, blocks):
        group = pieces[(s - 1) * heads : s * heads]
        product = jnp.zeros((rows, width), f32)
        for n, piece in enumerate(group):
            picked = columns(s, n)
            if cores == 2:
                swapped = columns(s, (n + per_core) % heads)
                picked = jnp.where(core == 0, picked.astype(f32), swapped.astype(f32)).astype(bf16)
            one_head = mm_t(picked, piece[:, width:]).astype(bf16)
            product = product + mm(one_head, piece[:, :width])
        mixed = mixed + product.astype(bf16).astype(f32)
    residual = (tokens[...].astype(f32) + unit_rows(mixed) * post_gain[...]).astype(bf16)
    residual_out[...] = residual
    ffn_in = (unit_rows(residual.astype(f32)) * ffn_gain[...]).astype(bf16)
    logit = jnp.sum(ffn_in.astype(f32) * gate_vec[...], axis=-1, keepdims=True)
    gate = 1.0 / (1.0 + jnp.exp(-logit))
    experts, _, total = outgoing.shape
    lane = lax.broadcasted_iota(jnp.int32, (rows, total - width), 1)
    place = jnp.where(lane < experts, lane, lane - experts)
    table = jnp.where(lane >= 2 * experts, gate, 0.0)
    for k in range(routes.shape[1]):
        at = slice(k, k + 1)
        named = jnp.logical_and(place == routes[:, at], lane < 2 * experts)
        table = table + jnp.where(named, route_weights[:, at], 0.0)
    high = table.astype(bf16).astype(f32)
    first = jnp.logical_or(lane < experts, lane == 2 * experts)
    extra = jnp.where(first, high, table - high).astype(bf16)
    for e in range(experts):
        outgoing[e, :, :width] = ffn_in
        outgoing[e, :, width:] = extra


def hidden_units(rows, gate_w, up_w, product):
    return (silu(product(rows, gate_w[...])) * product(rows, up_w[...])).astype(bf16)


def units_body(experts, arrived, exp_gate, exp_up, gate_w, up_w, *outs):
    weight_out, gate_out, routed_act, dense_act = outs
    width = exp_gate.shape[0]
    rows = arrived[:, :width]
    extra = arrived[:, width:].astype(f32)
    lane = lax.broadcasted_iota(jnp.int32, extra.shape, 1)
    mine = lax.axis_index("ep")
    named = jnp.logical_or(lane == mine, lane == mine + experts)
    row_weight = jnp.sum(jnp.where(named, extra, 0.0), axis=-1, keepdims=True)
    named = jnp.logical_or(lane == 2 * experts, lane == 2 * experts + 1)
    row_gate = jnp.sum(jnp.where(named, extra, 0.0), axis=-1, keepdims=True)
    weight_out[...] = row_weight
    gate_out[...] = row_gate
    routed_act[...] = hidden_units(rows, exp_gate, exp_up, mm)
    dense_act[...] = hidden_units(rows, gate_w, up_w, mm_t)


def down_body(row_weight, row_gate, routed_act, dense_act, exp_down, down_w, out):
    routed = mm(routed_act[...], exp_down[...]).astype(bf16)
    dense = mm(dense_act[...], down_w[...])
    out[...] = (row_weight[...] * routed.astype(f32) + row_gate[...] * dense).astype(bf16)


def finish_body(returned, residual, gain, out):
    combined = returned[0].astype(f32)
    for e in range(1, returned.shape[0]):
        combined = combined + returned[e].astype(f32)
    out[...] = (residual[...].astype(f32) + unit_rows(combined) * gain[...]).astype(bf16)


VMEM = pl.BlockSpec(memory_space=pltpu.VMEM)
HBM = pl.BlockSpec(memory_space=pltpu.HBM)
SMEM = pl.BlockSpec(memory_space=pltpu.SMEM)


def call(body, shapes, specs, scratch, flops, limit, args):
    return pl.pallas_call(
        body,
        out_shape=[jax.ShapeDtypeStruct(s, t) for s, t in shapes],
        in_specs=specs,
        out_specs=[VMEM] * len(shapes),
        scratch_shapes=scratch,
        cost_estimate=pl.CostEstimate(flops=flops, bytes_accessed=1 << 20, transcendentals=0),
        compiler_params=pltpu.CompilerParams(vmem_limit_bytes=limit << 20),
    )(*args)


def shards(
    tokens,
    lengths,
    cache_latent,
    cache_rope,
    attn_gain,
    latent_gain,
    post_gain,
    ffn_gain,
    out_gain,
    w_latent,
    w_rope_key,
    w_query,
    w_absorb_key,
    w_absorb_value,
    w_out,
    routes,
    route_weights,
    w_exp_gate,
    w_exp_up,
    w_exp_down,
    w_dense_gate,
    w_dense_up,
    w_dense_down,
    dense_gate_vector,
):
    own_rows, model_width = tokens.shape
    tp_count = lax.axis_size("tp")
    ep_count = lax.axis_size("ep")
    rope_width = w_rope_key.shape[1]
    heads, nope_width, rank = w_absorb_key.shape
    part = w_latent.shape[1]
    scale = (nope_width + rope_width) ** (-0.5)
    others = range(1, tp_count)
    extra_width = -(-(2 * ep_count + 2) // LANES) * LANES

    rows = [shift(tokens, s, "tp") for s in others]
    value_t = jnp.swapaxes(w_absorb_value, 1, 2)
    cores = 2 if ep_count % 2 == 0 and heads % 2 == 0 else 1
    core = lax.axis_index("ep") % cores
    per_core = heads // cores
    v_width = value_t.shape[1]
    flat_t = value_t.reshape(heads * v_width, rank)

    def head_weights(k):
        start = (core * per_core + k) * v_width
        return jnp.concatenate(
            [
                lax.dynamic_slice_in_dim(w_out, start, v_width),
                lax.dynamic_slice_in_dim(flat_t, start, v_width),
            ],
            axis=1,
        )

    shares = [head_weights(k) for k in range(per_core)]

    def swap_cores(values):
        return lax.ppermute(values, "ep", [(i, i ^ 1) for i in range(ep_count)])

    fetched = {}
    for s in others:
        fetched[s, 0] = shift(shares[0], -s, "tp")

    (inverse,) = call(frequency_body, [((1, rope_width), f32)], [], [], 1 << 32, 1, [])
    packed_width = heads * (rank + rope_width) + 2 * part
    *packed, raw_key = call(
        functools.partial(project_body, tp_count, heads),
        [((own_rows, packed_width), bf16)] * tp_count + [((own_rows, rope_width), f32)],
        [VMEM] * (tp_count + 5),
        [],
        1 << 32,
        6,
        [
            tokens,
            *rows,
            attn_gain.reshape(1, -1),
            w_latent,
            w_rope_key.T,
            w_query,
            w_absorb_key,
        ],
    )
    cosine, sine, new_rope_key, rope_key = call(
        prepare_body,
        [((own_rows, rope_width), f32)] * 2 + [((own_rows, rope_width), bf16)] * 2,
        [SMEM] + [VMEM] * 2,
        [],
        1 << 31,
        2,
        [lengths, inverse, raw_key],
    )
    mine = packed[0]
    packed = [mine] + [shift(packed[s], -s, "tp") for s in others]
    for k in range(1, per_core):
        late, _ = lax.optimization_barrier((shares[k], mine))
        for s in others:
            fetched[s, k] = shift(late, -s, "tp")
    pieces = []
    for s in others:
        group = [fetched[s, k] for k in range(per_core)]
        pieces += group
        if cores == 2:
            pieces += [swap_cores(piece) for piece in group]
    me = lax.axis_index("tp").reshape(1)
    new_latent, *attended = call(
        functools.partial(attend_body, tp_count, heads, scale),
        [((own_rows, rank), bf16)] + [((own_rows, heads * rank), bf16)] * tp_count,
        [VMEM] * tp_count + [SMEM, SMEM] + [VMEM] * 6,
        [
            pltpu.VMEM((own_rows, tp_count * heads, rank), f32),
            pltpu.VMEM((own_rows, tp_count * heads, rope_width), f32),
        ],
        1 << 29,
        8,
        [*packed, me, lengths, cosine, sine, rope_key, latent_gain.reshape(1, -1), cache_latent, cache_rope],
    )
    residual, outgoing = call(
        functools.partial(mix_body, tp_count, heads, cores),
        [
            ((own_rows, model_width), bf16),
            ((ep_count, own_rows, model_width + extra_width), bf16),
        ],
        [VMEM] * tp_count + [SMEM] + [VMEM] * (8 + len(pieces)),
        [],
        1 << 32,
        8,
        [*attended, core.reshape(1), flat_t, w_out, *pieces, tokens, post_gain.reshape(1, -1), ffn_gain.reshape(1, -1), dense_gate_vector.reshape(1, -1), routes, route_weights],
    )
    arrived = lax.all_to_all(outgoing, "ep", split_axis=0, concat_axis=0, tiled=True)
    units = call(
        functools.partial(units_body, ep_count),
        [((ep_count * own_rows, 1), f32)] * 2
        + [
            ((ep_count * own_rows, w_exp_gate.shape[2]), bf16),
            ((ep_count * own_rows, w_dense_gate.shape[0]), bf16),
        ],
        [VMEM] * 5,
        [],
        1<<27,
        8,
        [
            arrived.reshape(ep_count * own_rows, -1),
            w_exp_gate[0],
            w_exp_up[0],
            w_dense_gate,
            w_dense_up,
        ],
    )
    (partial,) = call(
        down_body,
        [((ep_count * own_rows, model_width), bf16)],
        [VMEM] * 6,
        [],
        1 << 31,
        6,
        [*units, w_exp_down[0], w_dense_down],
    )
    returned = lax.all_to_all(
        partial.reshape(ep_count, own_rows, model_width),
        "ep",
        split_axis=0,
        concat_axis=0,
        tiled=True,
    )
    (output,) = call(
        finish_body,
        [((own_rows, model_width), bf16)],
        [VMEM] * 3,
        [],
        1 << 30,
        2,
        [returned, residual, out_gain.reshape(1, -1)],
    )
    return (output, new_latent, new_rope_key)


def solution(mesh):
    placed = (
        P(("ep", "tp"), None),
        P(("ep", "tp")),
        P(("ep", "tp"), None, None),
        P(("ep", "tp"), None, None),
        P(),
        P(),
        P(),
        P(),
        P(),
        P(None, "tp"),
        P(),
        P(None, "tp"),
        P("tp", None, None),
        P("tp", None, None),
        P("tp", None),
        P(("ep", "tp"), None),
        P(("ep", "tp"), None),
        P("ep", None, None),
        P("ep", None, None),
        P("ep", None, None),
        P("ep", None),
        P("ep", None),
        P("ep", None),
        P(),
    )
    return jax.shard_map(
        shards,
        mesh=mesh,
        in_specs=placed,
        out_specs=(P(("ep", "tp"), None), P(("ep", "tp"), None), P(("ep", "tp"), None)),
        check_vma=False,
    )
```

time: 49.5 us -> 49.3 us (level)
  waiting for transfers between devices: 9.35 us -> 3.71 us
  local copies, waits for them, and re-layouts: 3.28 us -> 7.48 us
  starting transfers between devices: 4.7 us -> 5.28 us
    ppermute x4, waiting for transfers between devices: 9.35 us -> 3.71 us  [shift(): lax.ppermute(values, axis, [(i, (i + step) % count) for i in range(count)])]
    unnamed x48 -> x50, local copies, waits for them, and re-layouts: 2.44 us -> 5.62 us
    dynamic_slice x0 -> x2, local copies, waits for them, and re-layouts: none -> 1.76 us  [the longest x1 0.98 us: head_weights(): lax.dynamic_slice_in_dim(w_out, start, v_width)]
    reshape x1 -> x0, local copies, waits for them, and re-layouts: 0.75 us -> none  [shards(): lengths.reshape(-1, 1)]
    ppermute x4, starting transfers between devices: 4.7 us -> 5.27 us  [shift(): lax.ppermute(values, axis, [(i, (i + step) % count) for i in range(count)])]
    pallas_call x7 -> x8, Pallas kernels: 6.52 us -> 6.46 us  [call(): pl.pallas_call(body, out_shape=[jax.ShapeDtypeStruct(s, t) for s, t in sh...]
  transfers between devices with their start and end apart: 4 -> 6, of which waited for: 3 -> 1; matrix products, arithmetic and copies ran while one was open for 2% -> 4% of each run, Pallas kernels for 0% -> 8%
where the time goes in v3:
time: 49.3 us; the launch traced here: 48.8 us
  blocking collectives  24.9 us (51%)
  local copies, waits for them, and re-layouts  7.48 us (15%)
  Pallas kernels  6.46 us (13%)
  starting transfers between devices  5.28 us (11%)
  waiting for transfers between devices  3.71 us (8%)
  between operations  0.97 us (2%)
    all_to_all x1, blocking collectives, shards(): lax.all_to_all(outgoing, 'ep', split_axis=0, concat_axis=0, tiled=True)  14.4 us
    all_to_all x1, blocking collectives, shards(): lax.all_to_all(partial.reshape(ep_count, own_rows, model_width), 'ep', sp...  10.5 us
    pallas_call x8, Pallas kernels, call(): pl.pallas_call(body, out_shape=[jax.ShapeDtypeStruct(s, t) for s, t in sh...  6.46 us
    unnamed x50, local copies, waits for them, and re-layouts  5.62 us
    ppermute x4, starting transfers between devices, shift(): lax.ppermute(values, axis, [(i, (i + step) % count) for i in range(count)])  5.27 us
    ppermute x4, waiting for transfers between devices, shift(): lax.ppermute(values, axis, [(i, (i + step) % count) for i in range(count)])  3.71 us
  transfers between devices with their start and end apart: 6, of which 1 were waited for; matrix products, arithmetic and copies ran while one was open for 4% of the time, Pallas kernels for 8%

profile of v3, /device:TPU:0, one launch (start us, length us, event | category | flops | bytes accessed | tf_op | source)
XLA Modules:
  0.0 48.8 jit_solution(7706688492448131100)
XLA Ops:
  0.6 3.0 %collective-permute-start = (bf16[4,1024]{1,0:T(4,128)(2,1)}, bf16[4,1024]{1,0:T(4,128)(2,1)S(1)}, u32[]{:S(2)}, u32[]{:S(2)}) collective-permute-start(bf16[4,1024]{1,0:T(4,128)(2,1)} %refs_9_.3), channel_id=1, source_target_pairs={{0,1},{1,0},{2,3},{3,2},{4,5},{5,4},{6,7},{7,6},{8,9},{9,8},{10,11... | collective-permute-start | bytes 24584 | tf_op jit(solution)/shard_map/ppermute | solution.py:22
  3.7 0.8 %constant_dynamic-slice_fusion = (bf16[64,256]{1,0:T(8,128)(2,1)S(1)}, bf16[64,256]{1,0:T(8,128)(2,1)S(1)}) fusion(bf16[256,256]{1,0:T(8,128)(2,1)} %bitcast.17, s32[]{:T(128)S(6)} %select_n.17, s32[]{:T(128)S(6)} %select_n.16), kind=kLoop, calls=%fused_computation.2 | loop fusion | bytes 131080 | tf_op jit(solution)/shard_map/dynamic_slice | solution.py:323
  4.4 1.0 %constant_dynamic-slice_fusion.1 = (bf16[64,1024]{1,0:T(8,128)(2,1)S(1)}, bf16[64,1024]{1,0:T(8,128)(2,1)S(1)}) fusion(bf16[256,1024]{1,0:T(8,128)(2,1)} %refs_4_.1, s32[]{:T(128)S(6)} %select_n.17, s32[]{:T(128)S(6)} %select_n.16), kind=kLoop, calls=%fused_computation.3 | loop fusion | bytes 524296 | tf_op jit(solution)/shard_map/dynamic_slice | solution.py:322
  5.5 0.1 collective-permute-start.2
  5.6 1.1 %copy-done.10 = bf16[1024,384]{1,0:T(8,128)(2,1)S(1)} copy-done((bf16[1024,384]{1,0:T(8,128)(2,1)S(1)}, bf16[1024,384]{1,0:T(8,128)(2,1)}, u32[]{:S(2)}) %copy-start.10) | copy-done | bytes 786456
  6.7 0.9 %copy-done.13 = bf16[1024,128]{1,0:T(8,128)(2,1)S(1)} copy-done((bf16[1024,128]{1,0:T(8,128)(2,1)S(1)}, bf16[1024,128]{1,0:T(8,128)(2,1)}, u32[]{:S(2)}) %copy-start.13) | copy-done | bytes 262168
  7.7 0.9 %copy-done.14 = bf16[4,64,256]{2,1,0:T(8,128)(2,1)S(1)} copy-done((bf16[4,64,256]{2,1,0:T(8,128)(2,1)S(1)}, bf16[4,64,256]{2,1,0:T(8,128)(2,1)}, u32[]{:S(2)}) %copy-start.14) | copy-done | bytes 131096
  8.6 0.8 %copy-done.15 = bf16[1024,32]{0,1:T(8,128)(2,1)S(1)} copy-done((bf16[1024,32]{0,1:T(8,128)(2,1)S(1)}, bf16[1024,32]{0,1:T(8,128)(2,1)}, u32[]{:S(2)}) %copy-start.15) | copy-done | bytes 65560
  9.4 0.7 %copy-done.16 = bf16[4,1024]{1,0:T(4,128)(2,1)S(1)} copy-done((bf16[4,1024]{1,0:T(4,128)(2,1)S(1)}, bf16[4,1024]{1,0:T(4,128)(2,1)}, u32[]{:S(2)}) %copy-start.16) | copy-done | bytes 8216
  10.1 0.7 %copy-done.18 = f32[1024]{0:T(1024)S(1)} copy-done((f32[1024]{0:T(1024)S(1)}, f32[1024]{0:T(1024)}, u32[]{:S(2)}) %copy-start.18) | copy-done | bytes 4120
  10.8 0.5 %shard_map.247 = (bf16[4,1408]{1,0:T(4,128)(2,1)S(1)}, bf16[4,1408]{1,0:T(4,128)(2,1)S(1)}, f32[4,32]{1,0:T(4,128)S(1)}) custom-call(bf16[4,1024]{1,0:T(4,128)(2,1)S(1)} %copy-done.16, bf16[4,1024]{1,0:T(4,128)(2,1)S(1)} %collective-permute-done.refs_1_, f32[1,1024]{1,0:T(1,128)S(1)} %bitcast.22, bf16[1024,128]{1,0:T(8,128)(2,1)S(1)} %copy-done.13, ...), custom_call_target="tpu_custom_call" | custom-call | flops 4294967296 | bytes 1048576 | tf_op jit(solution)/shard_map/pallas_call | solution.py:263
  11.3 2.0 %collective-permute-start.3 = (bf16[64,1280]{1,0:T(8,128)(2,1)S(1)}, bf16[64,1280]{1,0:T(8,128)(2,1)S(1)}, u32[]{:S(2)}, u32[]{:S(2)}) collective-permute-start(bf16[64,1280]{1,0:T(8,128)(2,1)S(1)} %pad_maximum_fusion.1), channel_id=1, source_target_pairs={{0,1},{1,0},{2,3},{3,2},{4,5},{5,4},{6,7},{7,6},{8,9},{9,8},{10,11... | collective-permute-start | bytes 491528 | tf_op jit(solution)/shard_map/ppermute | solution.py:22
  13.4 0.1 collective-permute-start.1
  13.5 3.7 %collective-permute-done.3.refs_6_ = bf16[64,1280]{1,0:T(8,128)(2,1)S(1)} collective-permute-done((bf16[64,1280]{1,0:T(8,128)(2,1)S(1)}, bf16[64,1280]{1,0:T(8,128)(2,1)S(1)}, u32[]{:S(2)}, u32[]{:S(2)}) %collective-permute-start.3) | collective-permute-done | bytes 163872 | tf_op jit(solution)/shard_map/ppermute | solution.py:22
  17.2 0.0 copy-start.8
  17.2 1.2 %shard_map.249 = (f32[4,32]{1,0:T(4,128)S(1)}, f32[4,32]{1,0:T(4,128)S(1)}, bf16[4,32]{1,0:T(4,128)(2,1)}, bf16[4,32]{1,0:T(4,128)(2,1)S(1)}) custom-call(s32[4]{0:T(128)S(1)} %copy-done.9, f32[1,32]{1,0:T(1,128)S(1)} %shard_map.248.inverse, f32[4,32]{1,0:T(4,128)S(1)} %get-tuple-element.22.raw_key), custom_call_target="tpu_custom_call" | custom-call | flops 2147483648 | bytes 1048576 | tf_op jit(solution)/shard_map/pallas_call | solution.py:263
  18.4 0.0 copy-start.21
  18.4 0.0 copy-start.23
  18.5 0.3 copy-done
  18.8 2.0 %shard_map.250 = (bf16[4,256]{1,0:T(4,128)(2,1)}, bf16[4,1024]{1,0:T(4,128)(2,1)S(1)}, bf16[4,1024]{1,0:T(4,128)(2,1)S(1)}) custom-call(bf16[4,1408]{1,0:T(4,128)(2,1)S(1)} %get-tuple-element.20.refs_0_, bf16[4,1408]{1,0:T(4,128)(2,1)S(1)} %collective-permute-done.1.refs_1_, s32[1]{0:T(128)} %bitcast.2.refs_2_, s32[4]{0:T(128)S(1)} %copy-done.9, ...), custom_call_target="tpu_custom_call" | custom-call | flops 536870912 | bytes 1048576 | tf_op jit(solution)/shard_map/pallas_call | solution.py:263
  20.8 0.0 collective-permute-done.4.refs_7_
  20.9 0.0 copy-start.1
  20.9 0.0 copy-start.2
  20.9 1.1 %shard_map.251 = (bf16[4,1024]{1,0:T(4,128)(2,1)S(1)}, bf16[16,4,1152]{2,1,0:T(4,128)(2,1)S(1)}) custom-call(bf16[4,1024]{1,0:T(4,128)(2,1)S(1)} %get-tuple-element.26.refs_0_, bf16[4,1024]{1,0:T(4,128)(2,1)S(1)} %get-tuple-element.27.refs_1_, s32[1]{0:T(128)} %bitcast.4.refs_2_, bf16[256,256]{1,0:T(8,128)(2,1)S(1)} %bitcast.18, ...), custom_call_target="tpu_custom_call" | custom-call | flops 4294967296 | bytes 1048576 | tf_op jit(solution)/shard_map/pallas_call | solution.py:263
  22.0 0.0 copy-start.11
  22.1 0.0 copy-start.12
  22.1 14.4 %all_to_all.10 = bf16[16,4,1152]{2,1,0:T(4,128)(2,1)S(1)} all-to-all(bf16[16,4,1152]{2,1,0:T(4,128)(2,1)S(1)} %get-tuple-element.29), channel_id=1, replica_groups=mesh['ep'=16,'tp'=2] {'ep'}, dimensions={0} | all-to-all | bytes 294912 | tf_op jit(solution)/shard_map/all_to_all | solution.py:402
  36.5 0.6 %shard_map.252 = (f32[64,1]{1,0:T(8,128)S(1)}, f32[64,1]{1,0:T(8,128)S(1)}, bf16[64,256]{1,0:T(8,128)(2,1)S(1)}, bf16[64,256]{1,0:T(8,128)(2,1)S(1)}) custom-call(bf16[64,1152]{1,0:T(8,128)(2,1)S(1)} %reshape.47.arrived, bf16[1024,256]{1,0:T(8,128)(2,1)S(1)} %bitcast.15, bf16[1024,256]{1,0:T(8,128)(2,1)S(1)} %bitcast.16, bf16[256,1024]{1,0:T(8,128)(2,1)S(1)} %copy-done.3, ...), custom_call_target="tpu_custom_call" | custom-call | flops 134217728 | bytes 1048576 | tf_op jit(solution)/shard_map/pallas_call | solution.py:263
  37.2 0.3 shard_map.253
  37.5 0.1 reshape.48
  37.6 10.5 %all_to_all.11.returned = bf16[16,4,1024]{2,1,0:T(4,128)(2,1)S(1)} all-to-all(bf16[16,4,1024]{2,1,0:T(4,128)(2,1)S(1)} %reshape.48), channel_id=1, replica_groups=mesh['ep'=16,'tp'=2] {'ep'}, dimensions={0} | all-to-all | bytes 262144 | tf_op jit(solution)/shard_map/all_to_all | solution.py:431
  48.1 0.7 %shard_map.254 = bf16[4,1024]{1,0:T(4,128)(2,1)} custom-call(bf16[16,4,1024]{2,1,0:T(4,128)(2,1)S(1)} %all_to_all.11.returned, bf16[4,1024]{1,0:T(4,128)(2,1)S(1)} %get-tuple-element.34.residual, f32[1,1024]{1,0:T(1,128)S(1)} %bitcast.26), custom_call_target="tpu_custom_call" | custom-call | flops 1073741824 | bytes 1048576 | tf_op jit(solution)/shard_map/pallas_call | solution.py:263
  (46 shorter events, 0.2 us)
Async XLA Ops:
  0.6 4.9 %collective-permute-start = (bf16[4,1024]{1,0:T(4,128)(2,1)}, bf16[4,1024]{1,0:T(4,128)(2,1)S(1)}, u32[]{:S(2)}, u32[]{:S(2)}) collective-permute-start(bf16[4,1024]{1,0:T(4,128)(2,1)} %refs_9_.3), channel_id=1, source_target_pairs={{0,1},{1,0},{2,3},{3,2},{4,5},{5,4},{6,7},{7,6},{8,9},{9,8},{10,11... | collective-permute-start | bytes 24584 | tf_op jit(solution)/shard_map/ppermute | solution.py:22
  5.5 8.0 %collective-permute-start.2 = (bf16[64,1280]{1,0:T(8,128)(2,1)S(1)}, bf16[64,1280]{1,0:T(8,128)(2,1)S(1)}, u32[]{:S(2)}, u32[]{:S(2)}) collective-permute-start(bf16[64,1280]{1,0:T(8,128)(2,1)S(1)} %pad_maximum_fusion), channel_id=1, source_target_pairs={{0,1},{1,0},{2,3},{3,2},{4,5},{5,4},{6,7},{7,6},{8,9},{9,8},{10,11... | collective-permute-start | bytes 491528 | tf_op jit(solution)/shard_map/ppermute | solution.py:22
  5.6 1.1 %copy-start.10 = (bf16[1024,384]{1,0:T(8,128)(2,1)S(1)}, bf16[1024,384]{1,0:T(8,128)(2,1)}, u32[]{:S(2)}) copy-start(bf16[1024,384]{1,0:T(8,128)(2,1)} %refs_5_.1) | copy-start | bytes 2359300
  6.7 0.9 %copy-start.13 = (bf16[1024,128]{1,0:T(8,128)(2,1)S(1)}, bf16[1024,128]{1,0:T(8,128)(2,1)}, u32[]{:S(2)}) copy-start(bf16[1024,128]{1,0:T(8,128)(2,1)} %refs_3_.2) | copy-start | bytes 786436
  7.7 0.9 %copy-start.14 = (bf16[4,64,256]{2,1,0:T(8,128)(2,1)S(1)}, bf16[4,64,256]{2,1,0:T(8,128)(2,1)}, u32[]{:S(2)}) copy-start(bf16[4,64,256]{2,1,0:T(8,128)(2,1)} %refs_6_.1) | copy-start | bytes 393220
  8.6 0.8 %copy-start.15 = (bf16[1024,32]{0,1:T(8,128)(2,1)S(1)}, bf16[1024,32]{0,1:T(8,128)(2,1)}, u32[]{:S(2)}) copy-start(bf16[1024,32]{0,1:T(8,128)(2,1)} %param.34) | copy-start | bytes 196612
  9.4 0.7 %copy-start.16 = (bf16[4,1024]{1,0:T(4,128)(2,1)S(1)}, bf16[4,1024]{1,0:T(4,128)(2,1)}, u32[]{:S(2)}) copy-start(bf16[4,1024]{1,0:T(4,128)(2,1)} %refs_9_.3) | copy-start | bytes 24580
  10.1 0.7 %copy-start.18 = (f32[1024]{0:T(1024)S(1)}, f32[1024]{0:T(1024)}, u32[]{:S(2)}) copy-start(f32[1024]{0:T(1024)} %param.28) | copy-start | bytes 12292
  11.3 5.9 %copy-start.9 = (s32[4]{0:T(128)S(1)}, s32[4]{0:T(128)}, u32[]{:S(2)}) copy-start(s32[4]{0:T(128)} %refs_3_.3) | copy-start | bytes 52
  11.3 5.8 %collective-permute-start.3 = (bf16[64,1280]{1,0:T(8,128)(2,1)S(1)}, bf16[64,1280]{1,0:T(8,128)(2,1)S(1)}, u32[]{:S(2)}, u32[]{:S(2)}) collective-permute-start(bf16[64,1280]{1,0:T(8,128)(2,1)S(1)} %pad_maximum_fusion.1), channel_id=1, source_target_pairs={{0,1},{1,0},{2,3},{3,2},{4,5},{5,4},{6,7},{7,6},{8,9},{9,8},{10,11... | collective-permute-start | bytes 491528 | tf_op jit(solution)/shard_map/ppermute | solution.py:22
  13.4 5.1 %collective-permute-start.1 = (bf16[4,1408]{1,0:T(4,128)(2,1)S(1)}, bf16[4,1408]{1,0:T(4,128)(2,1)S(1)}, u32[]{:S(2)}, u32[]{:S(2)}) collective-permute-start(bf16[4,1408]{1,0:T(4,128)(2,1)S(1)} %get-tuple-element.21), channel_id=1, source_target_pairs={{0,1},{1,0},{2,3},{3,2},{4,5},{5,4},{6,7},{7,6},{8,9},{9,8},{10,11... | collective-permute-start | bytes 33800 | tf_op jit(solution)/shard_map/ppermute | solution.py:22
  13.5 7.3 %collective-permute-start.4 = (bf16[64,1280]{1,0:T(8,128)(2,1)S(1)}, bf16[64,1280]{1,0:T(8,128)(2,1)S(1)}, u32[]{:S(2)}, u32[]{:S(2)}) collective-permute-start(bf16[64,1280]{1,0:T(8,128)(2,1)S(1)} %collective-permute-done.2.refs_5_), channel_id=1, source_target_pairs={{0,2},{2,0},{4,6},{6,4},{8,10},{10,8},{12,14},{14,12},{16,18},{18,... | collective-permute-start | bytes 491528 | tf_op jit(solution)/shard_map/ppermute | solution.py:331
  17.2 3.6 %collective-permute-start.5 = (bf16[64,1280]{1,0:T(8,128)(2,1)S(1)}, bf16[64,1280]{1,0:T(8,128)(2,1)S(1)}, u32[]{:S(2)}, u32[]{:S(2)}) collective-permute-start(bf16[64,1280]{1,0:T(8,128)(2,1)S(1)} %collective-permute-done.3.refs_6_), channel_id=1, source_target_pairs={{0,2},{2,0},{4,6},{6,4},{8,10},{10,8},{12,14},{14,12},{16,18},{18,... | collective-permute-start | bytes 491528 | tf_op jit(solution)/shard_map/ppermute | solution.py:331
  17.2 1.6 %copy-start = (bf16[4,1024,256]{2,1,0:T(8,128)(2,1)S(1)}, bf16[4,1024,256]{2,1,0:T(8,128)(2,1)}, u32[]{:S(2)}) copy-start(bf16[4,1024,256]{2,1,0:T(8,128)(2,1)} %refs_8_.1) | copy-start | bytes 6291460
  17.2 1.6 %copy-start.5 = (bf16[4,32,1024]{2,1,0:T(8,128)(2,1)S(1)}, bf16[4,32,1024]{2,1,0:T(8,128)(2,1)}, u32[]{:S(2)}) copy-start(bf16[4,32,1024]{2,1,0:T(8,128)(2,1)} %refs_9_.2) | copy-start | bytes 786436
  17.2 1.6 %copy-start.8 = (f32[256]{0:T(256)S(1)}, f32[256]{0:T(256)}, u32[]{:S(2)}) copy-start(f32[256]{0:T(256)} %param.29) | copy-start | bytes 3076
  18.4 2.4 %copy-start.6 = (bf16[256,1024]{1,0:T(8,128)(2,1)S(1)}, bf16[256,1024]{1,0:T(8,128)(2,1)}, u32[]{:S(2)}) copy-start(bf16[256,1024]{1,0:T(8,128)(2,1)} %refs_4_.1) | copy-start | bytes 1572868
  18.4 2.4 %copy-start.7 = (bf16[4,256,64]{1,2,0:T(8,128)(2,1)S(1)}, bf16[4,256,64]{1,2,0:T(8,128)(2,1)}, u32[]{:S(2)}) copy-start(bf16[4,256,64]{1,2,0:T(8,128)(2,1)} %param.37) | copy-start | bytes 393220
  18.4 2.4 %copy-start.17 = (bf16[4,1024]{1,0:T(4,128)(2,1)S(1)}, bf16[4,1024]{1,0:T(4,128)(2,1)}, u32[]{:S(2)}) copy-start(bf16[4,1024]{1,0:T(4,128)(2,1)} %refs_9_.3) | copy-start | bytes 24580
  18.4 2.4 %copy-start.19 = (f32[1024]{0:T(1024)S(1)}, f32[1024]{0:T(1024)}, u32[]{:S(2)}) copy-start(f32[1024]{0:T(1024)} %param.30) | copy-start | bytes 12292
  18.4 2.4 %copy-start.20 = (f32[1024]{0:T(1024)S(1)}, f32[1024]{0:T(1024)}, u32[]{:S(2)}) copy-start(f32[1024]{0:T(1024)} %param.31) | copy-start | bytes 12292
  18.4 2.4 %copy-start.21 = (f32[1024]{0:T(1024)S(1)}, f32[1024]{0:T(1024)}, u32[]{:S(2)}) copy-start(f32[1024]{0:T(1024)} %param.47) | copy-start | bytes 12292
  18.4 2.4 %copy-start.23 = (s32[4,6]{1,0:T(4,128)S(1)}, s32[4,6]{1,0:T(4,128)}, u32[]{:S(2)}) copy-start(s32[4,6]{1,0:T(4,128)} %refs_13_.1) | copy-start | bytes 292
  18.4 2.4 %copy-start.24 = (f32[4,6]{1,0:T(4,128)S(1)}, f32[4,6]{1,0:T(4,128)}, u32[]{:S(2)}) copy-start(f32[4,6]{1,0:T(4,128)} %refs_14_.1) | copy-start | bytes 292
  20.9 15.6 %copy-start.1 = (bf16[1,1024,256]{2,1,0:T(8,128)(2,1)S(1)}, bf16[1,1024,256]{2,1,0:T(8,128)(2,1)}, u32[]{:S(2)}) copy-start(bf16[1,1024,256]{2,1,0:T(8,128)(2,1)} %param.41) | copy-start | bytes 1572868
  20.9 15.6 %copy-start.2 = (bf16[1,1024,256]{2,1,0:T(8,128)(2,1)S(1)}, bf16[1,1024,256]{2,1,0:T(8,128)(2,1)}, u32[]{:S(2)}) copy-start(bf16[1,1024,256]{2,1,0:T(8,128)(2,1)} %param.42) | copy-start | bytes 1572868
  20.9 15.6 %copy-start.3 = (bf16[256,1024]{1,0:T(8,128)(2,1)S(1)}, bf16[256,1024]{1,0:T(8,128)(2,1)}, u32[]{:S(2)}) copy-start(bf16[256,1024]{1,0:T(8,128)(2,1)} %gate_w.1) | copy-start | bytes 1572868
  20.9 15.6 %copy-start.4 = (bf16[256,1024]{1,0:T(8,128)(2,1)S(1)}, bf16[256,1024]{1,0:T(8,128)(2,1)}, u32[]{:S(2)}) copy-start(bf16[256,1024]{1,0:T(8,128)(2,1)} %up_w.1) | copy-start | bytes 1572868
  22.0 15.1 %copy-start.11 = (bf16[1,256,1024]{2,1,0:T(8,128)(2,1)S(1)}, bf16[1,256,1024]{2,1,0:T(8,128)(2,1)}, u32[]{:S(2)}) copy-start(bf16[1,256,1024]{2,1,0:T(8,128)(2,1)} %param.43) | copy-start | bytes 1572868
  22.1 15.1 %copy-start.12 = (bf16[256,1024]{1,0:T(8,128)(2,1)S(1)}, bf16[256,1024]{1,0:T(8,128)(2,1)}, u32[]{:S(2)}) copy-start(bf16[256,1024]{1,0:T(8,128)(2,1)} %down_w.1) | copy-start | bytes 1572868
  37.2 10.9 %copy-start.22 = (f32[1024]{0:T(1024)S(1)}, f32[1024]{0:T(1024)}, u32[]{:S(2)}) copy-start(f32[1024]{0:T(1024)} %param.32) | copy-start | bytes 12292

commit v4 on v3

--- a/solution.py
+++ b/solution.py
@@ -169,35 +169,61 @@
                 attended[s][b : b + 1, h * rank : (h + 1) * rank] = mixed[g : g + 1]
 
 
-def mix_body(blocks, heads, cores, *refs):
+def arrived_product(attended, pieces, numbers, heads, core, cores):
+    width = pieces[0].shape[1] - attended.shape[1] // heads
+    rank = attended.shape[1] // heads
+    per_core = heads // cores
+    product = jnp.zeros((attended.shape[0], width), f32)
+    for n, piece in zip(numbers, pieces):
+        picked = attended[:, n * rank : (n + 1) * rank]
+        if cores == 2:
+            other = (n + per_core) % heads
+            swapped = attended[:, other * rank : (other + 1) * rank]
+            picked = jnp.where(core == 0, picked.astype(f32), swapped.astype(f32)).astype(bf16)
+        one_head = mm_t(picked, piece[:, width:]).astype(bf16)
+        product = product + mm(one_head, piece[:, :width])
+    return product
+
+
+def own_body(blocks, heads, cores, numbers, *refs):
     attended = refs[:blocks]
     core_ref, value_t, w_out = refs[blocks : blocks + 3]
-    per_core = heads // cores
-    count = (blocks - 1) * heads
-    pieces = refs[blocks + 3 : blocks + 3 + count]
-    rest = refs[blocks + 3 + count :]
+    count = len(numbers)
+    pieces = refs[blocks + 3 : blocks + 3 + (blocks - 1) * count]
+    sums = refs[blocks + 3 + (blocks - 1) * count :]
+    rank = value_t.shape[1]
+    span = value_t.shape[0] // heads
+    outs = [
+        mm_t(
+            attended[0][:, h * rank : (h + 1) * rank],
+            value_t[h * span : (h + 1) * span],
+        )
+        for h in range(heads)
+    ]
+    product = mm(jnp.concatenate(outs, axis=-1).astype(bf16), w_out[...])
+    sums[0][...] = product.astype(bf16).astype(f32)
+    for s in range(1, blocks):
+        mine = pieces[(s - 1) * count : s * count]
+        sums[s][...] = arrived_product(attended[s], mine, numbers, heads, core_ref[0], cores)
+
+
+def mix_body(blocks, heads, cores, numbers, *refs):
+    sums = refs[:blocks]
+    attended = refs[blocks : 2 * blocks - 1]
+    core_ref = refs[2 * blocks - 1]
+    count = len(numbers)
+    pieces = refs[2 * blocks : 2 * blocks + (blocks - 1) * count]
+    rest = refs[2 * blocks + (blocks - 1) * count :]
     tokens, post_gain, ffn_gain, gate_vec, routes, route_weights, residual_out, outgoing = rest
     rows, width = tokens.shape
-    rank = value_t.shape[1]
-    span = value_t.shape[0] // heads
-    core = core_ref[0]
-
-    def columns(s, h):
-        return attended[s][:, h * rank : (h + 1) * rank]
-
-    outs = [mm_t(columns(0, h), value_t[h * span : (h + 1) * span]) for h in range(heads)]
-    product = mm(jnp.concatenate(outs, axis=-1).astype(bf16), w_out[...])
-    mixed = product.astype(bf16).astype(f32)
+    mixed = sums[0][...]
     for s in range(1, blocks):
-        group = pieces[(s - 1) * heads : s * heads]
-        product = jnp.zeros((rows, width), f32)
-        for n, piece in enumerate(group):
-            picked = columns(s, n)
-            if cores == 2:
-                swapped = columns(s, (n + per_core) % heads)
-                picked = jnp.where(core == 0, picked.astype(f32), swapped.astype(f32)).astype(bf16)
-            one_head = mm_t(picked, piece[:, width:]).astype(bf16)
-            product = product + mm(one_head, piece[:, :width])
+        product = sums[s][...]
+        if count:
+            late = pieces[(s - 1) * count : s * count]
+            product = product + arrived_product(
+                attended[s - 1], late, numbers, heads, core_ref[0], cores
+            )
         mixed = mixed + product.astype(bf16).astype(f32)
     residual = (tokens[...].astype(f32) + unit_rows(mixed) * post_gain[...]).astype(bf16)
     residual_out[...] = residual
@@ -371,9 +397,11 @@
     pieces = []
     for s in others:
         group = [fetched[s, k] for k in range(per_core)]
-        pieces += group
         if cores == 2:
-            pieces += [swap_cores(piece) for piece in group]
+            group += [swap_cores(piece) for piece in group]
+        pieces.append(group)
+    here = list(range(min(heads, per_core + 1)))
+    last = list(range(len(here), heads))
     me = lax.axis_index("tp").reshape(1)
     new_latent, *attended = call(
         functools.partial(attend_body, tp_count, heads, scale),
@@ -387,17 +415,38 @@
         8,
         [*packed, me, lengths, cosine, sine, rope_key, latent_gain.reshape(1, -1), cache_latent, cache_rope],
     )
+    core = core.reshape(1)
+    sums = call(
+        functools.partial(own_body, tp_count, heads, cores, tuple(here)),
+        [((own_rows, model_width), f32)] * tp_count,
+        [VMEM] * tp_count + [SMEM] + [VMEM] * (2 + (tp_count - 1) * len(here)),
+        [],
+        1 << 29,
+        8,
+        [*attended, core, flat_t, w_out, *[g[n] for g in pieces for n in here]],
+    )
     residual, outgoing = call(
-        functools.partial(mix_body, tp_count, heads, cores),
+        functools.partial(mix_body, tp_count, heads, cores, tuple(last)),
         [
             ((own_rows, model_width), bf16),
             ((ep_count, own_rows, model_width + extra_width), bf16),
         ],
-        [VMEM] * tp_count + [SMEM] + [VMEM] * (8 + len(pieces)),
+        [VMEM] * (2 * tp_count - 1) + [SMEM] + [VMEM] * (6 + (tp_count - 1) * len(last)),
         [],
         1 << 32,
         8,
-        [*attended, core.reshape(1), flat_t, w_out, *pieces, tokens, post_gain.reshape(1, -1), ffn_gain.reshape(1, -1), dense_gate_vector.reshape(1, -1), routes, route_weights],
+        [
+            *sums,
+            *attended[1:],
+            core,
+            *[g[n] for g in pieces for n in last],
+            tokens,
+            post_gain.reshape(1, -1),
+            ffn_gain.reshape(1, -1),
+            dense_gate_vector.reshape(1, -1),
+            routes,
+            route_weights,
+        ],
     )
     arrived = lax.all_to_all(outgoing, "ep", split_axis=0, concat_axis=0, tiled=True)
     units = call(

time: 49.3 us -> 49.5 us (level)
    pallas_call x8 -> x9, Pallas kernels: 6.46 us -> 6.5 us  [call(): pl.pallas_call(body, out_shape=[jax.ShapeDtypeStruct(s, t) for s, t in sh...]
  transfers between devices with their start and end apart: 6 -> 6, of which waited for: 1 -> 1; matrix products, arithmetic and copies ran while one was open for 4% -> 4% of each run, Pallas kernels for 8% -> 9%
where the time goes in v4:
time: 49.5 us; the launch traced here: 48.9 us
  blocking collectives  24.9 us (50%)
  local copies, waits for them, and re-layouts  7.62 us (15%)
  Pallas kernels  6.5 us (13%)
  starting transfers between devices  5.28 us (11%)
  waiting for transfers between devices  3.71 us (7%)
  between operations  0.95 us (2%)
    all_to_all x1, blocking collectives, shards(): lax.all_to_all(outgoing, 'ep', split_axis=0, concat_axis=0, tiled=True)  14.4 us
    all_to_all x1, blocking collectives, shards(): lax.all_to_all(partial.reshape(ep_count, own_rows, model_width), 'ep', sp...  10.5 us
    pallas_call x9, Pallas kernels, call(): pl.pallas_call(body, out_shape=[jax.ShapeDtypeStruct(s, t) for s, t in sh...  6.5 us
    unnamed x50, local copies, waits for them, and re-layouts  5.75 us
    ppermute x4, starting transfers between devices, shift(): lax.ppermute(values, axis, [(i, (i + step) % count) for i in range(count)])  5.27 us
    ppermute x4, waiting for transfers between devices, shift(): lax.ppermute(values, axis, [(i, (i + step) % count) for i in range(count)])  3.71 us
  transfers between devices with their start and end apart: 6, of which 1 were waited for; matrix products, arithmetic and copies ran while one was open for 4% of the time, Pallas kernels for 9%

profile of v4, /device:TPU:0, one launch (start us, length us, event | category | flops | bytes accessed | tf_op | source)
XLA Modules:
  0.0 48.9 jit_solution(9800071624911309208)
XLA Ops:
  0.6 3.0 %collective-permute-start = (bf16[4,1024]{1,0:T(4,128)(2,1)}, bf16[4,1024]{1,0:T(4,128)(2,1)S(1)}, u32[]{:S(2)}, u32[]{:S(2)}) collective-permute-start(bf16[4,1024]{1,0:T(4,128)(2,1)} %refs_5_.3), channel_id=1, source_target_pairs={{0,1},{1,0},{2,3},{3,2},{4,5},{5,4},{6,7},{7,6},{8,9},{9,8},{10,11... | collective-permute-start | bytes 24584 | tf_op jit(solution)/shard_map/ppermute | solution.py:22
  3.7 1.0 %constant_dynamic-slice_fusion.1 = (bf16[64,1024]{1,0:T(8,128)(2,1)S(1)}, bf16[64,1024]{1,0:T(8,128)(2,1)S(1)}) fusion(bf16[256,1024]{1,0:T(8,128)(2,1)} %refs_4_.1, s32[]{:T(128)S(6)} %select_n.17, s32[]{:T(128)S(6)} %select_n.16), kind=kLoop, calls=%fused_computation.3 | loop fusion | bytes 524296 | tf_op jit(solution)/shard_map/dynamic_slice | solution.py:348
  4.6 0.8 %constant_dynamic-slice_fusion = (bf16[64,256]{1,0:T(8,128)(2,1)S(1)}, bf16[64,256]{1,0:T(8,128)(2,1)S(1)}) fusion(bf16[256,256]{1,0:T(8,128)(2,1)} %bitcast.17, s32[]{:T(128)S(6)} %select_n.17, s32[]{:T(128)S(6)} %select_n.16), kind=kLoop, calls=%fused_computation.2 | loop fusion | bytes 131080 | tf_op jit(solution)/shard_map/dynamic_slice | solution.py:349
  5.5 0.1 collective-permute-start.2
  5.6 0.0 copy-start.10
  5.6 1.1 %copy-done.10 = bf16[1024,384]{1,0:T(8,128)(2,1)S(1)} copy-done((bf16[1024,384]{1,0:T(8,128)(2,1)S(1)}, bf16[1024,384]{1,0:T(8,128)(2,1)}, u32[]{:S(2)}) %copy-start.10) | copy-done | bytes 786456
  6.7 0.9 %copy-done.13 = bf16[1024,128]{1,0:T(8,128)(2,1)S(1)} copy-done((bf16[1024,128]{1,0:T(8,128)(2,1)S(1)}, bf16[1024,128]{1,0:T(8,128)(2,1)}, u32[]{:S(2)}) %copy-start.13) | copy-done | bytes 262168
  7.7 0.9 %copy-done.14 = bf16[4,64,256]{2,1,0:T(8,128)(2,1)S(1)} copy-done((bf16[4,64,256]{2,1,0:T(8,128)(2,1)S(1)}, bf16[4,64,256]{2,1,0:T(8,128)(2,1)}, u32[]{:S(2)}) %copy-start.14) | copy-done | bytes 131096
  8.6 0.8 %copy-done.15 = bf16[1024,32]{0,1:T(8,128)(2,1)S(1)} copy-done((bf16[1024,32]{0,1:T(8,128)(2,1)S(1)}, bf16[1024,32]{0,1:T(8,128)(2,1)}, u32[]{:S(2)}) %copy-start.15) | copy-done | bytes 65560
  9.4 0.7 %copy-done.16 = bf16[4,1024]{1,0:T(4,128)(2,1)S(1)} copy-done((bf16[4,1024]{1,0:T(4,128)(2,1)S(1)}, bf16[4,1024]{1,0:T(4,128)(2,1)}, u32[]{:S(2)}) %copy-start.16) | copy-done | bytes 8216
  10.1 0.7 %copy-done.18 = f32[1024]{0:T(1024)S(1)} copy-done((f32[1024]{0:T(1024)S(1)}, f32[1024]{0:T(1024)}, u32[]{:S(2)}) %copy-start.18) | copy-done | bytes 4120
  10.8 0.5 %shard_map.247 = (bf16[4,1408]{1,0:T(4,128)(2,1)S(1)}, bf16[4,1408]{1,0:T(4,128)(2,1)S(1)}, f32[4,32]{1,0:T(4,128)S(1)}) custom-call(bf16[4,1024]{1,0:T(4,128)(2,1)S(1)} %copy-done.16, bf16[4,1024]{1,0:T(4,128)(2,1)S(1)} %collective-permute-done.refs_1_, f32[1,1024]{1,0:T(1,128)S(1)} %bitcast.22, bf16[1024,128]{1,0:T(8,128)(2,1)S(1)} %copy-done.13, ...), custom_call_target="tpu_custom_call" | custom-call | flops 4294967296 | bytes 1048576 | tf_op jit(solution)/shard_map/pallas_call | solution.py:289
  11.3 2.0 %collective-permute-start.3 = (bf16[64,1280]{1,0:T(8,128)(2,1)S(1)}, bf16[64,1280]{1,0:T(8,128)(2,1)S(1)}, u32[]{:S(2)}, u32[]{:S(2)}) collective-permute-start(bf16[64,1280]{1,0:T(8,128)(2,1)S(1)} %pad_maximum_fusion.1), channel_id=1, source_target_pairs={{0,1},{1,0},{2,3},{3,2},{4,5},{5,4},{6,7},{7,6},{8,9},{9,8},{10,11... | collective-permute-start | bytes 491528 | tf_op jit(solution)/shard_map/ppermute | solution.py:22
  13.4 0.1 collective-permute-start.1
  13.5 3.7 %collective-permute-done.3.refs_6_ = bf16[64,1280]{1,0:T(8,128)(2,1)S(1)} collective-permute-done((bf16[64,1280]{1,0:T(8,128)(2,1)S(1)}, bf16[64,1280]{1,0:T(8,128)(2,1)S(1)}, u32[]{:S(2)}, u32[]{:S(2)}) %collective-permute-start.3) | collective-permute-done | bytes 163872 | tf_op jit(solution)/shard_map/ppermute | solution.py:22
  17.2 0.0 copy-start.5
  17.2 0.0 copy-start.8
  17.2 1.2 %shard_map.249 = (f32[4,32]{1,0:T(4,128)S(1)}, f32[4,32]{1,0:T(4,128)S(1)}, bf16[4,32]{1,0:T(4,128)(2,1)}, bf16[4,32]{1,0:T(4,128)(2,1)S(1)}) custom-call(s32[4]{0:T(128)S(1)} %copy-done.9, f32[1,32]{1,0:T(1,128)S(1)} %shard_map.248.inverse, f32[4,32]{1,0:T(4,128)S(1)} %get-tuple-element.24.raw_key), custom_call_target="tpu_custom_call" | custom-call | flops 2147483648 | bytes 1048576 | tf_op jit(solution)/shard_map/pallas_call | solution.py:289
  18.4 0.4 copy-done
  18.8 0.0 copy-start.21
  18.8 0.0 copy-start.23
  18.8 2.0 %shard_map.250 = (bf16[4,256]{1,0:T(4,128)(2,1)}, bf16[4,1024]{1,0:T(4,128)(2,1)S(1)}, bf16[4,1024]{1,0:T(4,128)(2,1)S(1)}) custom-call(bf16[4,1408]{1,0:T(4,128)(2,1)S(1)} %get-tuple-element.22.refs_0_, bf16[4,1408]{1,0:T(4,128)(2,1)S(1)} %collective-permute-done.1.refs_1_, s32[1]{0:T(128)} %bitcast.2.refs_2_, s32[4]{0:T(128)S(1)} %copy-done.9, ...), custom_call_target="tpu_custom_call" | custom-call | flops 536870912 | bytes 1048576 | tf_op jit(solution)/shard_map/pallas_call | solution.py:289
  20.8 0.0 collective-permute-done.4.refs_7_
  20.9 0.6 %shard_map.251 = (f32[4,1024]{1,0:T(4,128)S(1)}, f32[4,1024]{1,0:T(4,128)S(1)}) custom-call(bf16[4,1024]{1,0:T(4,128)(2,1)S(1)} %get-tuple-element.28.refs_0_, bf16[4,1024]{1,0:T(4,128)(2,1)S(1)} %get-tuple-element.29.refs_1_.refs_2_, s32[1]{0:T(128)} %bitcast.4.refs_2_.refs_3_, bf16[256,256]{1,0:T(8,128)(2,1)S(1)} %bitcast.18, ...), custom_call_target="tpu_custom_call" | custom-call | flops 536870912 | bytes 1048576 | tf_op jit(solution)/shard_map/pallas_call | solution.py:289
  21.5 0.1 copy-done.17
  21.6 0.6 %shard_map.252 = (bf16[4,1024]{1,0:T(4,128)(2,1)S(1)}, bf16[16,4,1152]{2,1,0:T(4,128)(2,1)S(1)}) custom-call(f32[4,1024]{1,0:T(4,128)S(1)} %get-tuple-element.31.refs_0_, f32[4,1024]{1,0:T(4,128)S(1)} %get-tuple-element.32.refs_1_, bf16[4,1024]{1,0:T(4,128)(2,1)S(1)} %get-tuple-element.29.refs_1_.refs_2_, s32[1]{0:T(128)} %bitcast.4.refs_2_.refs_3_, ...), custom_call_target="tpu_custom_call" | custom-call | flops 4294967296 | bytes 1048576 | tf_op jit(solution)/shard_map/pallas_call | solution.py:289
  22.2 14.4 %all_to_all.10 = bf16[16,4,1152]{2,1,0:T(4,128)(2,1)S(1)} all-to-all(bf16[16,4,1152]{2,1,0:T(4,128)(2,1)S(1)} %get-tuple-element.33), channel_id=1, replica_groups=mesh['ep'=16,'tp'=2] {'ep'}, dimensions={0} | all-to-all | bytes 294912 | tf_op jit(solution)/shard_map/all_to_all | solution.py:451
  36.7 0.6 %shard_map.253 = (f32[64,1]{1,0:T(8,128)S(1)}, f32[64,1]{1,0:T(8,128)S(1)}, bf16[64,256]{1,0:T(8,128)(2,1)S(1)}, bf16[64,256]{1,0:T(8,128)(2,1)S(1)}) custom-call(bf16[64,1152]{1,0:T(8,128)(2,1)S(1)} %reshape.47.arrived, bf16[1024,256]{1,0:T(8,128)(2,1)S(1)} %bitcast.15, bf16[1024,256]{1,0:T(8,128)(2,1)S(1)} %bitcast.16, bf16[256,1024]{1,0:T(8,128)(2,1)S(1)} %copy-done.3, ...), custom_call_target="tpu_custom_call" | custom-call | flops 134217728 | bytes 1048576 | tf_op jit(solution)/shard_map/pallas_call | solution.py:289
  37.4 0.3 shard_map.254
  37.7 0.1 reshape.48
  37.7 10.5 %all_to_all.11.returned = bf16[16,4,1024]{2,1,0:T(4,128)(2,1)S(1)} all-to-all(bf16[16,4,1024]{2,1,0:T(4,128)(2,1)S(1)} %reshape.48), channel_id=1, replica_groups=mesh['ep'=16,'tp'=2] {'ep'}, dimensions={0} | all-to-all | bytes 262144 | tf_op jit(solution)/shard_map/all_to_all | solution.py:480
  48.2 0.7 %shard_map.255 = bf16[4,1024]{1,0:T(4,128)(2,1)} custom-call(bf16[16,4,1024]{2,1,0:T(4,128)(2,1)S(1)} %all_to_all.11.returned, bf16[4,1024]{1,0:T(4,128)(2,1)S(1)} %get-tuple-element.38.residual, f32[1,1024]{1,0:T(1,128)S(1)} %bitcast.26), custom_call_target="tpu_custom_call" | custom-call | flops 1073741824 | bytes 1048576 | tf_op jit(solution)/shard_map/pallas_call | solution.py:289
  (47 shorter events, 0.2 us)
Async XLA Ops:
  0.6 5.0 %collective-permute-start = (bf16[4,1024]{1,0:T(4,128)(2,1)}, bf16[4,1024]{1,0:T(4,128)(2,1)S(1)}, u32[]{:S(2)}, u32[]{:S(2)}) collective-permute-start(bf16[4,1024]{1,0:T(4,128)(2,1)} %refs_5_.3), channel_id=1, source_target_pairs={{0,1},{1,0},{2,3},{3,2},{4,5},{5,4},{6,7},{7,6},{8,9},{9,8},{10,11... | collective-permute-start | bytes 24584 | tf_op jit(solution)/shard_map/ppermute | solution.py:22
  5.5 8.0 %collective-permute-start.2 = (bf16[64,1280]{1,0:T(8,128)(2,1)S(1)}, bf16[64,1280]{1,0:T(8,128)(2,1)S(1)}, u32[]{:S(2)}, u32[]{:S(2)}) collective-permute-start(bf16[64,1280]{1,0:T(8,128)(2,1)S(1)} %pad_maximum_fusion), channel_id=1, source_target_pairs={{0,1},{1,0},{2,3},{3,2},{4,5},{5,4},{6,7},{7,6},{8,9},{9,8},{10,11... | collective-permute-start | bytes 491528 | tf_op jit(solution)/shard_map/ppermute | solution.py:22
  5.6 1.1 %copy-start.10 = (bf16[1024,384]{1,0:T(8,128)(2,1)S(1)}, bf16[1024,384]{1,0:T(8,128)(2,1)}, u32[]{:S(2)}) copy-start(bf16[1024,384]{1,0:T(8,128)(2,1)} %refs_5_.2) | copy-start | bytes 2359300
  6.7 0.9 %copy-start.13 = (bf16[1024,128]{1,0:T(8,128)(2,1)S(1)}, bf16[1024,128]{1,0:T(8,128)(2,1)}, u32[]{:S(2)}) copy-start(bf16[1024,128]{1,0:T(8,128)(2,1)} %refs_3_.2) | copy-start | bytes 786436
  7.7 0.9 %copy-start.14 = (bf16[4,64,256]{2,1,0:T(8,128)(2,1)S(1)}, bf16[4,64,256]{2,1,0:T(8,128)(2,1)}, u32[]{:S(2)}) copy-start(bf16[4,64,256]{2,1,0:T(8,128)(2,1)} %refs_6_.1) | copy-start | bytes 393220
  8.6 0.8 %copy-start.15 = (bf16[1024,32]{0,1:T(8,128)(2,1)S(1)}, bf16[1024,32]{0,1:T(8,128)(2,1)}, u32[]{:S(2)}) copy-start(bf16[1024,32]{0,1:T(8,128)(2,1)} %param.34) | copy-start | bytes 196612
  9.4 0.7 %copy-start.16 = (bf16[4,1024]{1,0:T(4,128)(2,1)S(1)}, bf16[4,1024]{1,0:T(4,128)(2,1)}, u32[]{:S(2)}) copy-start(bf16[4,1024]{1,0:T(4,128)(2,1)} %refs_5_.3) | copy-start | bytes 24580
  10.1 0.7 %copy-start.18 = (f32[1024]{0:T(1024)S(1)}, f32[1024]{0:T(1024)}, u32[]{:S(2)}) copy-start(f32[1024]{0:T(1024)} %param.28) | copy-start | bytes 12292
  11.3 5.9 %copy-start.9 = (s32[4]{0:T(128)S(1)}, s32[4]{0:T(128)}, u32[]{:S(2)}) copy-start(s32[4]{0:T(128)} %refs_3_.3) | copy-start | bytes 52
  11.3 5.8 %collective-permute-start.3 = (bf16[64,1280]{1,0:T(8,128)(2,1)S(1)}, bf16[64,1280]{1,0:T(8,128)(2,1)S(1)}, u32[]{:S(2)}, u32[]{:S(2)}) collective-permute-start(bf16[64,1280]{1,0:T(8,128)(2,1)S(1)} %pad_maximum_fusion.1), channel_id=1, source_target_pairs={{0,1},{1,0},{2,3},{3,2},{4,5},{5,4},{6,7},{7,6},{8,9},{9,8},{10,11... | collective-permute-start | bytes 491528 | tf_op jit(solution)/shard_map/ppermute | solution.py:22
  13.4 5.0 %collective-permute-start.1 = (bf16[4,1408]{1,0:T(4,128)(2,1)S(1)}, bf16[4,1408]{1,0:T(4,128)(2,1)S(1)}, u32[]{:S(2)}, u32[]{:S(2)}) collective-permute-start(bf16[4,1408]{1,0:T(4,128)(2,1)S(1)} %get-tuple-element.23), channel_id=1, source_target_pairs={{0,1},{1,0},{2,3},{3,2},{4,5},{5,4},{6,7},{7,6},{8,9},{9,8},{10,11... | collective-permute-start | bytes 33800 | tf_op jit(solution)/shard_map/ppermute | solution.py:22
  13.5 7.4 %collective-permute-start.4 = (bf16[64,1280]{1,0:T(8,128)(2,1)S(1)}, bf16[64,1280]{1,0:T(8,128)(2,1)S(1)}, u32[]{:S(2)}, u32[]{:S(2)}) collective-permute-start(bf16[64,1280]{1,0:T(8,128)(2,1)S(1)} %collective-permute-done.2.refs_5_), channel_id=1, source_target_pairs={{0,2},{2,0},{4,6},{6,4},{8,10},{10,8},{12,14},{14,12},{16,18},{18,... | collective-permute-start | bytes 491528 | tf_op jit(solution)/shard_map/ppermute | solution.py:357
  17.2 4.3 %collective-permute-start.5 = (bf16[64,1280]{1,0:T(8,128)(2,1)S(1)}, bf16[64,1280]{1,0:T(8,128)(2,1)S(1)}, u32[]{:S(2)}, u32[]{:S(2)}) collective-permute-start(bf16[64,1280]{1,0:T(8,128)(2,1)S(1)} %collective-permute-done.3.refs_6_), channel_id=1, source_target_pairs={{0,2},{2,0},{4,6},{6,4},{8,10},{10,8},{12,14},{14,12},{16,18},{18,... | collective-permute-start | bytes 491528 | tf_op jit(solution)/shard_map/ppermute | solution.py:357
  17.2 1.6 %copy-start = (bf16[4,1024,256]{2,1,0:T(8,128)(2,1)S(1)}, bf16[4,1024,256]{2,1,0:T(8,128)(2,1)}, u32[]{:S(2)}) copy-start(bf16[4,1024,256]{2,1,0:T(8,128)(2,1)} %refs_8_.1) | copy-start | bytes 6291460
  17.2 1.6 %copy-start.5 = (bf16[4,32,1024]{2,1,0:T(8,128)(2,1)S(1)}, bf16[4,32,1024]{2,1,0:T(8,128)(2,1)}, u32[]{:S(2)}) copy-start(bf16[4,32,1024]{2,1,0:T(8,128)(2,1)} %refs_9_.2) | copy-start | bytes 786436
  17.2 1.6 %copy-start.8 = (f32[256]{0:T(256)S(1)}, f32[256]{0:T(256)}, u32[]{:S(2)}) copy-start(f32[256]{0:T(256)} %param.29) | copy-start | bytes 3076
  18.4 2.4 %copy-start.6 = (bf16[256,1024]{1,0:T(8,128)(2,1)S(1)}, bf16[256,1024]{1,0:T(8,128)(2,1)}, u32[]{:S(2)}) copy-start(bf16[256,1024]{1,0:T(8,128)(2,1)} %refs_4_.1) | copy-start | bytes 1572868
  18.4 2.5 %copy-start.7 = (bf16[4,256,64]{1,2,0:T(8,128)(2,1)S(1)}, bf16[4,256,64]{1,2,0:T(8,128)(2,1)}, u32[]{:S(2)}) copy-start(bf16[4,256,64]{1,2,0:T(8,128)(2,1)} %param.37) | copy-start | bytes 393220
  18.8 2.7 %copy-start.17 = (bf16[4,1024]{1,0:T(4,128)(2,1)S(1)}, bf16[4,1024]{1,0:T(4,128)(2,1)}, u32[]{:S(2)}) copy-start(bf16[4,1024]{1,0:T(4,128)(2,1)} %refs_5_.3) | copy-start | bytes 24580
  18.8 2.8 %copy-start.19 = (f32[1024]{0:T(1024)S(1)}, f32[1024]{0:T(1024)}, u32[]{:S(2)}) copy-start(f32[1024]{0:T(1024)} %param.30) | copy-start | bytes 12292
  18.8 2.8 %copy-start.20 = (f32[1024]{0:T(1024)S(1)}, f32[1024]{0:T(1024)}, u32[]{:S(2)}) copy-start(f32[1024]{0:T(1024)} %param.31) | copy-start | bytes 12292
  18.8 2.8 %copy-start.21 = (f32[1024]{0:T(1024)S(1)}, f32[1024]{0:T(1024)}, u32[]{:S(2)}) copy-start(f32[1024]{0:T(1024)} %param.47) | copy-start | bytes 12292
  18.8 2.7 %copy-start.23 = (s32[4,6]{1,0:T(4,128)S(1)}, s32[4,6]{1,0:T(4,128)}, u32[]{:S(2)}) copy-start(s32[4,6]{1,0:T(4,128)} %refs_9_.3) | copy-start | bytes 292
  18.8 2.7 %copy-start.24 = (f32[4,6]{1,0:T(4,128)S(1)}, f32[4,6]{1,0:T(4,128)}, u32[]{:S(2)}) copy-start(f32[4,6]{1,0:T(4,128)} %refs_10_.1) | copy-start | bytes 292
  21.6 15.1 %copy-start.1 = (bf16[1,1024,256]{2,1,0:T(8,128)(2,1)S(1)}, bf16[1,1024,256]{2,1,0:T(8,128)(2,1)}, u32[]{:S(2)}) copy-start(bf16[1,1024,256]{2,1,0:T(8,128)(2,1)} %param.41) | copy-start | bytes 1572868
  21.6 15.1 %copy-start.2 = (bf16[1,1024,256]{2,1,0:T(8,128)(2,1)S(1)}, bf16[1,1024,256]{2,1,0:T(8,128)(2,1)}, u32[]{:S(2)}) copy-start(bf16[1,1024,256]{2,1,0:T(8,128)(2,1)} %param.42) | copy-start | bytes 1572868
  21.6 15.1 %copy-start.3 = (bf16[256,1024]{1,0:T(8,128)(2,1)S(1)}, bf16[256,1024]{1,0:T(8,128)(2,1)}, u32[]{:S(2)}) copy-start(bf16[256,1024]{1,0:T(8,128)(2,1)} %gate_w.1) | copy-start | bytes 1572868
  21.6 15.1 %copy-start.4 = (bf16[256,1024]{1,0:T(8,128)(2,1)S(1)}, bf16[256,1024]{1,0:T(8,128)(2,1)}, u32[]{:S(2)}) copy-start(bf16[256,1024]{1,0:T(8,128)(2,1)} %up_w.1) | copy-start | bytes 1572868
  22.2 15.1 %copy-start.11 = (bf16[1,256,1024]{2,1,0:T(8,128)(2,1)S(1)}, bf16[1,256,1024]{2,1,0:T(8,128)(2,1)}, u32[]{:S(2)}) copy-start(bf16[1,256,1024]{2,1,0:T(8,128)(2,1)} %param.43) | copy-start | bytes 1572868
  22.2 15.1 %copy-start.12 = (bf16[256,1024]{1,0:T(8,128)(2,1)S(1)}, bf16[256,1024]{1,0:T(8,128)(2,1)}, u32[]{:S(2)}) copy-start(bf16[256,1024]{1,0:T(8,128)(2,1)} %down_w.1) | copy-start | bytes 1572868
  37.3 10.9 %copy-start.22 = (f32[1024]{0:T(1024)S(1)}, f32[1024]{0:T(1024)}, u32[]{:S(2)}) copy-start(f32[1024]{0:T(1024)} %param.32) | copy-start | bytes 12292

commit v5 on v4

--- a/solution.py
+++ b/solution.py
@@ -84,12 +84,13 @@
     out[...] = jnp.exp(place * (-math.log(rope_base) / half))
 
 
-def prepare_body(len_ref, inverse, raw_key, cosine, sine, key_out, key_own):
+def prepare_body(lengths, inverse, raw_key, cosine, sine, key_out, position_out):
     rows = raw_key.shape[0]
-    row = lax.broadcasted_iota(jnp.int32, (rows, 1), 0)
-    position = jnp.zeros((rows, 1), f32)
-    for b in range(rows):
-        position = jnp.where(row == b, len_ref[b].astype(f32), position)
+    shape = (rows, rows)
+    same = lax.broadcasted_iota(jnp.int32, shape, 0) == lax.broadcasted_iota(jnp.int32, shape, 1)
+    column = jnp.where(same, jnp.broadcast_to(lengths[...].astype(f32), shape), 0.0)
+    position = jnp.sum(column, axis=-1, keepdims=True)
+    position_out[...] = position
     angles = position * inverse[...]
     lane = lax.broadcasted_iota(jnp.int32, angles.shape, 1)
     cosines = jnp.cos(angles)
@@ -97,25 +98,23 @@
     cosine[...] = cosines
     sine[...] = sines
     key = raw_key[...]
-    key = (key * cosines + swap_halves(key) * sines).astype(bf16)
-    key_out[...] = key
-    key_own[...] = key
+    key_out[...] = (key * cosines + swap_halves(key) * sines).astype(bf16)
 
 
 def attend_body(blocks, heads, scale, *refs):
     packed = refs[:blocks]
     rest = refs[blocks:]
-    me_ref, len_ref, cosine, sine, rope_key, gain, cache_lat, cache_rot = rest[:8]
-    new_latent_out = rest[8]
-    attended = rest[9 : 9 + blocks]
-    latents, ropes = rest[9 + blocks :]
+    lengths, cosine, sine, rope_key, gain, cache_lat, cache_rot = rest[:7]
+    new_latent_out = rest[7]
+    attended = rest[8 : 8 + blocks]
+    latents, ropes = rest[8 + blocks :]
     rows = packed[0].shape[0]
     length, rank = cache_lat.shape[1:]
     rope = cache_rot.shape[1]
     part = rank // blocks
     cut = heads * rank
     rope_cut = cut + heads * rope
-    me = me_ref[0]
+    me = lax.axis_index("tp")
     pieces = []
     for s in range(blocks):
         values = packed[s][...].astype(f32)
@@ -136,7 +135,7 @@
     new_latent_out[...] = new_latent
     new_latent = new_latent.astype(f32)
     new_rope = rope_key[...].astype(f32)
-    position = lax.broadcasted_iota(jnp.int32, (blocks * heads, length), 1)
+    position = lax.broadcasted_iota(jnp.int32, (blocks * heads, length), 1).astype(f32)
     scores = []
     owns = []
     for b in range(rows):
@@ -146,7 +145,7 @@
         q_rot = q_rot * cosine[one, :] + swap_halves(q_rot) * sine[one, :]
         q_rot = q_rot.astype(bf16)
         score = mm_t(q_lat.astype(bf16), cache_lat[b]) + mm(q_rot, cache_rot[b])
-        scores.append(jnp.where(position < len_ref[b], score * scale, negative))
+        scores.append(jnp.where(position < lengths[b : b + 1, :], score * scale, negative))
         own = jnp.sum(q_lat * new_latent[one], axis=-1, keepdims=True)
         own = own + jnp.sum(q_rot.astype(f32) * new_rope[one], axis=-1, keepdims=True)
         owns.append(own * scale)
@@ -169,10 +168,11 @@
                 attended[s][b : b + 1, h * rank : (h + 1) * rank] = mixed[g : g + 1]
 
 
-def arrived_product(attended, pieces, numbers, heads, core, cores):
+def arrived_product(attended, pieces, numbers, heads, cores):
     width = pieces[0].shape[1] - attended.shape[1] // heads
     rank = attended.shape[1] // heads
     per_core = heads // cores
+    core = lax.axis_index("ep") % cores
     product = jnp.zeros((attended.shape[0], width), f32)
     for n, piece in zip(numbers, pieces):
         picked = attended[:, n * rank : (n + 1) * rank]
@@ -187,10 +187,10 @@
 
 def own_body(blocks, heads, cores, numbers, *refs):
     attended = refs[:blocks]
-    core_ref, value_t, w_out = refs[blocks : blocks + 3]
+    value_t, w_out = refs[blocks : blocks + 2]
     count = len(numbers)
-    pieces = refs[blocks + 3 : blocks + 3 + (blocks - 1) * count]
-    sums = refs[blocks + 3 + (blocks - 1) * count :]
+    pieces = refs[blocks + 2 : blocks + 2 + (blocks - 1) * count]
+    sums = refs[blocks + 2 + (blocks - 1) * count :]
     rank = value_t.shape[1]
     span = value_t.shape[0] // heads
     outs = [
@@ -204,16 +204,15 @@
     sums[0][...] = product.astype(bf16).astype(f32)
     for s in range(1, blocks):
         mine = pieces[(s - 1) * count : s * count]
-        sums[s][...] = arrived_product(attended[s], mine, numbers, heads, core_ref[0], cores)
+        sums[s][...] = arrived_product(attended[s], mine, numbers, heads, cores)
 
 
 def mix_body(blocks, heads, cores, numbers, *refs):
     sums = refs[:blocks]
     attended = refs[blocks : 2 * blocks - 1]
-    core_ref = refs[2 * blocks - 1]
     count = len(numbers)
-    pieces = refs[2 * blocks : 2 * blocks + (blocks - 1) * count]
-    rest = refs[2 * blocks + (blocks - 1) * count :]
+    pieces = refs[2 * blocks - 1 : 2 * blocks - 1 + (blocks - 1) * count]
+    rest = refs[2 * blocks - 1 + (blocks - 1) * count :]
     tokens, post_gain, ffn_gain, gate_vec, routes, route_weights, residual_out, outgoing = rest
     rows, width = tokens.shape
     mixed = sums[0][...]
@@ -222,7 +221,7 @@
         if count:
             late = pieces[(s - 1) * count : s * count]
             product = product + arrived_product(
-                attended[s - 1], late, numbers, heads, core_ref[0], cores
+                attended[s - 1], late, numbers, heads, cores
             )
         mixed = mixed + product.astype(bf16).astype(f32)
     residual = (tokens[...].astype(f32) + unit_rows(mixed) * post_gain[...]).astype(bf16)
@@ -273,7 +272,9 @@
     out[...] = (row_weight[...] * routed.astype(f32) + row_gate[...] * dense).astype(bf16)
 
 
-def finish_body(returned, residual, gain, out):
+def finish_body(returned, residual, gain, latent, key, out, latent_out, key_out):
+    latent_out[...] = latent[...]
+    key_out[...] = key[...]
     combined = returned[0].astype(f32)
     for e in range(1, returned.shape[0]):
         combined = combined + returned[e].astype(f32)
@@ -281,8 +282,6 @@
 
 
 VMEM = pl.BlockSpec(memory_space=pltpu.VMEM)
-HBM = pl.BlockSpec(memory_space=pltpu.HBM)
-SMEM = pl.BlockSpec(memory_space=pltpu.SMEM)
 
 
 def call(body, shapes, specs, scratch, flops, limit, args):
@@ -379,14 +378,15 @@
             w_absorb_key,
         ],
     )
-    cosine, sine, new_rope_key, rope_key = call(
+    cosine, sine, rope_key, position = call(
         prepare_body,
-        [((own_rows, rope_width), f32)] * 2 + [((own_rows, rope_width), bf16)] * 2,
-        [SMEM] + [VMEM] * 2,
+        [((own_rows, rope_width), f32)] * 2
+        + [((own_rows, rope_width), bf16), ((own_rows, 1), f32)],
+        [VMEM] * 3,
         [],
         1 << 31,
         2,
-        [lengths, inverse, raw_key],
+        [lengths.reshape(1, -1), inverse, raw_key],
     )
     mine = packed[0]
     packed = [mine] + [shift(packed[s], -s, "tp") for s in others]
@@ -400,30 +400,28 @@
         if cores == 2:
             group += [swap_cores(piece) for piece in group]
         pieces.append(group)
-    here = list(range(min(heads, per_core + 1)))
-    last = list(range(len(here), heads))
-    me = lax.axis_index("tp").reshape(1)
+    here = [0] if cores == 1 else [0, per_core]
+    last = [n for n in range(heads) if n not in here]
     new_latent, *attended = call(
         functools.partial(attend_body, tp_count, heads, scale),
         [((own_rows, rank), bf16)] + [((own_rows, heads * rank), bf16)] * tp_count,
-        [VMEM] * tp_count + [SMEM, SMEM] + [VMEM] * 6,
+        [VMEM] * (tp_count + 7),
         [
             pltpu.VMEM((own_rows, tp_count * heads, rank), f32),
             pltpu.VMEM((own_rows, tp_count * heads, rope_width), f32),
         ],
         1 << 29,
         8,
-        [*packed, me, lengths, cosine, sine, rope_key, latent_gain.reshape(1, -1), cache_latent, cache_rope],
-    )
-    core = core.reshape(1)
+        [*packed, position, cosine, sine, rope_key, latent_gain.reshape(1, -1), cache_latent, cache_rope],
+    )
     sums = call(
         functools.partial(own_body, tp_count, heads, cores, tuple(here)),
         [((own_rows, model_width), f32)] * tp_count,
-        [VMEM] * tp_count + [SMEM] + [VMEM] * (2 + (tp_count - 1) * len(here)),
+        [VMEM] * (tp_count + 2 + (tp_count - 1) * len(here)),
         [],
         1 << 29,
         8,
-        [*attended, core, flat_t, w_out, *[g[n] for g in pieces for n in here]],
+        [*attended, flat_t, w_out, *[g[n] for g in pieces for n in here]],
     )
     residual, outgoing = call(
         functools.partial(mix_body, tp_count, heads, cores, tuple(last)),
@@ -431,14 +429,13 @@
             ((own_rows, model_width), bf16),
             ((ep_count, own_rows, model_width + extra_width), bf16),
         ],
-        [VMEM] * (2 * tp_count - 1) + [SMEM] + [VMEM] * (6 + (tp_count - 1) * len(last)),
+        [VMEM] * (2 * tp_count + 5 + (tp_count - 1) * len(last)),
         [],
         1 << 32,
         8,
         [
             *sums,
             *attended[1:],
-            core,
             *[g[n] for g in pieces for n in last],
             tokens,
             post_gain.reshape(1, -1),
@@ -484,14 +481,18 @@
         concat_axis=0,
         tiled=True,
     )
-    (output,) = call(
+    output, new_latent, new_rope_key = call(
         finish_body,
-        [((own_rows, model_width), bf16)],
-        [VMEM] * 3,
+        [
+            ((own_rows, model_width), bf16),
+            ((own_rows, rank), bf16),
+            ((own_rows, rope_width), bf16),
+        ],
+        [VMEM] * 5,
         [],
         1 << 30,
         2,
-        [returned, residual, out_gain.reshape(1, -1)],
+        [returned, residual, out_gain.reshape(1, -1), new_latent, rope_key],
     )
     return (output, new_latent, new_rope_key)
 

time: 49.5 us -> 48.8 us (0.986)
  Pallas kernels: 6.5 us -> 4.86 us
  local copies, waits for them, and re-layouts: 7.62 us -> 8.59 us
    pallas_call x9, Pallas kernels: 6.5 us -> 4.86 us  [call(): pl.pallas_call(body, out_shape=[jax.ShapeDtypeStruct(s, t) for s, t in sh...]
    unnamed x50, local copies, waits for them, and re-layouts: 5.75 us -> 6.73 us
  transfers between devices with their start and end apart: 6 -> 6, of which waited for: 1 -> 1; matrix products, arithmetic and copies ran while one was open for 4% -> 4% of each run, Pallas kernels for 9% -> 5%
where the time goes in v5:
time: 48.8 us; the launch traced here: 48.3 us
  blocking collectives  24.9 us (51%)
  local copies, waits for them, and re-layouts  8.59 us (18%)
  starting transfers between devices  5.28 us (11%)
  Pallas kernels  4.86 us (10%)
  waiting for transfers between devices  3.71 us (8%)
  between operations  0.98 us (2%)
    all_to_all x1, blocking collectives, shards(): lax.all_to_all(outgoing, 'ep', split_axis=0, concat_axis=0, tiled=True)  14.4 us
    all_to_all x1, blocking collectives, shards(): lax.all_to_all(partial.reshape(ep_count, own_rows, model_width), 'ep', sp...  10.5 us
    unnamed x50, local copies, waits for them, and re-layouts  6.73 us
    ppermute x4, starting transfers between devices, shift(): lax.ppermute(values, axis, [(i, (i + step) % count) for i in range(count)])  5.27 us
    pallas_call x9, Pallas kernels, call(): pl.pallas_call(body, out_shape=[jax.ShapeDtypeStruct(s, t) for s, t in sh...  4.86 us
    ppermute x4, waiting for transfers between devices, shift(): lax.ppermute(values, axis, [(i, (i + step) % count) for i in range(count)])  3.7 us
    dynamic_slice x1, local copies, waits for them, and re-layouts, head_weights(): lax.dynamic_slice_in_dim(w_out, start, v_width)  0.98 us
  transfers between devices with their start and end apart: 6, of which 1 were waited for; matrix products, arithmetic and copies ran while one was open for 4% of the time, Pallas kernels for 5%

profile of v5, /device:TPU:0, one launch (start us, length us, event | category | flops | bytes accessed | tf_op | source)
XLA Modules:
  0.0 48.3 jit_solution(10948903038479590570)
XLA Ops:
  0.6 3.0 %collective-permute-start = (bf16[4,1024]{1,0:T(4,128)(2,1)}, bf16[4,1024]{1,0:T(4,128)(2,1)S(1)}, u32[]{:S(2)}, u32[]{:S(2)}) collective-permute-start(bf16[4,1024]{1,0:T(4,128)(2,1)} %refs_5_.3), channel_id=1, source_target_pairs={{0,1},{1,0},{2,3},{3,2},{4,5},{5,4},{6,7},{7,6},{8,9},{9,8},{10,11... | collective-permute-start | bytes 24584 | tf_op jit(solution)/shard_map/ppermute | solution.py:22
  3.7 0.8 %constant_dynamic-slice_fusion = (bf16[64,256]{1,0:T(8,128)(2,1)S(1)}, bf16[64,256]{1,0:T(8,128)(2,1)S(1)}) fusion(bf16[256,256]{1,0:T(8,128)(2,1)} %bitcast.16, s32[]{:T(128)S(6)} %select_n.17, s32[]{:T(128)S(6)} %select_n.16), kind=kLoop, calls=%fused_computation.2 | loop fusion | bytes 131080 | tf_op jit(solution)/shard_map/dynamic_slice | solution.py:348
  4.4 1.0 %constant_dynamic-slice_fusion.1 = (bf16[64,1024]{1,0:T(8,128)(2,1)S(1)}, bf16[64,1024]{1,0:T(8,128)(2,1)S(1)}) fusion(bf16[256,1024]{1,0:T(8,128)(2,1)} %refs_3_.3, s32[]{:T(128)S(6)} %select_n.17, s32[]{:T(128)S(6)} %select_n.16), kind=kLoop, calls=%fused_computation.3 | loop fusion | bytes 524296 | tf_op jit(solution)/shard_map/dynamic_slice | solution.py:347
  5.5 0.1 collective-permute-start.2
  5.6 0.0 copy-start.9
  5.6 1.1 %copy-done.9 = bf16[1024,384]{1,0:T(8,128)(2,1)S(1)} copy-done((bf16[1024,384]{1,0:T(8,128)(2,1)S(1)}, bf16[1024,384]{1,0:T(8,128)(2,1)}, u32[]{:S(2)}) %copy-start.9) | copy-done | bytes 786456
  6.7 0.9 %copy-done.12 = bf16[1024,128]{1,0:T(8,128)(2,1)S(1)} copy-done((bf16[1024,128]{1,0:T(8,128)(2,1)S(1)}, bf16[1024,128]{1,0:T(8,128)(2,1)}, u32[]{:S(2)}) %copy-start.12) | copy-done | bytes 262168
  7.7 0.9 %copy-done.13 = bf16[4,64,256]{2,1,0:T(8,128)(2,1)S(1)} copy-done((bf16[4,64,256]{2,1,0:T(8,128)(2,1)S(1)}, bf16[4,64,256]{2,1,0:T(8,128)(2,1)}, u32[]{:S(2)}) %copy-start.13) | copy-done | bytes 131096
  8.6 0.8 %copy-done.14 = bf16[1024,32]{0,1:T(8,128)(2,1)S(1)} copy-done((bf16[1024,32]{0,1:T(8,128)(2,1)S(1)}, bf16[1024,32]{0,1:T(8,128)(2,1)}, u32[]{:S(2)}) %copy-start.14) | copy-done | bytes 65560
  9.4 0.7 %copy-done.15 = bf16[4,1024]{1,0:T(4,128)(2,1)S(1)} copy-done((bf16[4,1024]{1,0:T(4,128)(2,1)S(1)}, bf16[4,1024]{1,0:T(4,128)(2,1)}, u32[]{:S(2)}) %copy-start.15) | copy-done | bytes 8216
  10.1 0.7 %copy-done.17 = f32[1024]{0:T(1024)S(1)} copy-done((f32[1024]{0:T(1024)S(1)}, f32[1024]{0:T(1024)}, u32[]{:S(2)}) %copy-start.17) | copy-done | bytes 4120
  10.8 0.5 %shard_map.247 = (bf16[4,1408]{1,0:T(4,128)(2,1)S(1)}, bf16[4,1408]{1,0:T(4,128)(2,1)S(1)}, f32[4,32]{1,0:T(4,128)S(1)}) custom-call(bf16[4,1024]{1,0:T(4,128)(2,1)S(1)} %copy-done.15, bf16[4,1024]{1,0:T(4,128)(2,1)S(1)} %collective-permute-done.refs_1_, f32[1,1024]{1,0:T(1,128)S(1)} %bitcast.21, bf16[1024,128]{1,0:T(8,128)(2,1)S(1)} %copy-done.12, ...), custom_call_target="tpu_custom_call" | custom-call | flops 4294967296 | bytes 1048576 | tf_op jit(solution)/shard_map/pallas_call | solution.py:288
  11.3 2.0 %collective-permute-start.4 = (bf16[64,1280]{1,0:T(8,128)(2,1)S(1)}, bf16[64,1280]{1,0:T(8,128)(2,1)S(1)}, u32[]{:S(2)}, u32[]{:S(2)}) collective-permute-start(bf16[64,1280]{1,0:T(8,128)(2,1)S(1)} %pad_maximum_fusion.1), channel_id=1, source_target_pairs={{0,1},{1,0},{2,3},{3,2},{4,5},{5,4},{6,7},{7,6},{8,9},{9,8},{10,11... | collective-permute-start | bytes 491528 | tf_op jit(solution)/shard_map/ppermute | solution.py:22
  13.4 0.1 collective-permute-start.1
  13.5 3.7 %collective-permute-done.4.refs_3_ = bf16[64,1280]{1,0:T(8,128)(2,1)S(1)} collective-permute-done((bf16[64,1280]{1,0:T(8,128)(2,1)S(1)}, bf16[64,1280]{1,0:T(8,128)(2,1)S(1)}, u32[]{:S(2)}, u32[]{:S(2)}) %collective-permute-start.4) | collective-permute-done | bytes 163872 | tf_op jit(solution)/shard_map/ppermute | solution.py:22
  17.2 0.0 copy-start.8
  17.2 0.1 shard_map.249
  17.3 0.0 copy-start.6
  17.3 0.0 copy-start.7
  17.4 1.4 %copy-done = bf16[4,1024,256]{2,1,0:T(8,128)(2,1)S(1)} copy-done((bf16[4,1024,256]{2,1,0:T(8,128)(2,1)S(1)}, bf16[4,1024,256]{2,1,0:T(8,128)(2,1)}, u32[]{:S(2)}) %copy-start) | copy-done | bytes 2097176
  18.8 0.0 copy-start.22
  18.8 1.5 %shard_map.250 = (bf16[4,256]{1,0:T(4,128)(2,1)S(1)}, bf16[4,1024]{1,0:T(4,128)(2,1)S(1)}, bf16[4,1024]{1,0:T(4,128)(2,1)S(1)}) custom-call(bf16[4,1408]{1,0:T(4,128)(2,1)S(1)} %get-tuple-element.22.refs_0_, bf16[4,1408]{1,0:T(4,128)(2,1)S(1)} %collective-permute-done.1.refs_1_, f32[4,1]{1,0:T(4,128)S(1)} %get-tuple-element.25.refs_2_, ...), custom_call_target="tpu_custom_call" | custom-call | flops 536870912 | bytes 1048576 | tf_op jit(solution)/shard_map/pallas_call | solution.py:288
  20.3 0.0 collective-permute-done.3.refs_5_
  20.3 0.5 %shard_map.251 = (f32[4,1024]{1,0:T(4,128)S(1)}, f32[4,1024]{1,0:T(4,128)S(1)}) custom-call(bf16[4,1024]{1,0:T(4,128)(2,1)S(1)} %get-tuple-element.29.refs_0_, bf16[4,1024]{1,0:T(4,128)(2,1)S(1)} %get-tuple-element.30.refs_1_.refs_2_, bf16[256,256]{1,0:T(8,128)(2,1)S(1)} %bitcast.17, bf16[256,1024]{1,0:T(8,128)(2,1)S(1)} %copy-done.6, ...), custom_call_target="tpu_custom_call" | custom-call | flops 536870912 | bytes 1048576 | tf_op jit(solution)/shard_map/pallas_call | solution.py:288
  20.8 0.0 copy-done.16
  21.0 0.6 %shard_map.252 = (bf16[4,1024]{1,0:T(4,128)(2,1)S(1)}, bf16[16,4,1152]{2,1,0:T(4,128)(2,1)S(1)}) custom-call(f32[4,1024]{1,0:T(4,128)S(1)} %get-tuple-element.31.refs_0_, f32[4,1024]{1,0:T(4,128)S(1)} %get-tuple-element.32.refs_1_, bf16[4,1024]{1,0:T(4,128)(2,1)S(1)} %get-tuple-element.30.refs_1_.refs_2_, ...), custom_call_target="tpu_custom_call" | custom-call | flops 4294967296 | bytes 1048576 | tf_op jit(solution)/shard_map/pallas_call | solution.py:288
  21.6 14.4 %all_to_all.10 = bf16[16,4,1152]{2,1,0:T(4,128)(2,1)S(1)} all-to-all(bf16[16,4,1152]{2,1,0:T(4,128)(2,1)S(1)} %get-tuple-element.34), channel_id=1, replica_groups=mesh['ep'=16,'tp'=2] {'ep'}, dimensions={0} | all-to-all | bytes 294912 | tf_op jit(solution)/shard_map/all_to_all | solution.py:448
  36.0 0.6 %shard_map.253 = (f32[64,1]{1,0:T(8,128)S(1)}, f32[64,1]{1,0:T(8,128)S(1)}, bf16[64,256]{1,0:T(8,128)(2,1)S(1)}, bf16[64,256]{1,0:T(8,128)(2,1)S(1)}) custom-call(bf16[64,1152]{1,0:T(8,128)(2,1)S(1)} %reshape.43.arrived, bf16[1024,256]{1,0:T(8,128)(2,1)S(1)} %bitcast.14, bf16[1024,256]{1,0:T(8,128)(2,1)S(1)} %bitcast.15, bf16[256,1024]{1,0:T(8,128)(2,1)S(1)} %copy-done.3, ...), custom_call_target="tpu_custom_call" | custom-call | flops 134217728 | bytes 1048576 | tf_op jit(solution)/shard_map/pallas_call | solution.py:288
  36.7 0.3 shard_map.254
  37.0 0.1 reshape.44
  37.1 10.5 %all_to_all.11.returned = bf16[16,4,1024]{2,1,0:T(4,128)(2,1)S(1)} all-to-all(bf16[16,4,1024]{2,1,0:T(4,128)(2,1)S(1)} %reshape.44), channel_id=1, replica_groups=mesh['ep'=16,'tp'=2] {'ep'}, dimensions={0} | all-to-all | bytes 262144 | tf_op jit(solution)/shard_map/all_to_all | solution.py:477
  47.6 0.7 %shard_map.255 = (bf16[4,1024]{1,0:T(4,128)(2,1)}, bf16[4,256]{1,0:T(4,128)(2,1)}, bf16[4,32]{1,0:T(4,128)(2,1)}) custom-call(bf16[16,4,1024]{2,1,0:T(4,128)(2,1)S(1)} %all_to_all.11.returned, bf16[4,1024]{1,0:T(4,128)(2,1)S(1)} %get-tuple-element.39.residual, f32[1,1024]{1,0:T(1,128)S(1)} %bitcast.25, bf16[4,256]{1,0:T(4,128)(2,1)S(1)} %get-tuple-element.40.latent, ...), custom_call_target="tpu_custom_call" | custom-call | flops 1073741824 | bytes 1048576 | tf_op jit(solution)/shard_map/pallas_call | solution.py:288
  (47 shorter events, 0.2 us)
Async XLA Ops:
  0.6 4.9 %collective-permute-start = (bf16[4,1024]{1,0:T(4,128)(2,1)}, bf16[4,1024]{1,0:T(4,128)(2,1)S(1)}, u32[]{:S(2)}, u32[]{:S(2)}) collective-permute-start(bf16[4,1024]{1,0:T(4,128)(2,1)} %refs_5_.3), channel_id=1, source_target_pairs={{0,1},{1,0},{2,3},{3,2},{4,5},{5,4},{6,7},{7,6},{8,9},{9,8},{10,11... | collective-permute-start | bytes 24584 | tf_op jit(solution)/shard_map/ppermute | solution.py:22
  5.5 8.0 %collective-permute-start.2 = (bf16[64,1280]{1,0:T(8,128)(2,1)S(1)}, bf16[64,1280]{1,0:T(8,128)(2,1)S(1)}, u32[]{:S(2)}, u32[]{:S(2)}) collective-permute-start(bf16[64,1280]{1,0:T(8,128)(2,1)S(1)} %pad_maximum_fusion), channel_id=1, source_target_pairs={{0,1},{1,0},{2,3},{3,2},{4,5},{5,4},{6,7},{7,6},{8,9},{9,8},{10,11... | collective-permute-start | bytes 491528 | tf_op jit(solution)/shard_map/ppermute | solution.py:22
  5.6 1.1 %copy-start.9 = (bf16[1024,384]{1,0:T(8,128)(2,1)S(1)}, bf16[1024,384]{1,0:T(8,128)(2,1)}, u32[]{:S(2)}) copy-start(bf16[1024,384]{1,0:T(8,128)(2,1)} %refs_5_.2) | copy-start | bytes 2359300
  6.7 0.9 %copy-start.12 = (bf16[1024,128]{1,0:T(8,128)(2,1)S(1)}, bf16[1024,128]{1,0:T(8,128)(2,1)}, u32[]{:S(2)}) copy-start(bf16[1024,128]{1,0:T(8,128)(2,1)} %refs_3_.2) | copy-start | bytes 786436
  7.7 0.9 %copy-start.13 = (bf16[4,64,256]{2,1,0:T(8,128)(2,1)S(1)}, bf16[4,64,256]{2,1,0:T(8,128)(2,1)}, u32[]{:S(2)}) copy-start(bf16[4,64,256]{2,1,0:T(8,128)(2,1)} %refs_6_.1) | copy-start | bytes 393220
  8.6 0.8 %copy-start.14 = (bf16[1024,32]{0,1:T(8,128)(2,1)S(1)}, bf16[1024,32]{0,1:T(8,128)(2,1)}, u32[]{:S(2)}) copy-start(bf16[1024,32]{0,1:T(8,128)(2,1)} %param.34) | copy-start | bytes 196612
  9.4 0.7 %copy-start.15 = (bf16[4,1024]{1,0:T(4,128)(2,1)S(1)}, bf16[4,1024]{1,0:T(4,128)(2,1)}, u32[]{:S(2)}) copy-start(bf16[4,1024]{1,0:T(4,128)(2,1)} %refs_5_.3) | copy-start | bytes 24580
  10.1 0.7 %copy-start.17 = (f32[1024]{0:T(1024)S(1)}, f32[1024]{0:T(1024)}, u32[]{:S(2)}) copy-start(f32[1024]{0:T(1024)} %param.28) | copy-start | bytes 12292
  11.3 5.9 %copy-start.24 = (s32[4]{0:T(128)S(1)}, s32[4]{0:T(128)}, u32[]{:S(2)}) copy-start(s32[4]{0:T(128)} %param.25) | copy-start | bytes 52
  11.3 5.8 %collective-permute-start.4 = (bf16[64,1280]{1,0:T(8,128)(2,1)S(1)}, bf16[64,1280]{1,0:T(8,128)(2,1)S(1)}, u32[]{:S(2)}, u32[]{:S(2)}) collective-permute-start(bf16[64,1280]{1,0:T(8,128)(2,1)S(1)} %pad_maximum_fusion.1), channel_id=1, source_target_pairs={{0,1},{1,0},{2,3},{3,2},{4,5},{5,4},{6,7},{7,6},{8,9},{9,8},{10,11... | collective-permute-start | bytes 491528 | tf_op jit(solution)/shard_map/ppermute | solution.py:22
  13.4 4.0 %collective-permute-start.1 = (bf16[4,1408]{1,0:T(4,128)(2,1)S(1)}, bf16[4,1408]{1,0:T(4,128)(2,1)S(1)}, u32[]{:S(2)}, u32[]{:S(2)}) collective-permute-start(bf16[4,1408]{1,0:T(4,128)(2,1)S(1)} %get-tuple-element.23), channel_id=1, source_target_pairs={{0,1},{1,0},{2,3},{3,2},{4,5},{5,4},{6,7},{7,6},{8,9},{9,8},{10,11... | collective-permute-start | bytes 33800 | tf_op jit(solution)/shard_map/ppermute | solution.py:22
  13.5 6.8 %collective-permute-start.3 = (bf16[64,1280]{1,0:T(8,128)(2,1)S(1)}, bf16[64,1280]{1,0:T(8,128)(2,1)S(1)}, u32[]{:S(2)}, u32[]{:S(2)}) collective-permute-start(bf16[64,1280]{1,0:T(8,128)(2,1)S(1)} %collective-permute-done.2.refs_4_), channel_id=1, source_target_pairs={{0,2},{2,0},{4,6},{6,4},{8,10},{10,8},{12,14},{14,12},{16,18},{18,... | collective-permute-start | bytes 491528 | tf_op jit(solution)/shard_map/ppermute | solution.py:356
  17.2 3.7 %collective-permute-start.5 = (bf16[64,1280]{1,0:T(8,128)(2,1)S(1)}, bf16[64,1280]{1,0:T(8,128)(2,1)S(1)}, u32[]{:S(2)}, u32[]{:S(2)}) collective-permute-start(bf16[64,1280]{1,0:T(8,128)(2,1)S(1)} %collective-permute-done.4.refs_3_), channel_id=1, source_target_pairs={{0,2},{2,0},{4,6},{6,4},{8,10},{10,8},{12,14},{14,12},{16,18},{18,... | collective-permute-start | bytes 491528 | tf_op jit(solution)/shard_map/ppermute | solution.py:356
  17.2 1.6 %copy-start = (bf16[4,1024,256]{2,1,0:T(8,128)(2,1)S(1)}, bf16[4,1024,256]{2,1,0:T(8,128)(2,1)}, u32[]{:S(2)}) copy-start(bf16[4,1024,256]{2,1,0:T(8,128)(2,1)} %refs_7_.1) | copy-start | bytes 6291460
  17.2 1.6 %copy-start.5 = (bf16[4,32,1024]{2,1,0:T(8,128)(2,1)S(1)}, bf16[4,32,1024]{2,1,0:T(8,128)(2,1)}, u32[]{:S(2)}) copy-start(bf16[4,32,1024]{2,1,0:T(8,128)(2,1)} %refs_8_.1) | copy-start | bytes 786436
  17.2 1.6 %copy-start.8 = (f32[256]{0:T(256)S(1)}, f32[256]{0:T(256)}, u32[]{:S(2)}) copy-start(f32[256]{0:T(256)} %param.29) | copy-start | bytes 3076
  17.3 3.0 %copy-start.6 = (bf16[256,1024]{1,0:T(8,128)(2,1)S(1)}, bf16[256,1024]{1,0:T(8,128)(2,1)}, u32[]{:S(2)}) copy-start(bf16[256,1024]{1,0:T(8,128)(2,1)} %refs_3_.3) | copy-start | bytes 1572868
  17.3 3.0 %copy-start.7 = (bf16[4,256,64]{1,2,0:T(8,128)(2,1)S(1)}, bf16[4,256,64]{1,2,0:T(8,128)(2,1)}, u32[]{:S(2)}) copy-start(bf16[4,256,64]{1,2,0:T(8,128)(2,1)} %param.37) | copy-start | bytes 393220
  18.8 2.1 %copy-start.16 = (bf16[4,1024]{1,0:T(4,128)(2,1)S(1)}, bf16[4,1024]{1,0:T(4,128)(2,1)}, u32[]{:S(2)}) copy-start(bf16[4,1024]{1,0:T(4,128)(2,1)} %refs_5_.3) | copy-start | bytes 24580
  18.8 2.1 %copy-start.18 = (f32[1024]{0:T(1024)S(1)}, f32[1024]{0:T(1024)}, u32[]{:S(2)}) copy-start(f32[1024]{0:T(1024)} %param.30) | copy-start | bytes 12292
  18.8 2.1 %copy-start.19 = (f32[1024]{0:T(1024)S(1)}, f32[1024]{0:T(1024)}, u32[]{:S(2)}) copy-start(f32[1024]{0:T(1024)} %param.31) | copy-start | bytes 12292
  18.8 2.1 %copy-start.20 = (f32[1024]{0:T(1024)S(1)}, f32[1024]{0:T(1024)}, u32[]{:S(2)}) copy-start(f32[1024]{0:T(1024)} %param.47) | copy-start | bytes 12292
  18.8 2.1 %copy-start.22 = (s32[4,6]{1,0:T(4,128)S(1)}, s32[4,6]{1,0:T(4,128)}, u32[]{:S(2)}) copy-start(s32[4,6]{1,0:T(4,128)} %refs_9_.1) | copy-start | bytes 292
  18.8 2.1 %copy-start.23 = (f32[4,6]{1,0:T(4,128)S(1)}, f32[4,6]{1,0:T(4,128)}, u32[]{:S(2)}) copy-start(f32[4,6]{1,0:T(4,128)} %refs_10_.1) | copy-start | bytes 292
  20.9 15.1 %copy-start.1 = (bf16[1,1024,256]{2,1,0:T(8,128)(2,1)S(1)}, bf16[1,1024,256]{2,1,0:T(8,128)(2,1)}, u32[]{:S(2)}) copy-start(bf16[1,1024,256]{2,1,0:T(8,128)(2,1)} %param.41) | copy-start | bytes 1572868
  20.9 15.1 %copy-start.2 = (bf16[1,1024,256]{2,1,0:T(8,128)(2,1)S(1)}, bf16[1,1024,256]{2,1,0:T(8,128)(2,1)}, u32[]{:S(2)}) copy-start(bf16[1,1024,256]{2,1,0:T(8,128)(2,1)} %param.42) | copy-start | bytes 1572868
  20.9 15.1 %copy-start.3 = (bf16[256,1024]{1,0:T(8,128)(2,1)S(1)}, bf16[256,1024]{1,0:T(8,128)(2,1)}, u32[]{:S(2)}) copy-start(bf16[256,1024]{1,0:T(8,128)(2,1)} %gate_w.1) | copy-start | bytes 1572868
  20.9 15.1 %copy-start.4 = (bf16[256,1024]{1,0:T(8,128)(2,1)S(1)}, bf16[256,1024]{1,0:T(8,128)(2,1)}, u32[]{:S(2)}) copy-start(bf16[256,1024]{1,0:T(8,128)(2,1)} %up_w.1) | copy-start | bytes 1572868
  21.6 15.1 %copy-start.10 = (bf16[1,256,1024]{2,1,0:T(8,128)(2,1)S(1)}, bf16[1,256,1024]{2,1,0:T(8,128)(2,1)}, u32[]{:S(2)}) copy-start(bf16[1,256,1024]{2,1,0:T(8,128)(2,1)} %param.43) | copy-start | bytes 1572868
  21.6 15.1 %copy-start.11 = (bf16[256,1024]{1,0:T(8,128)(2,1)S(1)}, bf16[256,1024]{1,0:T(8,128)(2,1)}, u32[]{:S(2)}) copy-start(bf16[256,1024]{1,0:T(8,128)(2,1)} %down_w.1) | copy-start | bytes 1572868
  36.7 10.9 %copy-start.21 = (f32[1024]{0:T(1024)S(1)}, f32[1024]{0:T(1024)}, u32[]{:S(2)}) copy-start(f32[1024]{0:T(1024)} %param.32) | copy-start | bytes 12292

commit v6 on v5

--- a/solution.py
+++ b/solution.py
@@ -168,21 +168,15 @@
                 attended[s][b : b + 1, h * rank : (h + 1) * rank] = mixed[g : g + 1]
 
 
-def arrived_product(attended, pieces, numbers, heads, cores):
-    width = pieces[0].shape[1] - attended.shape[1] // heads
+def seen_head(attended, n, heads, cores):
     rank = attended.shape[1] // heads
-    per_core = heads // cores
-    core = lax.axis_index("ep") % cores
-    product = jnp.zeros((attended.shape[0], width), f32)
-    for n, piece in zip(numbers, pieces):
-        picked = attended[:, n * rank : (n + 1) * rank]
-        if cores == 2:
-            other = (n + per_core) % heads
-            swapped = attended[:, other * rank : (other + 1) * rank]
-            picked = jnp.where(core == 0, picked.astype(f32), swapped.astype(f32)).astype(bf16)
-        one_head = mm_t(picked, piece[:, width:]).astype(bf16)
-        product = product + mm(one_head, piece[:, :width])
-    return product
+    picked = attended[:, n * rank : (n + 1) * rank]
+    if cores == 2:
+        other = (n + heads // cores) % heads
+        swapped = attended[:, other * rank : (other + 1) * rank]
+        core = lax.axis_index("ep") % cores
+        picked = jnp.where(core == 0, picked.astype(f32), swapped.astype(f32)).astype(bf16)
+    return picked
 
 
 def own_body(blocks, heads, cores, numbers, *refs):
@@ -190,7 +184,8 @@
     value_t, w_out = refs[blocks : blocks + 2]
     count = len(numbers)
     pieces = refs[blocks + 2 : blocks + 2 + (blocks - 1) * count]
-    sums = refs[blocks + 2 + (blocks - 1) * count :]
+    outs_at = refs[blocks + 2 + (blocks - 1) * count :]
+    sums, later = outs_at[:blocks], outs_at[blocks:]
     rank = value_t.shape[1]
     span = value_t.shape[0] // heads
     outs = [
@@ -202,27 +197,36 @@
     ]
     product = mm(jnp.concatenate(outs, axis=-1).astype(bf16), w_out[...])
     sums[0][...] = product.astype(bf16).astype(f32)
+    width = w_out.shape[1]
+    per_core = heads // cores
     for s in range(1, blocks):
-        mine = pieces[(s - 1) * count : s * count]
-        sums[s][...] = arrived_product(attended[s], mine, numbers, heads, cores)
-
-
-def mix_body(blocks, heads, cores, numbers, *refs):
+        product = jnp.zeros(sums[s].shape, f32)
+        waiting = []
+        for n, piece in zip(numbers, pieces[(s - 1) * count : s * count]):
+            for k in range(per_core):
+                values = piece[:, width + k * rank : width + (k + 1) * rank]
+                head_out = mm_t(seen_head(attended[s], n + k, heads, cores), values).astype(bf16)
+                if k == 0:
+                    product = product + mm(head_out, piece[:, :width])
+                else:
+                    waiting.append(head_out)
+        sums[s][...] = product
+        for n, head_out in enumerate(waiting):
+            later[s - 1][n] = head_out
+
+
+def mix_body(blocks, count, *refs):
     sums = refs[:blocks]
-    attended = refs[blocks : 2 * blocks - 1]
-    count = len(numbers)
-    pieces = refs[2 * blocks - 1 : 2 * blocks - 1 + (blocks - 1) * count]
-    rest = refs[2 * blocks - 1 + (blocks - 1) * count :]
+    later = refs[blocks : 2 * blocks - 1] if count else ()
+    pieces = refs[blocks + len(later) : blocks + len(later) + (blocks - 1) * count]
+    rest = refs[blocks + len(later) + (blocks - 1) * count :]
     tokens, post_gain, ffn_gain, gate_vec, routes, route_weights, residual_out, outgoing = rest
     rows, width = tokens.shape
     mixed = sums[0][...]
     for s in range(1, blocks):
         product = sums[s][...]
-        if count:
-            late = pieces[(s - 1) * count : s * count]
-            product = product + arrived_product(
-                attended[s - 1], late, numbers, heads, cores
-            )
+        for n in range(count):
+            product = product + mm(later[s - 1][n], pieces[(s - 1) * count + n][...])
         mixed = mixed + product.astype(bf16).astype(f32)
     residual = (tokens[...].astype(f32) + unit_rows(mixed) * post_gain[...]).astype(bf16)
     residual_out[...] = residual
@@ -341,14 +345,14 @@
     flat_t = value_t.reshape(heads * v_width, rank)
 
     def head_weights(k):
-        start = (core * per_core + k) * v_width
-        return jnp.concatenate(
-            [
-                lax.dynamic_slice_in_dim(w_out, start, v_width),
-                lax.dynamic_slice_in_dim(flat_t, start, v_width),
-            ],
-            axis=1,
-        )
+        first = core * per_core * v_width
+        parts = [lax.dynamic_slice_in_dim(w_out, first + k * v_width, v_width)]
+        if k == 0:
+            parts += [
+                lax.dynamic_slice_in_dim(flat_t, first + n * v_width, v_width)
+                for n in range(per_core)
+            ]
+        return jnp.concatenate(parts, axis=1)
 
     shares = [head_weights(k) for k in range(per_core)]
 
@@ -414,9 +418,10 @@
         8,
         [*packed, position, cosine, sine, rope_key, latent_gain.reshape(1, -1), cache_latent, cache_rope],
     )
-    sums = call(
+    own = call(
         functools.partial(own_body, tp_count, heads, cores, tuple(here)),
-        [((own_rows, model_width), f32)] * tp_count,
+        [((own_rows, model_width), f32)] * tp_count
+        + [((len(last), own_rows, v_width), bf16)] * (tp_count - 1 if last else 0),
         [VMEM] * (tp_count + 2 + (tp_count - 1) * len(here)),
         [],
         1 << 29,
@@ -424,18 +429,17 @@
         [*attended, flat_t, w_out, *[g[n] for g in pieces for n in here]],
     )
     residual, outgoing = call(
-        functools.partial(mix_body, tp_count, heads, cores, tuple(last)),
+        functools.partial(mix_body, tp_count, len(last)),
         [
             ((own_rows, model_width), bf16),
             ((ep_count, own_rows, model_width + extra_width), bf16),
         ],
-        [VMEM] * (2 * tp_count + 5 + (tp_count - 1) * len(last)),
+        [VMEM] * (len(own) + 6 + (tp_count - 1) * len(last)),
         [],
         1 << 32,
         8,
         [
-            *sums,
-            *attended[1:],
+            *own,
             *[g[n] for g in pieces for n in last],
             tokens,
             post_gain.reshape(1, -1),

time: 48.8 us -> 48.6 us (level)
  waiting for transfers between devices: 3.71 us -> 3.03 us
  starting transfers between devices: 5.28 us -> 5.78 us
    ppermute x4, waiting for transfers between devices: 3.7 us -> 3.02 us  [shift(): lax.ppermute(values, axis, [(i, (i + step) % count) for i in range(count)])]
    ppermute x2, starting transfers between devices: 0.01 us -> 0.51 us  [swap_cores(): return lax.ppermute(values, 'ep', [(i, i ^ 1) for i in range(ep_count)])]
where the time goes in v6:
time: 48.6 us; the launch traced here: 48.1 us
  blocking collectives  24.9 us (51%)
  local copies, waits for them, and re-layouts  8.61 us (18%)
  starting transfers between devices  5.78 us (12%)
  Pallas kernels  4.78 us (10%)
  waiting for transfers between devices  3.03 us (6%)
  between operations  0.96 us (2%)
    all_to_all x1, blocking collectives, shards(): lax.all_to_all(outgoing, 'ep', split_axis=0, concat_axis=0, tiled=True)  14.4 us
    all_to_all x1, blocking collectives, shards(): lax.all_to_all(partial.reshape(ep_count, own_rows, model_width), 'ep', sp...  10.5 us
    unnamed x50, local copies, waits for them, and re-layouts  6.74 us
    ppermute x4, starting transfers between devices, shift(): lax.ppermute(values, axis, [(i, (i + step) % count) for i in range(count)])  5.27 us
    pallas_call x9, Pallas kernels, call(): pl.pallas_call(body, out_shape=[jax.ShapeDtypeStruct(s, t) for s, t in sh...  4.78 us
    ppermute x4, waiting for transfers between devices, shift(): lax.ppermute(values, axis, [(i, (i + step) % count) for i in range(count)])  3.02 us
    dynamic_slice x1, local copies, waits for them, and re-layouts, head_weights(): parts = [lax.dynamic_slice_in_dim(w_out, first + k * v_width, v_width)]  0.98 us
  transfers between devices with their start and end apart: 6, of which 1 were waited for; matrix products, arithmetic and copies ran while one was open for 4% of the time, Pallas kernels for 5%

profile of v6, /device:TPU:0, one launch (start us, length us, event | category | flops | bytes accessed | tf_op | source)
XLA Modules:
  0.0 48.1 jit_solution(3217925114939983541)
XLA Ops:
  0.6 3.0 %collective-permute-start = (bf16[4,1024]{1,0:T(4,128)(2,1)}, bf16[4,1024]{1,0:T(4,128)(2,1)S(1)}, u32[]{:S(2)}, u32[]{:S(2)}) collective-permute-start(bf16[4,1024]{1,0:T(4,128)(2,1)} %refs_5_.3), channel_id=1, source_target_pairs={{0,1},{1,0},{2,3},{3,2},{4,5},{5,4},{6,7},{7,6},{8,9},{9,8},{10,11... | collective-permute-start | bytes 24584 | tf_op jit(solution)/shard_map/ppermute | solution.py:22
  3.7 1.0 %constant_dynamic-slice_fusion = (bf16[64,1024]{1,0:T(8,128)(2,1)S(1)}, bf16[64,1024]{1,0:T(8,128)(2,1)S(1)}) fusion(bf16[256,1024]{1,0:T(8,128)(2,1)} %refs_3_.3, s32[]{:T(128)S(6)} %select_n.17, s32[]{:T(128)S(6)} %select_n.16), kind=kLoop, calls=%fused_computation.1 | loop fusion | bytes 524296 | tf_op jit(solution)/shard_map/dynamic_slice | solution.py:349
  4.6 0.8 %constant_dynamic-slice_fusion.2 = (bf16[64,256]{1,0:T(8,128)(2,1)S(1)}, bf16[64,256]{1,0:T(8,128)(2,1)S(1)}) fusion(bf16[256,256]{1,0:T(8,128)(2,1)} %bitcast.16, s32[]{:T(128)S(6)} %select_n.16, s32[]{:T(128)S(6)} %select_n.17), kind=kLoop, calls=%fused_computation.3 | loop fusion | bytes 131080 | tf_op jit(solution)/shard_map/dynamic_slice | solution.py:352
  5.5 0.1 collective-permute-start.2
  5.6 1.1 %copy-done.9 = bf16[1024,384]{1,0:T(8,128)(2,1)S(1)} copy-done((bf16[1024,384]{1,0:T(8,128)(2,1)S(1)}, bf16[1024,384]{1,0:T(8,128)(2,1)}, u32[]{:S(2)}) %copy-start.9) | copy-done | bytes 786456
  6.7 0.9 %copy-done.12 = bf16[1024,128]{1,0:T(8,128)(2,1)S(1)} copy-done((bf16[1024,128]{1,0:T(8,128)(2,1)S(1)}, bf16[1024,128]{1,0:T(8,128)(2,1)}, u32[]{:S(2)}) %copy-start.12) | copy-done | bytes 262168
  7.7 0.9 %copy-done.13 = bf16[4,64,256]{2,1,0:T(8,128)(2,1)S(1)} copy-done((bf16[4,64,256]{2,1,0:T(8,128)(2,1)S(1)}, bf16[4,64,256]{2,1,0:T(8,128)(2,1)}, u32[]{:S(2)}) %copy-start.13) | copy-done | bytes 131096
  8.6 0.8 %copy-done.14 = bf16[1024,32]{0,1:T(8,128)(2,1)S(1)} copy-done((bf16[1024,32]{0,1:T(8,128)(2,1)S(1)}, bf16[1024,32]{0,1:T(8,128)(2,1)}, u32[]{:S(2)}) %copy-start.14) | copy-done | bytes 65560
  9.4 0.7 %copy-done.15 = bf16[4,1024]{1,0:T(4,128)(2,1)S(1)} copy-done((bf16[4,1024]{1,0:T(4,128)(2,1)S(1)}, bf16[4,1024]{1,0:T(4,128)(2,1)}, u32[]{:S(2)}) %copy-start.15) | copy-done | bytes 8216
  10.1 0.7 %copy-done.17 = f32[1024]{0:T(1024)S(1)} copy-done((f32[1024]{0:T(1024)S(1)}, f32[1024]{0:T(1024)}, u32[]{:S(2)}) %copy-start.17) | copy-done | bytes 4120
  10.8 0.5 %shard_map.247 = (bf16[4,1408]{1,0:T(4,128)(2,1)S(1)}, bf16[4,1408]{1,0:T(4,128)(2,1)S(1)}, f32[4,32]{1,0:T(4,128)S(1)}) custom-call(bf16[4,1024]{1,0:T(4,128)(2,1)S(1)} %copy-done.15, bf16[4,1024]{1,0:T(4,128)(2,1)S(1)} %collective-permute-done.refs_1_, f32[1,1024]{1,0:T(1,128)S(1)} %bitcast.21, bf16[1024,128]{1,0:T(8,128)(2,1)S(1)} %copy-done.12, ...), custom_call_target="tpu_custom_call" | custom-call | flops 4294967296 | bytes 1048576 | tf_op jit(solution)/shard_map/pallas_call | solution.py:292
  11.3 0.0 copy-start.24
  11.3 2.0 %collective-permute-start.4 = (bf16[64,1024]{1,0:T(8,128)(2,1)S(1)}, bf16[64,1024]{1,0:T(8,128)(2,1)S(1)}, u32[]{:S(2)}, u32[]{:S(2)}) collective-permute-start(bf16[64,1024]{1,0:T(8,128)(2,1)S(1)} %get-tuple-element.35), channel_id=1, source_target_pairs={{0,1},{1,0},{2,3},{3,2},{4,5},{5,4},{6,7},{7,6},{8,9},{9,8},{10,11... | collective-permute-start | bytes 393224 | tf_op jit(solution)/shard_map/ppermute | solution.py:22
  13.4 0.1 collective-permute-start.1
  13.4 3.0 %collective-permute-done.4.refs_3_ = bf16[64,1024]{1,0:T(8,128)(2,1)S(1)} collective-permute-done((bf16[64,1024]{1,0:T(8,128)(2,1)S(1)}, bf16[64,1024]{1,0:T(8,128)(2,1)S(1)}, u32[]{:S(2)}, u32[]{:S(2)}) %collective-permute-start.4) | collective-permute-done | bytes 131104 | tf_op jit(solution)/shard_map/ppermute | solution.py:22
  16.5 0.5 %collective-permute-start.3 = (bf16[64,1536]{1,0:T(8,128)(2,1)S(1)}, bf16[64,1536]{1,0:T(8,128)(2,1)S(1)}, u32[]{:S(2)}, u32[]{:S(2)}) collective-permute-start(bf16[64,1536]{1,0:T(8,128)(2,1)S(1)} %collective-permute-done.2.refs_4_), channel_id=1, source_target_pairs={{0,2},{2,0},{4,6},{6,4},{8,10},{10,8},{12,14},{14,12},{16,18},{18,... | collective-permute-start | bytes 589832 | tf_op jit(solution)/shard_map/ppermute | solution.py:360
  17.0 0.1 shard_map.249
  17.1 0.0 copy-start.7
  17.1 1.4 %copy-done = bf16[4,1024,256]{2,1,0:T(8,128)(2,1)S(1)} copy-done((bf16[4,1024,256]{2,1,0:T(8,128)(2,1)S(1)}, bf16[4,1024,256]{2,1,0:T(8,128)(2,1)}, u32[]{:S(2)}) %copy-start) | copy-done | bytes 2097176
  18.6 0.0 copy-start.20
  18.6 0.0 copy-start.22
  18.6 1.5 %shard_map.250 = (bf16[4,256]{1,0:T(4,128)(2,1)S(1)}, bf16[4,1024]{1,0:T(4,128)(2,1)S(1)}, bf16[4,1024]{1,0:T(4,128)(2,1)S(1)}) custom-call(bf16[4,1408]{1,0:T(4,128)(2,1)S(1)} %get-tuple-element.23.refs_0_, bf16[4,1408]{1,0:T(4,128)(2,1)S(1)} %collective-permute-done.1.refs_1_, f32[4,1]{1,0:T(4,128)S(1)} %get-tuple-element.26.refs_2_, ...), custom_call_target="tpu_custom_call" | custom-call | flops 536870912 | bytes 1048576 | tf_op jit(solution)/shard_map/pallas_call | solution.py:292
  20.1 0.0 collective-permute-done.3.refs_5_
  20.1 0.6 %shard_map.251 = (f32[4,1024]{1,0:T(4,128)S(1)}, f32[4,1024]{1,0:T(4,128)S(1)}, bf16[2,4,64]{2,1,0:T(4,128)(2,1)S(1)}) custom-call(bf16[4,1024]{1,0:T(4,128)(2,1)S(1)} %get-tuple-element.30.refs_0_, bf16[4,1024]{1,0:T(4,128)(2,1)S(1)} %get-tuple-element.31.refs_1_, bf16[256,256]{1,0:T(8,128)(2,1)S(1)} %bitcast.17, bf16[256,1024]{1,0:T(8,128)(2,1)S(1)} %copy-done.6, ...), custom_call_target="tpu_custom_call" | custom-call | flops 536870912 | bytes 1048576 | tf_op jit(solution)/shard_map/pallas_call | solution.py:292
  20.8 0.0 copy-start.1
  20.8 0.5 shard_map.252
  21.3 14.4 %all_to_all.10 = bf16[16,4,1152]{2,1,0:T(4,128)(2,1)S(1)} all-to-all(bf16[16,4,1152]{2,1,0:T(4,128)(2,1)S(1)} %get-tuple-element.36), channel_id=1, replica_groups=mesh['ep'=16,'tp'=2] {'ep'}, dimensions={0} | all-to-all | bytes 294912 | tf_op jit(solution)/shard_map/all_to_all | solution.py:452
  35.8 0.6 %shard_map.253 = (f32[64,1]{1,0:T(8,128)S(1)}, f32[64,1]{1,0:T(8,128)S(1)}, bf16[64,256]{1,0:T(8,128)(2,1)S(1)}, bf16[64,256]{1,0:T(8,128)(2,1)S(1)}) custom-call(bf16[64,1152]{1,0:T(8,128)(2,1)S(1)} %reshape.43.arrived, bf16[1024,256]{1,0:T(8,128)(2,1)S(1)} %bitcast.14, bf16[1024,256]{1,0:T(8,128)(2,1)S(1)} %bitcast.15, bf16[256,1024]{1,0:T(8,128)(2,1)S(1)} %copy-done.3, ...), custom_call_target="tpu_custom_call" | custom-call | flops 134217728 | bytes 1048576 | tf_op jit(solution)/shard_map/pallas_call | solution.py:292
  36.5 0.3 shard_map.254
  36.8 0.1 reshape.44
  36.8 10.5 %all_to_all.11.returned = bf16[16,4,1024]{2,1,0:T(4,128)(2,1)S(1)} all-to-all(bf16[16,4,1024]{2,1,0:T(4,128)(2,1)S(1)} %reshape.44), channel_id=1, replica_groups=mesh['ep'=16,'tp'=2] {'ep'}, dimensions={0} | all-to-all | bytes 262144 | tf_op jit(solution)/shard_map/all_to_all | solution.py:481
  47.3 0.7 %shard_map.255 = (bf16[4,1024]{1,0:T(4,128)(2,1)}, bf16[4,256]{1,0:T(4,128)(2,1)}, bf16[4,32]{1,0:T(4,128)(2,1)}) custom-call(bf16[16,4,1024]{2,1,0:T(4,128)(2,1)S(1)} %all_to_all.11.returned, bf16[4,1024]{1,0:T(4,128)(2,1)S(1)} %get-tuple-element.41.residual, f32[1,1024]{1,0:T(1,128)S(1)} %bitcast.25, bf16[4,256]{1,0:T(4,128)(2,1)S(1)} %get-tuple-element.42.latent, ...), custom_call_target="tpu_custom_call" | custom-call | flops 1073741824 | bytes 1048576 | tf_op jit(solution)/shard_map/pallas_call | solution.py:292
  (46 shorter events, 0.2 us)
Async XLA Ops:
  0.6 4.9 %collective-permute-start = (bf16[4,1024]{1,0:T(4,128)(2,1)}, bf16[4,1024]{1,0:T(4,128)(2,1)S(1)}, u32[]{:S(2)}, u32[]{:S(2)}) collective-permute-start(bf16[4,1024]{1,0:T(4,128)(2,1)} %refs_5_.3), channel_id=1, source_target_pairs={{0,1},{1,0},{2,3},{3,2},{4,5},{5,4},{6,7},{7,6},{8,9},{9,8},{10,11... | collective-permute-start | bytes 24584 | tf_op jit(solution)/shard_map/ppermute | solution.py:22
  5.5 11.0 %collective-permute-start.2 = (bf16[64,1536]{1,0:T(8,128)(2,1)S(1)}, bf16[64,1536]{1,0:T(8,128)(2,1)S(1)}, u32[]{:S(2)}, u32[]{:S(2)}) collective-permute-start(bf16[64,1536]{1,0:T(8,128)(2,1)S(1)} %pad_maximum_fusion), channel_id=1, source_target_pairs={{0,1},{1,0},{2,3},{3,2},{4,5},{5,4},{6,7},{7,6},{8,9},{9,8},{10,11... | collective-permute-start | bytes 589832 | tf_op jit(solution)/shard_map/ppermute | solution.py:22
  5.6 1.1 %copy-start.9 = (bf16[1024,384]{1,0:T(8,128)(2,1)S(1)}, bf16[1024,384]{1,0:T(8,128)(2,1)}, u32[]{:S(2)}) copy-start(bf16[1024,384]{1,0:T(8,128)(2,1)} %refs_5_.2) | copy-start | bytes 2359300
  6.7 0.9 %copy-start.12 = (bf16[1024,128]{1,0:T(8,128)(2,1)S(1)}, bf16[1024,128]{1,0:T(8,128)(2,1)}, u32[]{:S(2)}) copy-start(bf16[1024,128]{1,0:T(8,128)(2,1)} %refs_3_.2) | copy-start | bytes 786436
  7.7 0.9 %copy-start.13 = (bf16[4,64,256]{2,1,0:T(8,128)(2,1)S(1)}, bf16[4,64,256]{2,1,0:T(8,128)(2,1)}, u32[]{:S(2)}) copy-start(bf16[4,64,256]{2,1,0:T(8,128)(2,1)} %refs_6_.1) | copy-start | bytes 393220
  8.6 0.8 %copy-start.14 = (bf16[1024,32]{0,1:T(8,128)(2,1)S(1)}, bf16[1024,32]{0,1:T(8,128)(2,1)}, u32[]{:S(2)}) copy-start(bf16[1024,32]{0,1:T(8,128)(2,1)} %param.34) | copy-start | bytes 196612
  9.4 0.7 %copy-start.15 = (bf16[4,1024]{1,0:T(4,128)(2,1)S(1)}, bf16[4,1024]{1,0:T(4,128)(2,1)}, u32[]{:S(2)}) copy-start(bf16[4,1024]{1,0:T(4,128)(2,1)} %refs_5_.3) | copy-start | bytes 24580
  10.1 0.7 %copy-start.17 = (f32[1024]{0:T(1024)S(1)}, f32[1024]{0:T(1024)}, u32[]{:S(2)}) copy-start(f32[1024]{0:T(1024)} %param.28) | copy-start | bytes 12292
  11.3 5.7 %copy-start.24 = (s32[4]{0:T(128)S(1)}, s32[4]{0:T(128)}, u32[]{:S(2)}) copy-start(s32[4]{0:T(128)} %param.25) | copy-start | bytes 52
  11.3 5.2 %collective-permute-start.4 = (bf16[64,1024]{1,0:T(8,128)(2,1)S(1)}, bf16[64,1024]{1,0:T(8,128)(2,1)S(1)}, u32[]{:S(2)}, u32[]{:S(2)}) collective-permute-start(bf16[64,1024]{1,0:T(8,128)(2,1)S(1)} %get-tuple-element.35), channel_id=1, source_target_pairs={{0,1},{1,0},{2,3},{3,2},{4,5},{5,4},{6,7},{7,6},{8,9},{9,8},{10,11... | collective-permute-start | bytes 393224 | tf_op jit(solution)/shard_map/ppermute | solution.py:22
  13.4 3.8 %collective-permute-start.1 = (bf16[4,1408]{1,0:T(4,128)(2,1)S(1)}, bf16[4,1408]{1,0:T(4,128)(2,1)S(1)}, u32[]{:S(2)}, u32[]{:S(2)}) collective-permute-start(bf16[4,1408]{1,0:T(4,128)(2,1)S(1)} %get-tuple-element.24), channel_id=1, source_target_pairs={{0,1},{1,0},{2,3},{3,2},{4,5},{5,4},{6,7},{7,6},{8,9},{9,8},{10,11... | collective-permute-start | bytes 33800 | tf_op jit(solution)/shard_map/ppermute | solution.py:22
  16.5 4.2 %collective-permute-start.5 = (bf16[64,1024]{1,0:T(8,128)(2,1)S(1)}, bf16[64,1024]{1,0:T(8,128)(2,1)S(1)}, u32[]{:S(2)}, u32[]{:S(2)}) collective-permute-start(bf16[64,1024]{1,0:T(8,128)(2,1)S(1)} %collective-permute-done.4.refs_3_), channel_id=1, source_target_pairs={{0,2},{2,0},{4,6},{6,4},{8,10},{10,8},{12,14},{14,12},{16,18},{18,... | collective-permute-start | bytes 393224 | tf_op jit(solution)/shard_map/ppermute | solution.py:360
  16.5 3.6 %collective-permute-start.3 = (bf16[64,1536]{1,0:T(8,128)(2,1)S(1)}, bf16[64,1536]{1,0:T(8,128)(2,1)S(1)}, u32[]{:S(2)}, u32[]{:S(2)}) collective-permute-start(bf16[64,1536]{1,0:T(8,128)(2,1)S(1)} %collective-permute-done.2.refs_4_), channel_id=1, source_target_pairs={{0,2},{2,0},{4,6},{6,4},{8,10},{10,8},{12,14},{14,12},{16,18},{18,... | collective-permute-start | bytes 589832 | tf_op jit(solution)/shard_map/ppermute | solution.py:360
  17.0 1.6 %copy-start = (bf16[4,1024,256]{2,1,0:T(8,128)(2,1)S(1)}, bf16[4,1024,256]{2,1,0:T(8,128)(2,1)}, u32[]{:S(2)}) copy-start(bf16[4,1024,256]{2,1,0:T(8,128)(2,1)} %refs_7_.1) | copy-start | bytes 6291460
  17.0 1.6 %copy-start.5 = (bf16[4,32,1024]{2,1,0:T(8,128)(2,1)S(1)}, bf16[4,32,1024]{2,1,0:T(8,128)(2,1)}, u32[]{:S(2)}) copy-start(bf16[4,32,1024]{2,1,0:T(8,128)(2,1)} %refs_8_.1) | copy-start | bytes 786436
  17.0 1.6 %copy-start.8 = (f32[256]{0:T(256)S(1)}, f32[256]{0:T(256)}, u32[]{:S(2)}) copy-start(f32[256]{0:T(256)} %param.29) | copy-start | bytes 3076
  17.1 3.0 %copy-start.6 = (bf16[256,1024]{1,0:T(8,128)(2,1)S(1)}, bf16[256,1024]{1,0:T(8,128)(2,1)}, u32[]{:S(2)}) copy-start(bf16[256,1024]{1,0:T(8,128)(2,1)} %refs_3_.3) | copy-start | bytes 1572868
  17.1 3.0 %copy-start.7 = (bf16[4,256,64]{1,2,0:T(8,128)(2,1)S(1)}, bf16[4,256,64]{1,2,0:T(8,128)(2,1)}, u32[]{:S(2)}) copy-start(bf16[4,256,64]{1,2,0:T(8,128)(2,1)} %param.37) | copy-start | bytes 393220
  18.6 2.1 %copy-start.16 = (bf16[4,1024]{1,0:T(4,128)(2,1)S(1)}, bf16[4,1024]{1,0:T(4,128)(2,1)}, u32[]{:S(2)}) copy-start(bf16[4,1024]{1,0:T(4,128)(2,1)} %refs_5_.3) | copy-start | bytes 24580
  18.6 2.1 %copy-start.18 = (f32[1024]{0:T(1024)S(1)}, f32[1024]{0:T(1024)}, u32[]{:S(2)}) copy-start(f32[1024]{0:T(1024)} %param.30) | copy-start | bytes 12292
  18.6 2.1 %copy-start.19 = (f32[1024]{0:T(1024)S(1)}, f32[1024]{0:T(1024)}, u32[]{:S(2)}) copy-start(f32[1024]{0:T(1024)} %param.31) | copy-start | bytes 12292
  18.6 2.1 %copy-start.20 = (f32[1024]{0:T(1024)S(1)}, f32[1024]{0:T(1024)}, u32[]{:S(2)}) copy-start(f32[1024]{0:T(1024)} %param.47) | copy-start | bytes 12292
  18.6 2.1 %copy-start.22 = (s32[4,6]{1,0:T(4,128)S(1)}, s32[4,6]{1,0:T(4,128)}, u32[]{:S(2)}) copy-start(s32[4,6]{1,0:T(4,128)} %refs_9_.1) | copy-start | bytes 292
  18.6 2.1 %copy-start.23 = (f32[4,6]{1,0:T(4,128)S(1)}, f32[4,6]{1,0:T(4,128)}, u32[]{:S(2)}) copy-start(f32[4,6]{1,0:T(4,128)} %refs_10_.1) | copy-start | bytes 292
  20.8 15.0 %copy-start.1 = (bf16[1,1024,256]{2,1,0:T(8,128)(2,1)S(1)}, bf16[1,1024,256]{2,1,0:T(8,128)(2,1)}, u32[]{:S(2)}) copy-start(bf16[1,1024,256]{2,1,0:T(8,128)(2,1)} %param.41) | copy-start | bytes 1572868
  20.8 15.0 %copy-start.2 = (bf16[1,1024,256]{2,1,0:T(8,128)(2,1)S(1)}, bf16[1,1024,256]{2,1,0:T(8,128)(2,1)}, u32[]{:S(2)}) copy-start(bf16[1,1024,256]{2,1,0:T(8,128)(2,1)} %param.42) | copy-start | bytes 1572868
  20.8 15.0 %copy-start.3 = (bf16[256,1024]{1,0:T(8,128)(2,1)S(1)}, bf16[256,1024]{1,0:T(8,128)(2,1)}, u32[]{:S(2)}) copy-start(bf16[256,1024]{1,0:T(8,128)(2,1)} %gate_w.1) | copy-start | bytes 1572868
  20.8 15.0 %copy-start.4 = (bf16[256,1024]{1,0:T(8,128)(2,1)S(1)}, bf16[256,1024]{1,0:T(8,128)(2,1)}, u32[]{:S(2)}) copy-start(bf16[256,1024]{1,0:T(8,128)(2,1)} %up_w.1) | copy-start | bytes 1572868
  21.3 15.2 %copy-start.10 = (bf16[1,256,1024]{2,1,0:T(8,128)(2,1)S(1)}, bf16[1,256,1024]{2,1,0:T(8,128)(2,1)}, u32[]{:S(2)}) copy-start(bf16[1,256,1024]{2,1,0:T(8,128)(2,1)} %param.43) | copy-start | bytes 1572868
  21.3 15.2 %copy-start.11 = (bf16[256,1024]{1,0:T(8,128)(2,1)S(1)}, bf16[256,1024]{1,0:T(8,128)(2,1)}, u32[]{:S(2)}) copy-start(bf16[256,1024]{1,0:T(8,128)(2,1)} %down_w.1) | copy-start | bytes 1572868
  36.5 10.9 %copy-start.21 = (f32[1024]{0:T(1024)S(1)}, f32[1024]{0:T(1024)}, u32[]{:S(2)}) copy-start(f32[1024]{0:T(1024)} %param.32) | copy-start | bytes 12292

commit v7 on v6

--- a/solution.py
+++ b/solution.py
@@ -256,8 +256,10 @@
 def units_body(experts, arrived, exp_gate, exp_up, gate_w, up_w, *outs):
     weight_out, gate_out, routed_act, dense_act = outs
     width = exp_gate.shape[0]
-    rows = arrived[:, :width]
-    extra = arrived[:, width:].astype(f32)
+    blocks = arrived.shape[0]
+    values = jnp.concatenate([arrived[e].astype(f32) for e in range(blocks)], axis=0)
+    rows = values[:, :width].astype(bf16)
+    extra = values[:, width:]
     lane = lax.broadcasted_iota(jnp.int32, extra.shape, 1)
     mine = lax.axis_index("ep")
     named = jnp.logical_or(lane == mine, lane == mine + experts)
@@ -273,7 +275,10 @@
 def down_body(row_weight, row_gate, routed_act, dense_act, exp_down, down_w, out):
     routed = mm(routed_act[...], exp_down[...]).astype(bf16)
     dense = mm(dense_act[...], down_w[...])
-    out[...] = (row_weight[...] * routed.astype(f32) + row_gate[...] * dense).astype(bf16)
+    total = row_weight[...] * routed.astype(f32) + row_gate[...] * dense
+    rows = out.shape[1]
+    for e in range(out.shape[0]):
+        out[e] = total[e * rows : (e + 1) * rows].astype(bf16)
 
 
 def finish_body(returned, residual, gain, latent, key, out, latent_out, key_out):
@@ -462,7 +467,7 @@
         1<<27,
         8,
         [
-            arrived.reshape(ep_count * own_rows, -1),
+            arrived,
             w_exp_gate[0],
             w_exp_up[0],
             w_dense_gate,
@@ -471,7 +476,7 @@
     )
     (partial,) = call(
         down_body,
-        [((ep_count * own_rows, model_width), bf16)],
+        [((ep_count, own_rows, model_width), bf16)],
         [VMEM] * 6,
         [],
         1 << 31,
@@ -479,7 +484,7 @@
         [*units, w_exp_down[0], w_dense_down],
     )
     returned = lax.all_to_all(
-        partial.reshape(ep_count, own_rows, model_width),
+        partial,
         "ep",
         split_axis=0,
         concat_axis=0,

time: 48.6 us -> 48.5 us (level)
  transfers between devices with their start and end apart: 6 -> 6, of which waited for: 1 -> 1; matrix products, arithmetic and copies ran while one was open for 4% -> 4% of each run, Pallas kernels for 5% -> 6%
where the time goes in v7:
time: 48.5 us; the launch traced here: 48 us
  blocking collectives  24.9 us (51%)
  local copies, waits for them, and re-layouts  8.51 us (18%)
  starting transfers between devices  5.78 us (12%)
  Pallas kernels  4.78 us (10%)
  waiting for transfers between devices  3.03 us (6%)
  between operations  0.93 us (2%)
    all_to_all x1, blocking collectives, shards(): lax.all_to_all(outgoing, 'ep', split_axis=0, concat_axis=0, tiled=True)  14.4 us
    all_to_all x1, blocking collectives, shards(): lax.all_to_all(partial, 'ep', split_axis=0, concat_axis=0, tiled=True)  10.5 us
    unnamed x50, local copies, waits for them, and re-layouts  6.74 us
    ppermute x4, starting transfers between devices, shift(): lax.ppermute(values, axis, [(i, (i + step) % count) for i in range(count)])  5.27 us
    pallas_call x9, Pallas kernels, call(): pl.pallas_call(body, out_shape=[jax.ShapeDtypeStruct(s, t) for s, t in sh...  4.78 us
    ppermute x4, waiting for transfers between devices, shift(): lax.ppermute(values, axis, [(i, (i + step) % count) for i in range(count)])  3.02 us
    dynamic_slice x1, local copies, waits for them, and re-layouts, head_weights(): parts = [lax.dynamic_slice_in_dim(w_out, first + k * v_width, v_width)]  0.98 us
  transfers between devices with their start and end apart: 6, of which 1 were waited for; matrix products, arithmetic and copies ran while one was open for 4% of the time, Pallas kernels for 6%

profile of v7, /device:TPU:0, one launch (start us, length us, event | category | flops | bytes accessed | tf_op | source)
XLA Modules:
  0.0 48.0 jit_solution(15283391783938833071)
XLA Ops:
  0.6 3.0 %collective-permute-start = (bf16[4,1024]{1,0:T(4,128)(2,1)}, bf16[4,1024]{1,0:T(4,128)(2,1)S(1)}, u32[]{:S(2)}, u32[]{:S(2)}) collective-permute-start(bf16[4,1024]{1,0:T(4,128)(2,1)} %refs_5_.3), channel_id=1, source_target_pairs={{0,1},{1,0},{2,3},{3,2},{4,5},{5,4},{6,7},{7,6},{8,9},{9,8},{10,11... | collective-permute-start | bytes 24584 | tf_op jit(solution)/shard_map/ppermute | solution.py:22
  3.7 1.0 %constant_dynamic-slice_fusion = (bf16[64,1024]{1,0:T(8,128)(2,1)S(1)}, bf16[64,1024]{1,0:T(8,128)(2,1)S(1)}) fusion(bf16[256,1024]{1,0:T(8,128)(2,1)} %refs_3_.3, s32[]{:T(128)S(6)} %select_n.17, s32[]{:T(128)S(6)} %select_n.16), kind=kLoop, calls=%fused_computation.1 | loop fusion | bytes 524296 | tf_op jit(solution)/shard_map/dynamic_slice | solution.py:354
  4.6 0.8 %constant_dynamic-slice_fusion.2 = (bf16[64,256]{1,0:T(8,128)(2,1)S(1)}, bf16[64,256]{1,0:T(8,128)(2,1)S(1)}) fusion(bf16[256,256]{1,0:T(8,128)(2,1)} %bitcast.16, s32[]{:T(128)S(6)} %select_n.16, s32[]{:T(128)S(6)} %select_n.17), kind=kLoop, calls=%fused_computation.3 | loop fusion | bytes 131080 | tf_op jit(solution)/shard_map/dynamic_slice | solution.py:357
  5.5 0.1 collective-permute-start.2
  5.6 1.1 %copy-done.9 = bf16[1024,384]{1,0:T(8,128)(2,1)S(1)} copy-done((bf16[1024,384]{1,0:T(8,128)(2,1)S(1)}, bf16[1024,384]{1,0:T(8,128)(2,1)}, u32[]{:S(2)}) %copy-start.9) | copy-done | bytes 786456
  6.7 0.9 %copy-done.12 = bf16[1024,128]{1,0:T(8,128)(2,1)S(1)} copy-done((bf16[1024,128]{1,0:T(8,128)(2,1)S(1)}, bf16[1024,128]{1,0:T(8,128)(2,1)}, u32[]{:S(2)}) %copy-start.12) | copy-done | bytes 262168
  7.7 0.9 %copy-done.13 = bf16[4,64,256]{2,1,0:T(8,128)(2,1)S(1)} copy-done((bf16[4,64,256]{2,1,0:T(8,128)(2,1)S(1)}, bf16[4,64,256]{2,1,0:T(8,128)(2,1)}, u32[]{:S(2)}) %copy-start.13) | copy-done | bytes 131096
  8.6 0.8 %copy-done.14 = bf16[1024,32]{0,1:T(8,128)(2,1)S(1)} copy-done((bf16[1024,32]{0,1:T(8,128)(2,1)S(1)}, bf16[1024,32]{0,1:T(8,128)(2,1)}, u32[]{:S(2)}) %copy-start.14) | copy-done | bytes 65560
  9.4 0.7 %copy-done.15 = bf16[4,1024]{1,0:T(4,128)(2,1)S(1)} copy-done((bf16[4,1024]{1,0:T(4,128)(2,1)S(1)}, bf16[4,1024]{1,0:T(4,128)(2,1)}, u32[]{:S(2)}) %copy-start.15) | copy-done | bytes 8216
  10.1 0.7 %copy-done.17 = f32[1024]{0:T(1024)S(1)} copy-done((f32[1024]{0:T(1024)S(1)}, f32[1024]{0:T(1024)}, u32[]{:S(2)}) %copy-start.17) | copy-done | bytes 4120
  10.8 0.5 %shard_map.247 = (bf16[4,1408]{1,0:T(4,128)(2,1)S(1)}, bf16[4,1408]{1,0:T(4,128)(2,1)S(1)}, f32[4,32]{1,0:T(4,128)S(1)}) custom-call(bf16[4,1024]{1,0:T(4,128)(2,1)S(1)} %copy-done.15, bf16[4,1024]{1,0:T(4,128)(2,1)S(1)} %collective-permute-done.refs_1_, f32[1,1024]{1,0:T(1,128)S(1)} %bitcast.21, bf16[1024,128]{1,0:T(8,128)(2,1)S(1)} %copy-done.12, ...), custom_call_target="tpu_custom_call" | custom-call | flops 4294967296 | bytes 1048576 | tf_op jit(solution)/shard_map/pallas_call | solution.py:297
  11.3 0.0 copy-start.24
  11.3 2.0 %collective-permute-start.4 = (bf16[64,1024]{1,0:T(8,128)(2,1)S(1)}, bf16[64,1024]{1,0:T(8,128)(2,1)S(1)}, u32[]{:S(2)}, u32[]{:S(2)}) collective-permute-start(bf16[64,1024]{1,0:T(8,128)(2,1)S(1)} %get-tuple-element.35), channel_id=1, source_target_pairs={{0,1},{1,0},{2,3},{3,2},{4,5},{5,4},{6,7},{7,6},{8,9},{9,8},{10,11... | collective-permute-start | bytes 393224 | tf_op jit(solution)/shard_map/ppermute | solution.py:22
  13.4 0.1 collective-permute-start.1
  13.4 3.0 %collective-permute-done.4.refs_3_ = bf16[64,1024]{1,0:T(8,128)(2,1)S(1)} collective-permute-done((bf16[64,1024]{1,0:T(8,128)(2,1)S(1)}, bf16[64,1024]{1,0:T(8,128)(2,1)S(1)}, u32[]{:S(2)}, u32[]{:S(2)}) %collective-permute-start.4) | collective-permute-done | bytes 131104 | tf_op jit(solution)/shard_map/ppermute | solution.py:22
  16.5 0.5 %collective-permute-start.3 = (bf16[64,1536]{1,0:T(8,128)(2,1)S(1)}, bf16[64,1536]{1,0:T(8,128)(2,1)S(1)}, u32[]{:S(2)}, u32[]{:S(2)}) collective-permute-start(bf16[64,1536]{1,0:T(8,128)(2,1)S(1)} %collective-permute-done.2.refs_4_), channel_id=1, source_target_pairs={{0,2},{2,0},{4,6},{6,4},{8,10},{10,8},{12,14},{14,12},{16,18},{18,... | collective-permute-start | bytes 589832 | tf_op jit(solution)/shard_map/ppermute | solution.py:365
  17.0 0.1 shard_map.249
  17.1 0.0 copy-start.7
  17.1 1.4 %copy-done = bf16[4,1024,256]{2,1,0:T(8,128)(2,1)S(1)} copy-done((bf16[4,1024,256]{2,1,0:T(8,128)(2,1)S(1)}, bf16[4,1024,256]{2,1,0:T(8,128)(2,1)}, u32[]{:S(2)}) %copy-start) | copy-done | bytes 2097176
  18.6 0.0 copy-start.20
  18.6 0.0 copy-start.22
  18.6 1.5 %shard_map.250 = (bf16[4,256]{1,0:T(4,128)(2,1)S(1)}, bf16[4,1024]{1,0:T(4,128)(2,1)S(1)}, bf16[4,1024]{1,0:T(4,128)(2,1)S(1)}) custom-call(bf16[4,1408]{1,0:T(4,128)(2,1)S(1)} %get-tuple-element.23.refs_0_, bf16[4,1408]{1,0:T(4,128)(2,1)S(1)} %collective-permute-done.1.refs_1_, f32[4,1]{1,0:T(4,128)S(1)} %get-tuple-element.26.refs_2_, ...), custom_call_target="tpu_custom_call" | custom-call | flops 536870912 | bytes 1048576 | tf_op jit(solution)/shard_map/pallas_call | solution.py:297
  20.1 0.0 collective-permute-done.3.refs_5_
  20.1 0.6 %shard_map.251 = (f32[4,1024]{1,0:T(4,128)S(1)}, f32[4,1024]{1,0:T(4,128)S(1)}, bf16[2,4,64]{2,1,0:T(4,128)(2,1)S(1)}) custom-call(bf16[4,1024]{1,0:T(4,128)(2,1)S(1)} %get-tuple-element.30.refs_0_, bf16[4,1024]{1,0:T(4,128)(2,1)S(1)} %get-tuple-element.31.refs_1_, bf16[256,256]{1,0:T(8,128)(2,1)S(1)} %bitcast.17, bf16[256,1024]{1,0:T(8,128)(2,1)S(1)} %copy-done.6, ...), custom_call_target="tpu_custom_call" | custom-call | flops 536870912 | bytes 1048576 | tf_op jit(solution)/shard_map/pallas_call | solution.py:297
  20.8 0.0 copy-start.1
  20.8 0.0 copy-start.4
  20.8 0.5 shard_map.252
  21.3 14.4 %all_to_all.10.arrived = bf16[16,4,1152]{2,1,0:T(4,128)(2,1)S(1)} all-to-all(bf16[16,4,1152]{2,1,0:T(4,128)(2,1)S(1)} %get-tuple-element.36), channel_id=1, replica_groups=mesh['ep'=16,'tp'=2] {'ep'}, dimensions={0} | all-to-all | bytes 294912 | tf_op jit(solution)/shard_map/all_to_all | solution.py:457
  35.7 0.7 %shard_map.253 = (f32[64,1]{1,0:T(8,128)S(1)}, f32[64,1]{1,0:T(8,128)S(1)}, bf16[64,256]{1,0:T(8,128)(2,1)S(1)}, bf16[64,256]{1,0:T(8,128)(2,1)S(1)}) custom-call(bf16[16,4,1152]{2,1,0:T(4,128)(2,1)S(1)} %all_to_all.10.arrived, bf16[1024,256]{1,0:T(8,128)(2,1)S(1)} %bitcast.14, bf16[1024,256]{1,0:T(8,128)(2,1)S(1)} %bitcast.15, ...), custom_call_target="tpu_custom_call" | custom-call | flops 134217728 | bytes 1048576 | tf_op jit(solution)/shard_map/pallas_call | solution.py:297
  36.4 0.3 shard_map.254
  36.7 10.5 %all_to_all.11.returned = bf16[16,4,1024]{2,1,0:T(4,128)(2,1)S(1)} all-to-all(bf16[16,4,1024]{2,1,0:T(4,128)(2,1)S(1)} %shard_map.254), channel_id=1, replica_groups=mesh['ep'=16,'tp'=2] {'ep'}, dimensions={0} | all-to-all | bytes 262144 | tf_op jit(solution)/shard_map/all_to_all | solution.py:486
  47.2 0.7 %shard_map.255 = (bf16[4,1024]{1,0:T(4,128)(2,1)}, bf16[4,256]{1,0:T(4,128)(2,1)}, bf16[4,32]{1,0:T(4,128)(2,1)}) custom-call(bf16[16,4,1024]{2,1,0:T(4,128)(2,1)S(1)} %all_to_all.11.returned, bf16[4,1024]{1,0:T(4,128)(2,1)S(1)} %get-tuple-element.41.residual, f32[1,1024]{1,0:T(1,128)S(1)} %bitcast.25, bf16[4,256]{1,0:T(4,128)(2,1)S(1)} %get-tuple-element.42.latent, ...), custom_call_target="tpu_custom_call" | custom-call | flops 1073741824 | bytes 1048576 | tf_op jit(solution)/shard_map/pallas_call | solution.py:297
  (44 shorter events, 0.1 us)
Async XLA Ops:
  0.6 4.9 %collective-permute-start = (bf16[4,1024]{1,0:T(4,128)(2,1)}, bf16[4,1024]{1,0:T(4,128)(2,1)S(1)}, u32[]{:S(2)}, u32[]{:S(2)}) collective-permute-start(bf16[4,1024]{1,0:T(4,128)(2,1)} %refs_5_.3), channel_id=1, source_target_pairs={{0,1},{1,0},{2,3},{3,2},{4,5},{5,4},{6,7},{7,6},{8,9},{9,8},{10,11... | collective-permute-start | bytes 24584 | tf_op jit(solution)/shard_map/ppermute | solution.py:22
  5.5 11.0 %collective-permute-start.2 = (bf16[64,1536]{1,0:T(8,128)(2,1)S(1)}, bf16[64,1536]{1,0:T(8,128)(2,1)S(1)}, u32[]{:S(2)}, u32[]{:S(2)}) collective-permute-start(bf16[64,1536]{1,0:T(8,128)(2,1)S(1)} %pad_maximum_fusion), channel_id=1, source_target_pairs={{0,1},{1,0},{2,3},{3,2},{4,5},{5,4},{6,7},{7,6},{8,9},{9,8},{10,11... | collective-permute-start | bytes 589832 | tf_op jit(solution)/shard_map/ppermute | solution.py:22
  5.6 1.1 %copy-start.9 = (bf16[1024,384]{1,0:T(8,128)(2,1)S(1)}, bf16[1024,384]{1,0:T(8,128)(2,1)}, u32[]{:S(2)}) copy-start(bf16[1024,384]{1,0:T(8,128)(2,1)} %refs_5_.2) | copy-start | bytes 2359300
  6.7 0.9 %copy-start.12 = (bf16[1024,128]{1,0:T(8,128)(2,1)S(1)}, bf16[1024,128]{1,0:T(8,128)(2,1)}, u32[]{:S(2)}) copy-start(bf16[1024,128]{1,0:T(8,128)(2,1)} %refs_3_.2) | copy-start | bytes 786436
  7.7 0.9 %copy-start.13 = (bf16[4,64,256]{2,1,0:T(8,128)(2,1)S(1)}, bf16[4,64,256]{2,1,0:T(8,128)(2,1)}, u32[]{:S(2)}) copy-start(bf16[4,64,256]{2,1,0:T(8,128)(2,1)} %refs_6_.1) | copy-start | bytes 393220
  8.6 0.8 %copy-start.14 = (bf16[1024,32]{0,1:T(8,128)(2,1)S(1)}, bf16[1024,32]{0,1:T(8,128)(2,1)}, u32[]{:S(2)}) copy-start(bf16[1024,32]{0,1:T(8,128)(2,1)} %param.34) | copy-start | bytes 196612
  9.4 0.7 %copy-start.15 = (bf16[4,1024]{1,0:T(4,128)(2,1)S(1)}, bf16[4,1024]{1,0:T(4,128)(2,1)}, u32[]{:S(2)}) copy-start(bf16[4,1024]{1,0:T(4,128)(2,1)} %refs_5_.3) | copy-start | bytes 24580
  10.1 0.7 %copy-start.17 = (f32[1024]{0:T(1024)S(1)}, f32[1024]{0:T(1024)}, u32[]{:S(2)}) copy-start(f32[1024]{0:T(1024)} %param.28) | copy-start | bytes 12292
  11.3 5.7 %copy-start.24 = (s32[4]{0:T(128)S(1)}, s32[4]{0:T(128)}, u32[]{:S(2)}) copy-start(s32[4]{0:T(128)} %param.25) | copy-start | bytes 52
  11.3 5.2 %collective-permute-start.4 = (bf16[64,1024]{1,0:T(8,128)(2,1)S(1)}, bf16[64,1024]{1,0:T(8,128)(2,1)S(1)}, u32[]{:S(2)}, u32[]{:S(2)}) collective-permute-start(bf16[64,1024]{1,0:T(8,128)(2,1)S(1)} %get-tuple-element.35), channel_id=1, source_target_pairs={{0,1},{1,0},{2,3},{3,2},{4,5},{5,4},{6,7},{7,6},{8,9},{9,8},{10,11... | collective-permute-start | bytes 393224 | tf_op jit(solution)/shard_map/ppermute | solution.py:22
  13.4 3.8 %collective-permute-start.1 = (bf16[4,1408]{1,0:T(4,128)(2,1)S(1)}, bf16[4,1408]{1,0:T(4,128)(2,1)S(1)}, u32[]{:S(2)}, u32[]{:S(2)}) collective-permute-start(bf16[4,1408]{1,0:T(4,128)(2,1)S(1)} %get-tuple-element.24), channel_id=1, source_target_pairs={{0,1},{1,0},{2,3},{3,2},{4,5},{5,4},{6,7},{7,6},{8,9},{9,8},{10,11... | collective-permute-start | bytes 33800 | tf_op jit(solution)/shard_map/ppermute | solution.py:22
  16.5 4.2 %collective-permute-start.5 = (bf16[64,1024]{1,0:T(8,128)(2,1)S(1)}, bf16[64,1024]{1,0:T(8,128)(2,1)S(1)}, u32[]{:S(2)}, u32[]{:S(2)}) collective-permute-start(bf16[64,1024]{1,0:T(8,128)(2,1)S(1)} %collective-permute-done.4.refs_3_), channel_id=1, source_target_pairs={{0,2},{2,0},{4,6},{6,4},{8,10},{10,8},{12,14},{14,12},{16,18},{18,... | collective-permute-start | bytes 393224 | tf_op jit(solution)/shard_map/ppermute | solution.py:365
  16.5 3.6 %collective-permute-start.3 = (bf16[64,1536]{1,0:T(8,128)(2,1)S(1)}, bf16[64,1536]{1,0:T(8,128)(2,1)S(1)}, u32[]{:S(2)}, u32[]{:S(2)}) collective-permute-start(bf16[64,1536]{1,0:T(8,128)(2,1)S(1)} %collective-permute-done.2.refs_4_), channel_id=1, source_target_pairs={{0,2},{2,0},{4,6},{6,4},{8,10},{10,8},{12,14},{14,12},{16,18},{18,... | collective-permute-start | bytes 589832 | tf_op jit(solution)/shard_map/ppermute | solution.py:365
  17.0 1.6 %copy-start = (bf16[4,1024,256]{2,1,0:T(8,128)(2,1)S(1)}, bf16[4,1024,256]{2,1,0:T(8,128)(2,1)}, u32[]{:S(2)}) copy-start(bf16[4,1024,256]{2,1,0:T(8,128)(2,1)} %refs_7_.1) | copy-start | bytes 6291460
  17.0 1.6 %copy-start.5 = (bf16[4,32,1024]{2,1,0:T(8,128)(2,1)S(1)}, bf16[4,32,1024]{2,1,0:T(8,128)(2,1)}, u32[]{:S(2)}) copy-start(bf16[4,32,1024]{2,1,0:T(8,128)(2,1)} %refs_8_.1) | copy-start | bytes 786436
  17.0 1.6 %copy-start.8 = (f32[256]{0:T(256)S(1)}, f32[256]{0:T(256)}, u32[]{:S(2)}) copy-start(f32[256]{0:T(256)} %param.29) | copy-start | bytes 3076
  17.1 3.0 %copy-start.6 = (bf16[256,1024]{1,0:T(8,128)(2,1)S(1)}, bf16[256,1024]{1,0:T(8,128)(2,1)}, u32[]{:S(2)}) copy-start(bf16[256,1024]{1,0:T(8,128)(2,1)} %refs_3_.3) | copy-start | bytes 1572868
  17.1 3.0 %copy-start.7 = (bf16[4,256,64]{1,2,0:T(8,128)(2,1)S(1)}, bf16[4,256,64]{1,2,0:T(8,128)(2,1)}, u32[]{:S(2)}) copy-start(bf16[4,256,64]{1,2,0:T(8,128)(2,1)} %param.37) | copy-start | bytes 393220
  18.6 2.1 %copy-start.16 = (bf16[4,1024]{1,0:T(4,128)(2,1)S(1)}, bf16[4,1024]{1,0:T(4,128)(2,1)}, u32[]{:S(2)}) copy-start(bf16[4,1024]{1,0:T(4,128)(2,1)} %refs_5_.3) | copy-start | bytes 24580
  18.6 2.1 %copy-start.18 = (f32[1024]{0:T(1024)S(1)}, f32[1024]{0:T(1024)}, u32[]{:S(2)}) copy-start(f32[1024]{0:T(1024)} %param.30) | copy-start | bytes 12292
  18.6 2.1 %copy-start.19 = (f32[1024]{0:T(1024)S(1)}, f32[1024]{0:T(1024)}, u32[]{:S(2)}) copy-start(f32[1024]{0:T(1024)} %param.31) | copy-start | bytes 12292
  18.6 2.1 %copy-start.20 = (f32[1024]{0:T(1024)S(1)}, f32[1024]{0:T(1024)}, u32[]{:S(2)}) copy-start(f32[1024]{0:T(1024)} %param.47) | copy-start | bytes 12292
  18.6 2.1 %copy-start.22 = (s32[4,6]{1,0:T(4,128)S(1)}, s32[4,6]{1,0:T(4,128)}, u32[]{:S(2)}) copy-start(s32[4,6]{1,0:T(4,128)} %refs_9_.1) | copy-start | bytes 292
  18.6 2.1 %copy-start.23 = (f32[4,6]{1,0:T(4,128)S(1)}, f32[4,6]{1,0:T(4,128)}, u32[]{:S(2)}) copy-start(f32[4,6]{1,0:T(4,128)} %refs_10_.1) | copy-start | bytes 292
  20.8 15.0 %copy-start.1 = (bf16[1,1024,256]{2,1,0:T(8,128)(2,1)S(1)}, bf16[1,1024,256]{2,1,0:T(8,128)(2,1)}, u32[]{:S(2)}) copy-start(bf16[1,1024,256]{2,1,0:T(8,128)(2,1)} %param.41) | copy-start | bytes 1572868
  20.8 14.9 %copy-start.2 = (bf16[1,1024,256]{2,1,0:T(8,128)(2,1)S(1)}, bf16[1,1024,256]{2,1,0:T(8,128)(2,1)}, u32[]{:S(2)}) copy-start(bf16[1,1024,256]{2,1,0:T(8,128)(2,1)} %param.42) | copy-start | bytes 1572868
  20.8 14.9 %copy-start.3 = (bf16[256,1024]{1,0:T(8,128)(2,1)S(1)}, bf16[256,1024]{1,0:T(8,128)(2,1)}, u32[]{:S(2)}) copy-start(bf16[256,1024]{1,0:T(8,128)(2,1)} %gate_w.1) | copy-start | bytes 1572868
  20.8 14.9 %copy-start.4 = (bf16[256,1024]{1,0:T(8,128)(2,1)S(1)}, bf16[256,1024]{1,0:T(8,128)(2,1)}, u32[]{:S(2)}) copy-start(bf16[256,1024]{1,0:T(8,128)(2,1)} %up_w.1) | copy-start | bytes 1572868
  21.3 15.1 %copy-start.10 = (bf16[1,256,1024]{2,1,0:T(8,128)(2,1)S(1)}, bf16[1,256,1024]{2,1,0:T(8,128)(2,1)}, u32[]{:S(2)}) copy-start(bf16[1,256,1024]{2,1,0:T(8,128)(2,1)} %param.43) | copy-start | bytes 1572868
  21.3 15.1 %copy-start.11 = (bf16[256,1024]{1,0:T(8,128)(2,1)S(1)}, bf16[256,1024]{1,0:T(8,128)(2,1)}, u32[]{:S(2)}) copy-start(bf16[256,1024]{1,0:T(8,128)(2,1)} %down_w.1) | copy-start | bytes 1572868
  36.4 10.8 %copy-start.21 = (f32[1024]{0:T(1024)S(1)}, f32[1024]{0:T(1024)}, u32[]{:S(2)}) copy-start(f32[1024]{0:T(1024)} %param.32) | copy-start | bytes 12292
